TPU v7x, 512 devices: a 8x2x16 block of a 8x16x16 slice. The times are simulated.
512 devices in a mesh: grp: 2 (over y), kv: 16 (over z), tp: 16 (over x, core).
Axes of the slice: x: 8, y: 2, z: 16, core: 2. Of those that a mesh axis runs over, the one named last changes fastest.
The devices are a block of a 8x16x16 slice.
Arguments:
- stream_in: bfloat16 [384, 4096], P(('grp', 'tp'), 'kv'), parts along dimension 0, may hold values from -40 to 40
- positions: int32 [384], P(('grp', 'kv')), parts along dimension 0, may hold values from 1024 to 32767
- ret_state: float32 [384, 16, 128, 128], P(('grp', 'kv'), 'tp'), parts along dimension 0, may hold values from -0.6 to 0.6
- first_gain: float32 [4096], P('kv'), may hold values from 0.1 to 1.9
- first_gate: bfloat16 [4096, 11008], P('kv', 'tp'), may hold values from -0.09375 to 0.09375
- first_up: bfloat16 [4096, 11008], P('kv', 'tp'), may hold values from -0.09375 to 0.09375
- first_down: bfloat16 [11008, 4096], P('tp', 'kv'), may hold values from -0.1875 to 0.1875
- mix_gain: float32 [4096], P('kv'), may hold values from 0.1 to 1.9
- w_query: bfloat16 [4096, 2048], P('kv', 'tp'), may hold values from -0.09375 to 0.09375
- w_key: bfloat16 [4096, 2048], P('kv', 'tp'), may hold values from -0.09375 to 0.09375
- w_value: bfloat16 [4096, 2048], P('kv', 'tp'), may hold values from -0.09375 to 0.09375
- w_outgate: bfloat16 [4096, 2048], P('kv', 'tp'), may hold values from -0.09375 to 0.09375
- w_out: bfloat16 [2048, 4096], P('tp', 'kv'), may hold values from -0.21875 to 0.21875
- head_gain: float32 [2048], P('tp'), may hold values from 0.1 to 1.9
- second_gain: float32 [4096], P('kv'), may hold values from 0.1 to 1.9
- second_gate: bfloat16 [4096, 11008], P('kv', 'tp'), may hold values from -0.09375 to 0.09375
- second_up: bfloat16 [4096, 11008], P('kv', 'tp'), may hold values from -0.09375 to 0.09375
- second_down: bfloat16 [11008, 4096], P('tp', 'kv'), may hold values from -0.1875 to 0.1875
Outputs:
- stream_out: bfloat16 [384, 4096], P(('grp', 'tp'), 'kv'), parts along dimension 0
- new_state: float32 [384, 16, 128, 128], P(('grp', 'kv'), 'tp'), parts along dimension 0
There are 2 independent parts, one for each index of `grp`. A program takes and returns all parts, laid end to end along the dimension named above; an argument that names none is the same for every part. Nothing has to cross between parts.
All inputs are finite; a program needn't handle non-finite values.
Results may differ from a plain program's by a relative error of at most 0.03.
Values may be sent and summed in bfloat16 or wider, within the bound.
No kernel may reach another device: no remote copies, remote signals or barrier semaphores. Data moves between devices by JAX's collectives and lax.ppermute only.
A program may use at most 64 MiB of HBM per device.

v0:
```python
import jax
import jax.numpy as jnp
from jax import lax
from jax.sharding import PartitionSpec as P

D = 4096


EPS_NORM = 1e-06
EPS_GROUP = 1e-05


def in_blocks(x, dim, length):
    lengths = x.shape
    parts = x.reshape(*lengths[:dim], length, lengths[dim] // length, *lengths[dim + 1 :])
    return jnp.moveaxis(parts, dim, 0)


def sent_and_summed(x, axis, dim):
    parts = in_blocks(x, dim, lax.axis_size(axis))
    arrived = lax.all_to_all(parts, axis, split_axis=0, concat_axis=0, tiled=True)
    return arrived.astype(jnp.float32).sum(axis=0)


def sent_together(arrays, axis, dim, along):
    columns = [a.reshape(*a.shape[:along], -1) for a in arrays]
    both = jnp.concatenate(columns, axis=along)
    filled, at, done = (sent_and_summed(both, axis, dim), 0, [])
    for a, column in zip(arrays, columns):
        section = filled[..., at : at + column.shape[along]]
        done.append(section.reshape(*section.shape[:along], *a.shape[along:]))
        at += column.shape[along]
    return tuple(done)


def from_everyone(x, axis):
    length = lax.axis_size(axis)
    return lax.all_to_all(jnp.broadcast_to(x[None], (length, *x.shape)), axis, 0, 0, tiled=True)


def joined_along(parts, dim):
    parts = jnp.moveaxis(parts, 0, dim)
    lengths = parts.shape
    return parts.reshape(*lengths[:dim], lengths[dim] * lengths[dim + 1], *lengths[dim + 2 :])


def collect(x, axis, dim):
    parts = from_everyone(x, axis)
    return joined_along(parts, dim)


def widen_rows(stream_rows):
    return lax.all_gather(stream_rows, "tp", axis=0, tiled=True)


def prepare(stream, norm_gain):
    widened = stream.astype(jnp.float32)
    squares = jnp.sum(widened * widened, axis=1)
    scaled = (widened * norm_gain).astype(jnp.bfloat16)
    return (squares, scaled)


def feed_forward(stream, norm_gain, w_gate, w_up):
    squares, scaled = prepare(stream, norm_gain)
    gate_part = jnp.dot(scaled, w_gate, preferred_element_type=jnp.float32)
    up_part = jnp.dot(scaled, w_up, preferred_element_type=jnp.float32)
    gate_part, up_part, squares = sent_together(
        (
            gate_part.astype(jnp.bfloat16),
            up_part.astype(jnp.bfloat16),
            squares.astype(jnp.bfloat16),
        ),
        "kv",
        0,
        1,
    )
    factor = lax.rsqrt(squares / D + EPS_NORM)[:, None]
    own_hidden = (jax.nn.silu(factor * gate_part) * (factor * up_part)).astype(jnp.bfloat16)
    return collect(own_hidden, "kv", 0)


def advance(stream, inputs_back, weight_back, factor_branch):
    row_count = stream.shape[0] // lax.axis_size("tp")
    row_share = sent_and_summed(
        jnp.dot(inputs_back, weight_back, preferred_element_type=jnp.float32).astype(jnp.bfloat16),
        "tp",
        0,
    )
    own_rows = lax.dynamic_slice_in_dim(stream, lax.axis_index("tp") * row_count, row_count, 0)
    return (own_rows.astype(jnp.float32) + factor_branch * row_share).astype(jnp.bfloat16)


def rotate(values_in, cosine, sine_part):
    half_dim = values_in.shape[-1] // 2
    lower_half = values_in[..., :half_dim]
    upper_half = values_in[..., half_dim:]
    return jnp.concatenate(
        [
            lower_half * cosine - upper_half * sine_part,
            lower_half * sine_part + upper_half * cosine,
        ],
        axis=-1,
    )


def retention(
    stream, norm_gain, w_query, w_key, w_value, w_outgate, head_gain, state_old, positions
):
    squares, scaled = prepare(stream, norm_gain)
    query_part = jnp.dot(scaled, w_query, preferred_element_type=jnp.float32)
    key_part = jnp.dot(scaled, w_key, preferred_element_type=jnp.float32)
    value_part = jnp.dot(scaled, w_value, preferred_element_type=jnp.float32)
    gate_part = jnp.dot(scaled, w_outgate, preferred_element_type=jnp.float32)
    query_part, key_part, value_part, gate_part, squares = sent_together(
        (
            query_part.astype(jnp.bfloat16),
            key_part.astype(jnp.bfloat16),
            value_part.astype(jnp.bfloat16),
            gate_part.astype(jnp.bfloat16),
            squares.astype(jnp.bfloat16),
        ),
        "kv",
        0,
        1,
    )
    factor = lax.rsqrt(squares / D + EPS_NORM)[:, None]
    sequences = state_old.shape[0]
    head_count = state_old.shape[1]
    width_head = state_old.shape[2]
    shape_heads = (sequences, head_count, width_head)
    queries = (factor * query_part).reshape(shape_heads)
    key_vec = (factor * key_part).reshape(shape_heads)
    values_new = (factor * value_part).reshape(shape_heads)
    gate_pre = (factor * gate_part).reshape(shape_heads)
    half_dim = width_head // 2
    inverse = 10000.0 ** (-jnp.arange(half_dim, dtype=jnp.float32) / half_dim)
    angles = positions.astype(jnp.float32)[:, None] * inverse[None, :]
    cosine = jnp.cos(angles)[:, None, :]
    sine_part = jnp.sin(angles)[:, None, :]
    queries = rotate(queries, cosine, sine_part)
    key_vec = rotate(key_vec, cosine, sine_part) * width_head ** (-0.5)
    head_ids = (lax.axis_index("tp") * head_count + jnp.arange(head_count)).astype(jnp.float32)
    decays = jnp.exp(jnp.log1p(-(2.0 ** (-5.0 - head_ids))))
    carried = jnp.einsum("shd,shde->she", queries, state_old, precision=lax.Precision.HIGHEST)
    within = jnp.sum(queries * key_vec, axis=-1, keepdims=True)
    mixture = decays[None, :, None] * carried + within * values_new
    new_state = (
        decays[None, :, None, None] * state_old + key_vec[..., :, None] * values_new[..., None, :]
    )
    average = jnp.mean(mixture, axis=-1, keepdims=True)
    centered = mixture - average
    variance = jnp.mean(centered * centered, axis=-1, keepdims=True)
    normed = centered * lax.rsqrt(variance + EPS_GROUP) * head_gain.reshape(head_count, width_head)
    ret_out = (
        (jax.nn.silu(gate_pre) * normed)
        .astype(jnp.bfloat16)
        .reshape(sequences, head_count * width_head)
    )
    return (collect(ret_out, "kv", 0), new_state)


def per_device(
    stream_in,
    positions,
    ret_state,
    first_gain,
    first_gate,
    first_up,
    first_down,
    mix_gain,
    w_query,
    w_key,
    w_value,
    w_outgate,
    w_out,
    head_gain,
    second_gain,
    second_gate,
    second_up,
    second_down,
):
    stream = widen_rows(stream_in)
    hidden = feed_forward(stream, first_gain, first_gate, first_up)
    stream = advance(stream, hidden, first_down, 0.5)
    stream = widen_rows(stream)
    ret_out, new_state = retention(
        stream, mix_gain, w_query, w_key, w_value, w_outgate, head_gain, ret_state, positions
    )
    stream = advance(stream, ret_out, w_out, 1.0)
    stream = widen_rows(stream)
    hidden = feed_forward(stream, second_gain, second_gate, second_up)
    stream = advance(stream, hidden, second_down, 0.5)
    return (stream, new_state)


def solution(mesh):
    in_specs = (
        P(("grp", "tp"), "kv"),
        P(("grp", "kv")),
        P(("grp", "kv"), "tp", None, None),
        P("kv"),
        P("kv", "tp"),
        P("kv", "tp"),
        P("tp", "kv"),
        P("kv"),
        P("kv", "tp"),
        P("kv", "tp"),
        P("kv", "tp"),
        P("kv", "tp"),
        P("tp", "kv"),
        P("tp"),
        P("kv"),
        P("kv", "tp"),
        P("kv", "tp"),
        P("tp", "kv"),
    )
    out_specs = (P(("grp", "tp"), "kv"), P(("grp", "kv"), "tp", None, None))
    return jax.shard_map(
        per_device, mesh=mesh, in_specs=in_specs, out_specs=out_specs, check_vma=False
    )
```

profile of v0, /device:TPU:65, one launch (start us, length us, event | category | flops | bytes accessed | tf_op | source)
XLA Modules:
  0.0 336.0 jit_solution(10473639947356605988)
XLA Ops:
  0.6 56.3 %all-gather = bf16[16,12,256]{2,1,0:T(8,128)(2,1)S(1)} all-gather(bf16[1,12,256]{2,1,0:T(8,128)(2,1)} %bitcast.43), channel_id=1, replica_groups=mesh['grp'=2,'kv'=16,'tp'=16] {'tp'}, dimensions={0}, use_global_device_ids=true | all-gather | bytes 104448 | tf_op jit(solution)/shard_map/all_gather | solution.py:53
  57.4 1.0 convolution_convert_fusion.2
  59.3 42.3 %all_to_all.45 = bf16[16,12,1377]{2,1,0:T(8,128)(2,1)S(1)} all-to-all(bf16[16,12,1377]{2,1,0:T(8,128)(2,1)S(1)} %concatenate.63), channel_id=1, replica_groups=mesh['grp'=2,'kv'=16,'tp'=16] {'kv'}, dimensions={0} | all-to-all | bytes 1057536 | tf_op jit(solution)/shard_map/all_to_all | solution.py:21
  102.1 26.0 %all_to_all.46 = bf16[16,12,688]{2,1,0:T(8,128)(2,1)S(1)} all-to-all(bf16[16,12,688]{2,1,0:T(8,128)(2,1)S(1)} %broadcast_in_dim.6), channel_id=1, replica_groups=mesh['grp'=2,'kv'=16,'tp'=16] {'kv'}, dimensions={0} | all-to-all | bytes 528384 | tf_op jit(solution)/shard_map/all_to_all | solution.py:38
  128.5 0.7 reshape.328
  129.1 11.7 %all-to-all-start.2 = ((bf16[16,12,256]{2,1,0:T(8,128)(2,1)}), bf16[16,12,256]{2,1,0:T(8,128)(2,1)S(1)}, u32[]{:S(2)}, u32[]{:S(2)}) async-start(bf16[16,12,256]{2,1,0:T(8,128)(2,1)} %reshape.328), calls=%async_computation.2 | async-start | bytes 262144 | tf_op jit(solution)/shard_map/all_to_all | solution.py:21
  140.8 8.9 %all-to-all-done.2 = bf16[16,12,256]{2,1,0:T(8,128)(2,1)S(1)} async-done(((bf16[16,12,256]{2,1,0:T(8,128)(2,1)}), bf16[16,12,256]{2,1,0:T(8,128)(2,1)S(1)}, u32[]{:S(2)}, u32[]{:S(2)}) %all-to-all-start.2) | async-done | bytes 98336 | tf_op jit(solution)/shard_map/all_to_all | solution.py:21
  149.8 14.9 %all-gather.1 = bf16[16,12,256]{2,1,0:T(8,128)(2,1)S(1)} all-gather(bf16[1,12,256]{2,1,0:T(8,128)(2,1)S(1)} %fusion.32), channel_id=1, replica_groups=mesh['grp'=2,'kv'=16,'tp'=16] {'tp'}, dimensions={0}, use_global_device_ids=true | all-gather | bytes 104448 | tf_op jit(solution)/shard_map/all_gather | solution.py:53
  165.9 0.6 constant_dynamic-update-slice_fusion.4
  166.5 0.6 constant_dynamic-update-slice_fusion.3
  169.1 5.7 %all-to-all-start.3 = ((bf16[16,12,513]{2,1,0:T(8,128)(2,1)}), bf16[16,12,513]{2,1,0:T(8,128)(2,1)S(1)}, u32[]{:S(2)}, u32[]{:S(2)}) async-start(bf16[16,12,513]{2,1,0:T(8,128)(2,1)} %constant_dynamic-update-slice_fusion), calls=%async_computation.3 | async-start | bytes 655360 | tf_op jit(solution)/shard_map/all_to_all | solution.py:21
  175.0 15.2 %all-to-all-done.3 = bf16[16,12,513]{2,1,0:T(8,128)(2,1)S(1)} async-done(((bf16[16,12,513]{2,1,0:T(8,128)(2,1)}), bf16[16,12,513]{2,1,0:T(8,128)(2,1)S(1)}, u32[]{:S(2)}, u32[]{:S(2)}) %all-to-all-start.3) | async-done | bytes 197024 | tf_op jit(solution)/shard_map/all_to_all | solution.py:21
  190.6 0.8 fusion
  192.2 22.9 %all_to_all.47 = bf16[16,12,128]{2,1,0:T(8,128)(2,1)S(1)} all-to-all(bf16[16,12,128]{2,1,0:T(8,128)(2,1)S(1)} %broadcast_in_dim.7), channel_id=1, replica_groups=mesh['grp'=2,'kv'=16,'tp'=16] {'kv'}, dimensions={0} | all-to-all | bytes 98304 | tf_op jit(solution)/shard_map/all_to_all | solution.py:38
  215.4 15.6 %all_to_all.48 = bf16[16,12,256]{2,1,0:T(8,128)(2,1)S(1)} all-to-all(bf16[16,12,256]{2,1,0:T(8,128)(2,1)S(1)} %reshape.334), channel_id=1, replica_groups=mesh['grp'=2,'kv'=16,'tp'=16] {'tp'}, dimensions={0} | all-to-all | bytes 196608 | tf_op jit(solution)/shard_map/all_to_all | solution.py:21
  231.1 14.9 %all-gather.2 = bf16[16,12,256]{2,1,0:T(8,128)(2,1)S(1)} all-gather(bf16[1,12,256]{2,1,0:T(8,128)(2,1)S(1)} %fusion.33), channel_id=1, replica_groups=mesh['grp'=2,'kv'=16,'tp'=16] {'tp'}, dimensions={0}, use_global_device_ids=true | all-gather | bytes 104448 | tf_op jit(solution)/shard_map/all_gather | solution.py:53
  247.8 38.5 %all_to_all.49 = bf16[16,12,1377]{2,1,0:T(8,128)(2,1)S(1)} all-to-all(bf16[16,12,1377]{2,1,0:T(8,128)(2,1)S(1)} %concatenate.73), channel_id=1, replica_groups=mesh['grp'=2,'kv'=16,'tp'=16] {'kv'}, dimensions={0} | all-to-all | bytes 1057536 | tf_op jit(solution)/shard_map/all_to_all | solution.py:21
  286.8 0.8 broadcast_in_dim.8
  287.6 8.4 %all-to-all-start.7 = ((bf16[16,12,688]{2,1,0:T(8,128)(2,1)}), bf16[16,12,688]{2,1,0:T(8,128)(2,1)S(1)}, u32[]{:S(2)}, u32[]{:S(2)}) async-start(bf16[16,12,688]{2,1,0:T(8,128)(2,1)} %broadcast_in_dim.8), calls=%async_computation.7 | async-start | bytes 786432 | tf_op jit(solution)/shard_map/all_to_all | solution.py:38
  296.1 17.5 %all-to-all-done.7 = bf16[16,12,688]{2,1,0:T(8,128)(2,1)S(1)} async-done(((bf16[16,12,688]{2,1,0:T(8,128)(2,1)}), bf16[16,12,688]{2,1,0:T(8,128)(2,1)S(1)}, u32[]{:S(2)}, u32[]{:S(2)}) %all-to-all-start.7) | async-done | bytes 264224 | tf_op jit(solution)/shard_map/all_to_all | solution.py:38
  314.0 0.7 reshape.336
  314.7 11.8 %all-to-all-start.8 = ((bf16[16,12,256]{2,1,0:T(8,128)(2,1)}), bf16[16,12,256]{2,1,0:T(8,128)(2,1)S(1)}, u32[]{:S(2)}, u32[]{:S(2)}) async-start(bf16[16,12,256]{2,1,0:T(8,128)(2,1)} %reshape.336), calls=%async_computation.8 | async-start | bytes 262144 | tf_op jit(solution)/shard_map/all_to_all | solution.py:21
  326.4 1.2 multiply_add_fusion
  327.6 7.7 %all-to-all-done.8 = bf16[16,12,256]{2,1,0:T(8,128)(2,1)S(1)} async-done(((bf16[16,12,256]{2,1,0:T(8,128)(2,1)}), bf16[16,12,256]{2,1,0:T(8,128)(2,1)S(1)}, u32[]{:S(2)}, u32[]{:S(2)}) %all-to-all-start.8) | async-done | bytes 98336 | tf_op jit(solution)/shard_map/all_to_all | solution.py:21
  (101 shorter events, 9.9 us)
Async XLA Ops:
  0.6 56.7 %copy-start = (bf16[256,688]{0,1:T(8,128)(2,1)S(1)}, bf16[256,688]{0,1:T(8,128)(2,1)}, u32[]{:S(2)}) copy-start(bf16[256,688]{0,1:T(8,128)(2,1)} %param.23) | copy-start | bytes 1056772
  57.0 1.4 copy-start.2
  57.0 1.4 copy-start.13
  102.1 26.1 %copy-start.3 = (bf16[688,256]{1,0:T(8,128)(2,1)S(1)}, bf16[688,256]{1,0:T(8,128)(2,1)}, u32[]{:S(2)}) copy-start(bf16[688,256]{1,0:T(8,128)(2,1)} %param.24) | copy-start | bytes 1056772
  128.2 36.6 %copy-start.7 = (bf16[256,128]{1,0:T(8,128)(2,1)S(1)}, bf16[256,128]{1,0:T(8,128)(2,1)}, u32[]{:S(2)}) copy-start(bf16[256,128]{1,0:T(8,128)(2,1)} %param.27) | copy-start | bytes 196612
  128.2 36.6 %copy-start.12 = (f32[256]{0:T(256)S(1)}, f32[256]{0:T(256)}, u32[]{:S(2)}) copy-start(f32[256]{0:T(256)} %param.25) | copy-start | bytes 3076
  128.4 36.6 %copy-start.8 = (bf16[256,128]{1,0:T(8,128)(2,1)S(1)}, bf16[256,128]{1,0:T(8,128)(2,1)}, u32[]{:S(2)}) copy-start(bf16[256,128]{1,0:T(8,128)(2,1)} %param.28) | copy-start | bytes 196612
  129.1 36.1 %copy-start.9 = (bf16[256,128]{1,0:T(8,128)(2,1)S(1)}, bf16[256,128]{1,0:T(8,128)(2,1)}, u32[]{:S(2)}) copy-start(bf16[256,128]{1,0:T(8,128)(2,1)} %param.29) | copy-start | bytes 196612
  129.1 20.6 %all-to-all-start.2 = ((bf16[16,12,256]{2,1,0:T(8,128)(2,1)}), bf16[16,12,256]{2,1,0:T(8,128)(2,1)S(1)}, u32[]{:S(2)}, u32[]{:S(2)}) async-start(bf16[16,12,256]{2,1,0:T(8,128)(2,1)} %reshape.328), calls=%async_computation.2 | async-start | bytes 262144 | tf_op jit(solution)/shard_map/all_to_all | solution.py:21
  140.8 24.6 %copy-start.10 = (bf16[256,128]{1,0:T(8,128)(2,1)S(1)}, bf16[256,128]{1,0:T(8,128)(2,1)}, u32[]{:S(2)}) copy-start(bf16[256,128]{1,0:T(8,128)(2,1)} %param.26) | copy-start | bytes 196612
  165.6 9.3 %copy-start.16 = (s32[12]{0:T(128)S(1)}, s32[12]{0:T(128)}, u32[]{:S(2)}) copy-start(s32[12]{0:T(128)} %param.19) | copy-start | bytes 148
  167.1 23.5 %copy-start.1 = (f32[12,1,128,128]{3,2,1,0:T(8,128)S(1)}, f32[12,1,128,128]{3,2,1,0:T(8,128)}, u32[]{:S(2)}) copy-start(f32[12,1,128,128]{3,2,1,0:T(8,128)} %param.20) | copy-start | bytes 2359300
  169.1 21.1 %all-to-all-start.3 = ((bf16[16,12,513]{2,1,0:T(8,128)(2,1)}), bf16[16,12,513]{2,1,0:T(8,128)(2,1)S(1)}, u32[]{:S(2)}, u32[]{:S(2)}) async-start(bf16[16,12,513]{2,1,0:T(8,128)(2,1)} %constant_dynamic-update-slice_fusion), calls=%async_computation.3 | async-start | bytes 655360 | tf_op jit(solution)/shard_map/all_to_all | solution.py:21
  174.8 17.3 %copy-start.15 = (f32[128]{0:T(128)S(1)}, f32[128]{0:T(128)}, u32[]{:S(2)}) copy-start(f32[128]{0:T(128)} %param.31) | copy-start | bytes 1540
  190.2 25.0 %copy-start.11 = (bf16[128,256]{1,0:T(8,128)(2,1)S(1)}, bf16[128,256]{1,0:T(8,128)(2,1)}, u32[]{:S(2)}) copy-start(bf16[128,256]{1,0:T(8,128)(2,1)} %param.30) | copy-start | bytes 196612
  215.1 31.2 %copy-start.4 = (bf16[256,688]{0,1:T(8,128)(2,1)S(1)}, bf16[256,688]{0,1:T(8,128)(2,1)}, u32[]{:S(2)}) copy-start(bf16[256,688]{0,1:T(8,128)(2,1)} %param.34) | copy-start | bytes 1056772
  215.1 31.3 %copy-start.14 = (f32[256]{0:T(256)S(1)}, f32[256]{0:T(256)}, u32[]{:S(2)}) copy-start(f32[256]{0:T(256)} %param.32) | copy-start | bytes 3076
  246.0 1.0 copy-start.5
  287.6 26.2 %copy-start.6 = (bf16[688,256]{1,0:T(8,128)(2,1)S(1)}, bf16[688,256]{1,0:T(8,128)(2,1)}, u32[]{:S(2)}) copy-start(bf16[688,256]{1,0:T(8,128)(2,1)} %param.35) | copy-start | bytes 1056772
  287.6 26.0 %all-to-all-start.7 = ((bf16[16,12,688]{2,1,0:T(8,128)(2,1)}), bf16[16,12,688]{2,1,0:T(8,128)(2,1)S(1)}, u32[]{:S(2)}, u32[]{:S(2)}) async-start(bf16[16,12,688]{2,1,0:T(8,128)(2,1)} %broadcast_in_dim.8), calls=%async_computation.7 | async-start | bytes 786432 | tf_op jit(solution)/shard_map/all_to_all | solution.py:38
  314.7 20.7 %all-to-all-start.8 = ((bf16[16,12,256]{2,1,0:T(8,128)(2,1)}), bf16[16,12,256]{2,1,0:T(8,128)(2,1)S(1)}, u32[]{:S(2)}, u32[]{:S(2)}) async-start(bf16[16,12,256]{2,1,0:T(8,128)(2,1)} %reshape.336), calls=%async_computation.8 | async-start | bytes 262144 | tf_op jit(solution)/shard_map/all_to_all | solution.py:21
where the time goes:
time: 337 us; the launch traced here: 336 us
  blocking collectives  232 us (69%)
  waiting for transfers between devices  49.3 us (15%)
  starting transfers between devices  37.6 us (11%)
  local copies, waits for them, and re-layouts  8.12 us (2%)
  other arithmetic  4.29 us (1%)
  matrix products  3.82 us (1%)
    all_to_all x3, blocking collectives, sent_and_summed(): lax.all_to_all(parts, axis, split_axis=0, concat_axis=0, tiled=True)  96.5 us
    all_gather x3, blocking collectives, widen_rows(): return lax.all_gather(stream_rows, 'tp', axis=0, tiled=True)  86.1 us
    all_to_all x2, blocking collectives, from_everyone(): lax.all_to_all(jnp.broadcast_to(x[None], (length, *x.shape)), axis, 0, 0,...  48.9 us
    all_to_all x3, waiting for transfers between devices, sent_and_summed(): lax.all_to_all(parts, axis, split_axis=0, concat_axis=0, tiled=True)  31.8 us
    all_to_all x3, starting transfers between devices, sent_and_summed(): lax.all_to_all(parts, axis, split_axis=0, concat_axis=0, tiled=True)  29.2 us
    all_to_all x1, waiting for transfers between devices, from_everyone(): lax.all_to_all(jnp.broadcast_to(x[None], (length, *x.shape)), axis, 0, 0,...  17.5 us
    all_to_all x1, starting transfers between devices, from_everyone(): lax.all_to_all(jnp.broadcast_to(x[None], (length, *x.shape)), axis, 0, 0,...  8.45 us
  transfers between devices with their start and end apart: 4, of which 4 were waited for; matrix products, arithmetic and copies ran while one was open for 0% of the time, Pallas kernels for 0%

commit v1 on v0

v1 whole, which is shorter than its diff:
```python
import jax
import jax.numpy as jnp
from jax import lax
from jax.sharding import PartitionSpec as P

EPS_NORM = 1e-06
EPS_GROUP = 1e-05
CHAINS = ((0, 8), (8, 4))


def exchange(x, axis):
    return lax.all_to_all(x, axis, split_axis=0, concat_axis=0, tiled=True)


def summed(x, axis):
    return exchange(x, axis).astype(jnp.float32).sum(axis=0)


def spread(x, axis):
    return exchange(jnp.broadcast_to(x[None], (lax.axis_size(axis), *x.shape)), axis)


def prepare(stream, norm_gain):
    widened = stream.astype(jnp.float32)
    squares = jnp.sum(widened * widened, axis=1, keepdims=True).astype(jnp.bfloat16)
    return squares, (widened * norm_gain).astype(jnp.bfloat16)


def dot(a, b):
    return jnp.dot(a, b, preferred_element_type=jnp.float32)


def feed_forward(stream, norm_gain, w_gate, w_up, w_down):
    members = lax.axis_size("kv")
    rows, width = stream.shape[0], w_gate.shape[1]
    tall = rows // members
    cuts = 1
    while (tall * cuts) % 8:
        cuts *= 2
    tall, part = tall * cuts, width // cuts
    features = lax.axis_size("kv") * stream.shape[1]
    squares, scaled = prepare(stream, norm_gain)
    pieces = []
    for c in range(cuts):
        gate = dot(scaled, w_gate[:, c * part : (c + 1) * part]).astype(jnp.bfloat16)
        up = dot(scaled, w_up[:, c * part : (c + 1) * part]).astype(jnp.bfloat16)
        piece = jnp.concatenate([gate, up, squares], axis=1)
        pieces.append(piece.reshape(members // cuts, tall, 2 * part + 1))
    sent = pieces[0] if cuts == 1 else jnp.stack(pieces, axis=1).reshape(members, tall, 2 * part + 1)
    total = summed(sent, "kv")
    factor = lax.rsqrt(total[:, 2 * part :] / features + EPS_NORM)
    hidden = (jax.nn.silu(factor * total[:, :part]) * (factor * total[:, part : 2 * part])).astype(jnp.bfloat16)
    everyone = spread(hidden, "kv").reshape(members // cuts, cuts, tall, part)
    back = 0.0
    for c in range(cuts):
        back += dot(everyone[:, c].reshape(rows, part), w_down[c * part : (c + 1) * part])
    return back


def advance(own, back, branch):
    members = lax.axis_size("tp")
    share = summed(back.astype(jnp.bfloat16).reshape(members, -1, back.shape[1]), "tp")
    return (own.astype(jnp.float32) + branch * share).astype(jnp.bfloat16)


def widen(own):
    gathered = spread(own, "tp")
    return gathered.reshape(-1, own.shape[1])


def rotate(values_in, cosine, sine):
    half = values_in.shape[-1] // 2
    low, high = values_in[..., :half], values_in[..., half:]
    return jnp.concatenate([low * cosine - high * sine, low * sine + high * cosine], axis=-1)


def retention(stream, norm_gain, w_heads, head_gain, state, positions):
    members = lax.axis_size("kv")
    features = members * stream.shape[1]
    squares, scaled = prepare(stream, norm_gain)
    parts = [dot(scaled, w).astype(jnp.bfloat16) for w in w_heads]
    sent = jnp.concatenate([*parts, squares], axis=1).reshape(members, -1, 4 * parts[0].shape[1] + 1)
    total = summed(sent, "kv")
    count, heads, width, _ = state.shape
    factor = lax.rsqrt(total[:, 4 * heads * width :] / features + EPS_NORM)
    shape = (count, heads, width)
    q, k, v, o = ((factor * total[:, i * heads * width : (i + 1) * heads * width]).reshape(shape) for i in range(4))
    half = width // 2
    inverse = 10000.0 ** (-jnp.arange(half, dtype=jnp.float32) / half)
    angles = positions.astype(jnp.float32)[:, None] * inverse[None, :]
    cosine, sine = jnp.cos(angles)[:, None, :], jnp.sin(angles)[:, None, :]
    q = rotate(q, cosine, sine)
    k = rotate(k, cosine, sine) * width ** (-0.5)
    head_ids = (lax.axis_index("tp") * heads + jnp.arange(heads)).astype(jnp.float32)
    decays = jnp.exp(jnp.log1p(-(2.0 ** (-5.0 - head_ids))))
    carried = jnp.einsum("shd,shde->she", q, state, precision=lax.Precision.HIGHEST)
    within = jnp.sum(q * k, axis=-1, keepdims=True)
    mixture = decays[None, :, None] * carried + within * v
    centered = mixture - jnp.mean(mixture, axis=-1, keepdims=True)
    variance = jnp.mean(centered * centered, axis=-1, keepdims=True)
    normed = centered * lax.rsqrt(variance + EPS_GROUP) * head_gain.reshape(heads, width)
    ret_out = (jax.nn.silu(o) * normed).astype(jnp.bfloat16).reshape(count, heads * width)
    new_state = decays[None, :, None, None] * state + k[..., :, None] * v[..., None, :]
    return spread(ret_out, "kv").reshape(stream.shape[0], heads * width), new_state


def per_device(
    stream_in,
    positions,
    ret_state,
    first_gain,
    first_gate,
    first_up,
    first_down,
    mix_gain,
    w_query,
    w_key,
    w_value,
    w_outgate,
    w_out,
    head_gain,
    second_gain,
    second_gate,
    second_up,
    second_down,
):
    outs, states = [], []
    for start, count in CHAINS:
        own = stream_in[start : start + count]
        stream = widen(own)
        back = feed_forward(stream, first_gain, first_gate, first_up, first_down)
        own = advance(own, back, 0.5)
        stream = widen(own)
        ret_out, state = retention(
            stream,
            mix_gain,
            (w_query, w_key, w_value, w_outgate),
            head_gain,
            ret_state[start : start + count],
            positions[start : start + count],
        )
        own = advance(own, dot(ret_out, w_out), 1.0)
        stream = widen(own)
        back = feed_forward(stream, second_gain, second_gate, second_up, second_down)
        outs.append(advance(own, back, 0.5))
        states.append(state)
    return jnp.concatenate(outs, axis=0), jnp.concatenate(states, axis=0)


def solution(mesh):
    in_specs = (
        P(("grp", "tp"), "kv"),
        P(("grp", "kv")),
        P(("grp", "kv"), "tp", None, None),
        P("kv"),
        P("kv", "tp"),
        P("kv", "tp"),
        P("tp", "kv"),
        P("kv"),
        P("kv", "tp"),
        P("kv", "tp"),
        P("kv", "tp"),
        P("kv", "tp"),
        P("tp", "kv"),
        P("tp"),
        P("kv"),
        P("kv", "tp"),
        P("kv", "tp"),
        P("tp", "kv"),
    )
    out_specs = (P(("grp", "tp"), "kv"), P(("grp", "kv"), "tp", None, None))
    return jax.shard_map(
        per_device, mesh=mesh, in_specs=in_specs, out_specs=out_specs, check_vma=False
    )
```

time: 337 us -> 456 us (1.35)
  waiting for transfers between devices: 49.3 us -> 210 us
  blocking collectives: 232 us -> 71.6 us
  starting transfers between devices: 37.6 us -> 131 us
  local copies, waits for them, and re-layouts: 8.12 us -> 22.3 us
  matrix products: 3.82 us -> 11.1 us
    all_to_all x4 -> x22, waiting for transfers between devices: 49.3 us -> 210 us  [exchange(): return lax.all_to_all(x, axis, split_axis=0, concat_axis=0, tiled=True)]
    all_to_all x4 -> x22, starting transfers between devices: 37.6 us -> 131 us  [exchange(): return lax.all_to_all(x, axis, split_axis=0, concat_axis=0, tiled=True)]
    all_gather x3 -> x0, blocking collectives: 86.1 us -> none  [widen_rows(): return lax.all_gather(stream_rows, 'tp', axis=0, tiled=True)]
    all_to_all x5 -> x2, blocking collectives: 145 us -> 71.6 us  [exchange(): return lax.all_to_all(x, axis, split_axis=0, concat_axis=0, tiled=True)]
    dot_general x12 -> x30, matrix products: 3.82 us -> 11.1 us  [the longest x28 10.3 us: dot(): return jnp.dot(a, b, preferred_element_type=jnp.float32)]
    broadcast_in_dim x3 -> x12, local copies, waits for them, and re-layouts: 0.81 us -> 7.07 us  [spread(): jnp.broadcast_to(x[None], (lax.axis_size(axis), *x.shape))]
    unnamed x41, local copies, waits for them, and re-layouts: 2.95 us -> 7.95 us
  transfers between devices with their start and end apart: 4 -> 22, of which waited for: 4 -> 22; matrix products, arithmetic and copies ran while one was open for 0% -> 2% of each run, Pallas kernels for 0% -> 0%
where the time goes in v1:
time: 456 us; the launch traced here: 454 us
  waiting for transfers between devices  210 us (46%)
  starting transfers between devices  131 us (29%)
  blocking collectives  71.6 us (16%)
  local copies, waits for them, and re-layouts  22.3 us (5%)
  matrix products  11.1 us (2%)
  other arithmetic  7.69 us (2%)
    all_to_all x22, waiting for transfers between devices, exchange(): return lax.all_to_all(x, axis, split_axis=0, concat_axis=0, tiled=True)  210 us
    all_to_all x22, starting transfers between devices, exchange(): return lax.all_to_all(x, axis, split_axis=0, concat_axis=0, tiled=True)  131 us
    all_to_all x2, blocking collectives, exchange(): return lax.all_to_all(x, axis, split_axis=0, concat_axis=0, tiled=True)  71.6 us
    dot_general x28, matrix products, dot(): return jnp.dot(a, b, preferred_element_type=jnp.float32)  10.3 us
  transfers between devices with their start and end apart: 22, of which 22 were waited for; matrix products, arithmetic and copies ran while one was open for 2% of the time, Pallas kernels for 0%

profile of v1, /device:TPU:65, one launch (start us, length us, event | category | flops | bytes accessed | tf_op | source)
XLA Modules:
  0.0 454.4 jit_solution(4476503734597790470)
XLA Ops:
  1.4 51.5 %all_to_all.120 = bf16[16,4,256]{2,1,0:T(4,128)(2,1)S(1)} all-to-all(bf16[16,4,256]{2,1,0:T(4,128)(2,1)S(1)} %broadcast_in_dim.30), channel_id=1, replica_groups=mesh['grp'=2,'kv'=16,'tp'=16] {'tp'}, dimensions={0} | all-to-all | bytes 65536 | tf_op jit(solution)/shard_map/all_to_all | solution.py:12
  55.6 20.1 %all_to_all.121 = bf16[16,8,689]{2,1,0:T(8,128)(2,1)S(1)} all-to-all(bf16[16,8,689]{2,1,0:T(8,128)(2,1)S(1)} %bitcast.185), channel_id=1, replica_groups=mesh['grp'=2,'kv'=16,'tp'=16] {'kv'}, dimensions={0} | all-to-all | bytes 352768 | tf_op jit(solution)/shard_map/all_to_all | solution.py:12
  76.7 8.9 %all-to-all-start.14 = ((bf16[16,8,344]{2,1,0:T(8,128)(2,1)}), bf16[16,8,344]{2,1,0:T(8,128)(2,1)S(1)}, u32[]{:S(2)}, u32[]{:S(2)}) async-start(bf16[16,8,344]{2,1,0:T(8,128)(2,1)} %broadcast_in_dim.31), calls=%async_computation.14 | async-start | bytes 196608 | tf_op jit(solution)/shard_map/all_to_all | solution.py:12
  86.5 10.8 %all-to-all-done.14 = bf16[16,8,344]{2,1,0:T(8,128)(2,1)S(1)} async-done(((bf16[16,8,344]{2,1,0:T(8,128)(2,1)}), bf16[16,8,344]{2,1,0:T(8,128)(2,1)S(1)}, u32[]{:S(2)}, u32[]{:S(2)}) %all-to-all-start.14) | async-done | bytes 88096 | tf_op jit(solution)/shard_map/all_to_all | solution.py:12
  104.5 7.6 %all-to-all-done.15 = bf16[16,4,256]{2,1,0:T(4,128)(2,1)S(1)} async-done(((bf16[16,4,256]{2,1,0:T(4,128)(2,1)}), bf16[16,4,256]{2,1,0:T(4,128)(2,1)S(1)}, u32[]{:S(2)}, u32[]{:S(2)}) %all-to-all-start.15) | async-done | bytes 32800 | tf_op jit(solution)/shard_map/all_to_all | solution.py:12
  149.0 9.5 %all-to-all-done.17 = bf16[16,4,513]{2,1,0:T(4,128)(2,1)S(1)} async-done(((bf16[16,4,513]{2,1,0:T(4,128)(2,1)}), bf16[16,4,513]{2,1,0:T(4,128)(2,1)S(1)}, u32[]{:S(2)}, u32[]{:S(2)}) %all-to-all-start.17) | async-done | bytes 65696 | tf_op jit(solution)/shard_map/all_to_all | solution.py:12
  165.2 13.8 %all-to-all-done.1 = bf16[16,8,1377]{2,1,0:T(8,128)(2,1)S(1)} async-done(((bf16[16,8,1377]{2,1,0:T(8,128)(2,1)}), bf16[16,8,1377]{2,1,0:T(8,128)(2,1)S(1)}, u32[]{:S(2)}, u32[]{:S(2)}) %all-to-all-start.1) | async-done | bytes 352544 | tf_op jit(solution)/shard_map/all_to_all | solution.py:12
  179.6 12.5 %all-to-all-start.18 = ((bf16[16,4,128]{2,1,0:T(4,128)(2,1)}), bf16[16,4,128]{2,1,0:T(4,128)(2,1)S(1)}, u32[]{:S(2)}, u32[]{:S(2)}) async-start(bf16[16,4,128]{2,1,0:T(4,128)(2,1)} %broadcast_in_dim.33), calls=%async_computation.18 | async-start | bytes 32768 | tf_op jit(solution)/shard_map/all_to_all | solution.py:12
  192.3 10.9 %all-to-all-done.18 = bf16[16,4,128]{2,1,0:T(4,128)(2,1)S(1)} async-done(((bf16[16,4,128]{2,1,0:T(4,128)(2,1)}), bf16[16,4,128]{2,1,0:T(4,128)(2,1)S(1)}, u32[]{:S(2)}, u32[]{:S(2)}) %all-to-all-start.18) | async-done | bytes 16416 | tf_op jit(solution)/shard_map/all_to_all | solution.py:12
  221.9 12.9 %all-to-all-done.2 = bf16[16,8,688]{2,1,0:T(8,128)(2,1)S(1)} async-done(((bf16[16,8,688]{2,1,0:T(8,128)(2,1)}), bf16[16,8,688]{2,1,0:T(8,128)(2,1)S(1)}, u32[]{:S(2)}, u32[]{:S(2)}) %all-to-all-start.2) | async-done | bytes 176160 | tf_op jit(solution)/shard_map/all_to_all | solution.py:12
  242.2 7.9 %all-to-all-done.3 = bf16[16,8,256]{2,1,0:T(8,128)(2,1)S(1)} async-done(((bf16[16,8,256]{2,1,0:T(8,128)(2,1)}), bf16[16,8,256]{2,1,0:T(8,128)(2,1)S(1)}, u32[]{:S(2)}, u32[]{:S(2)}) %all-to-all-start.3) | async-done | bytes 65568 | tf_op jit(solution)/shard_map/all_to_all | solution.py:12
  254.4 7.6 %all-to-all-done.20 = bf16[16,4,256]{2,1,0:T(4,128)(2,1)S(1)} async-done(((bf16[16,4,256]{2,1,0:T(4,128)(2,1)}), bf16[16,4,256]{2,1,0:T(4,128)(2,1)S(1)}, u32[]{:S(2)}, u32[]{:S(2)}) %all-to-all-start.20) | async-done | bytes 32800 | tf_op jit(solution)/shard_map/all_to_all | solution.py:12
  266.4 7.9 %all-to-all-done.4 = bf16[16,8,256]{2,1,0:T(8,128)(2,1)S(1)} async-done(((bf16[16,8,256]{2,1,0:T(8,128)(2,1)}), bf16[16,8,256]{2,1,0:T(8,128)(2,1)S(1)}, u32[]{:S(2)}, u32[]{:S(2)}) %all-to-all-start.4) | async-done | bytes 65568 | tf_op jit(solution)/shard_map/all_to_all | solution.py:12
  285.5 10.7 %all-to-all-done.5 = bf16[16,8,513]{2,1,0:T(8,128)(2,1)S(1)} async-done(((bf16[16,8,513]{2,1,0:T(8,128)(2,1)}), bf16[16,8,513]{2,1,0:T(8,128)(2,1)S(1)}, u32[]{:S(2)}, u32[]{:S(2)}) %all-to-all-start.5) | async-done | bytes 131360 | tf_op jit(solution)/shard_map/all_to_all | solution.py:12
  298.3 8.0 %all-to-all-start.6 = ((bf16[16,8,128]{2,1,0:T(8,128)(2,1)}), bf16[16,8,128]{2,1,0:T(8,128)(2,1)S(1)}, u32[]{:S(2)}, u32[]{:S(2)}) async-start(bf16[16,8,128]{2,1,0:T(8,128)(2,1)} %broadcast_in_dim.27), calls=%async_computation.6 | async-start | bytes 65536 | tf_op jit(solution)/shard_map/all_to_all | solution.py:12
  307.3 10.3 %all-to-all-done.6 = bf16[16,8,128]{2,1,0:T(8,128)(2,1)S(1)} async-done(((bf16[16,8,128]{2,1,0:T(8,128)(2,1)}), bf16[16,8,128]{2,1,0:T(8,128)(2,1)S(1)}, u32[]{:S(2)}, u32[]{:S(2)}) %all-to-all-start.6) | async-done | bytes 32800 | tf_op jit(solution)/shard_map/all_to_all | solution.py:12
  322.5 11.1 %all-to-all-done.21 = bf16[16,8,689]{2,1,0:T(8,128)(2,1)S(1)} async-done(((bf16[16,8,689]{2,1,0:T(8,128)(2,1)}), bf16[16,8,689]{2,1,0:T(8,128)(2,1)S(1)}, u32[]{:S(2)}, u32[]{:S(2)}) %all-to-all-start.21) | async-done | bytes 176416 | tf_op jit(solution)/shard_map/all_to_all | solution.py:12
  333.6 8.6 %all-to-all-start.7 = ((bf16[16,8,256]{2,1,0:T(8,128)(2,1)}), bf16[16,8,256]{2,1,0:T(8,128)(2,1)S(1)}, u32[]{:S(2)}, u32[]{:S(2)}) async-start(bf16[16,8,256]{2,1,0:T(8,128)(2,1)} %fusion), calls=%async_computation.7 | async-start | bytes 131072 | tf_op jit(solution)/shard_map/all_to_all | solution.py:12
  342.4 7.7 %all-to-all-done.7 = bf16[16,8,256]{2,1,0:T(8,128)(2,1)S(1)} async-done(((bf16[16,8,256]{2,1,0:T(8,128)(2,1)}), bf16[16,8,256]{2,1,0:T(8,128)(2,1)S(1)}, u32[]{:S(2)}, u32[]{:S(2)}) %all-to-all-start.7) | async-done | bytes 65568 | tf_op jit(solution)/shard_map/all_to_all | solution.py:12
  354.5 7.8 %all-to-all-done.8 = bf16[16,8,256]{2,1,0:T(8,128)(2,1)S(1)} async-done(((bf16[16,8,256]{2,1,0:T(8,128)(2,1)}), bf16[16,8,256]{2,1,0:T(8,128)(2,1)S(1)}, u32[]{:S(2)}, u32[]{:S(2)}) %all-to-all-start.8) | async-done | bytes 65568 | tf_op jit(solution)/shard_map/all_to_all | solution.py:12
  369.7 9.6 %all-to-all-done.22 = bf16[16,8,344]{2,1,0:T(8,128)(2,1)S(1)} async-done(((bf16[16,8,344]{2,1,0:T(8,128)(2,1)}), bf16[16,8,344]{2,1,0:T(8,128)(2,1)S(1)}, u32[]{:S(2)}, u32[]{:S(2)}) %all-to-all-start.22) | async-done | bytes 88096 | tf_op jit(solution)/shard_map/all_to_all | solution.py:12
  385.6 15.2 %all-to-all-done.9 = bf16[16,8,1377]{2,1,0:T(8,128)(2,1)S(1)} async-done(((bf16[16,8,1377]{2,1,0:T(8,128)(2,1)}), bf16[16,8,1377]{2,1,0:T(8,128)(2,1)S(1)}, u32[]{:S(2)}, u32[]{:S(2)}) %all-to-all-start.9) | async-done | bytes 352544 | tf_op jit(solution)/shard_map/all_to_all | solution.py:12
  400.7 9.9 %all-to-all-start.23 = ((bf16[16,4,256]{2,1,0:T(4,128)(2,1)}), bf16[16,4,256]{2,1,0:T(4,128)(2,1)S(1)}, u32[]{:S(2)}, u32[]{:S(2)}) async-start(bf16[16,4,256]{2,1,0:T(4,128)(2,1)} %reshape.675), calls=%async_computation.23 | async-start | bytes 65536 | tf_op jit(solution)/shard_map/all_to_all | solution.py:12
  425.7 12.1 %all-to-all-done.10 = bf16[16,8,688]{2,1,0:T(8,128)(2,1)S(1)} async-done(((bf16[16,8,688]{2,1,0:T(8,128)(2,1)}), bf16[16,8,688]{2,1,0:T(8,128)(2,1)S(1)}, u32[]{:S(2)}, u32[]{:S(2)}) %all-to-all-start.10) | async-done | bytes 176160 | tf_op jit(solution)/shard_map/all_to_all | solution.py:12
  (194 shorter events, 160.4 us)
Async XLA Ops:
  0.6 139.4 %copy-start = (bf16[256,128]{1,0:T(8,128)(2,1)S(1)}, bf16[256,128]{1,0:T(8,128)(2,1)}, u32[]{:S(2)}) copy-start(bf16[256,128]{1,0:T(8,128)(2,1)} %param.26) | copy-start | bytes 196612
  0.7 54.0 %copy-start.2 = (bf16[256,688]{0,1:T(8,128)(2,1)S(1)}, bf16[256,688]{0,1:T(8,128)(2,1)}, u32[]{:S(2)}) copy-start(bf16[256,688]{0,1:T(8,128)(2,1)} %param.23) | copy-start | bytes 1056772
  76.7 20.6 %all-to-all-start.14 = ((bf16[16,8,344]{2,1,0:T(8,128)(2,1)}), bf16[16,8,344]{2,1,0:T(8,128)(2,1)S(1)}, u32[]{:S(2)}, u32[]{:S(2)}) async-start(bf16[16,8,344]{2,1,0:T(8,128)(2,1)} %broadcast_in_dim.31), calls=%async_computation.14 | async-start | bytes 196608 | tf_op jit(solution)/shard_map/all_to_all | solution.py:12
  98.3 13.8 %all-to-all-start.15 = ((bf16[16,4,256]{2,1,0:T(4,128)(2,1)}), bf16[16,4,256]{2,1,0:T(4,128)(2,1)S(1)}, u32[]{:S(2)}, u32[]{:S(2)}) async-start(bf16[16,4,256]{2,1,0:T(4,128)(2,1)} %reshape.666), calls=%async_computation.15 | async-start | bytes 65536 | tf_op jit(solution)/shard_map/all_to_all | solution.py:12
  112.7 11.6 %all-to-all-start = ((bf16[16,8,256]{2,1,0:T(8,128)(2,1)}), bf16[16,8,256]{2,1,0:T(8,128)(2,1)S(1)}, u32[]{:S(2)}, u32[]{:S(2)}) async-start(bf16[16,8,256]{2,1,0:T(8,128)(2,1)} %broadcast_in_dim.24), calls=%async_computation | async-start | bytes 131072 | tf_op jit(solution)/shard_map/all_to_all | solution.py:12
  125.0 11.4 %all-to-all-start.16 = ((bf16[16,4,256]{2,1,0:T(4,128)(2,1)}), bf16[16,4,256]{2,1,0:T(4,128)(2,1)S(1)}, u32[]{:S(2)}, u32[]{:S(2)}) async-start(bf16[16,4,256]{2,1,0:T(4,128)(2,1)} %broadcast_in_dim.32), calls=%async_computation.16 | async-start | bytes 65536 | tf_op jit(solution)/shard_map/all_to_all | solution.py:12
  143.2 15.3 %all-to-all-start.17 = ((bf16[16,4,513]{2,1,0:T(4,128)(2,1)}), bf16[16,4,513]{2,1,0:T(4,128)(2,1)S(1)}, u32[]{:S(2)}, u32[]{:S(2)}) async-start(bf16[16,4,513]{2,1,0:T(4,128)(2,1)} %constant_dynamic-update-slice_fusion.1), calls=%async_computation.17 | async-start | bytes 163840 | tf_op jit(solution)/shard_map/all_to_all | solution.py:12
  158.5 20.5 %all-to-all-start.1 = ((bf16[16,8,1377]{2,1,0:T(8,128)(2,1)}), bf16[16,8,1377]{2,1,0:T(8,128)(2,1)S(1)}, u32[]{:S(2)}, u32[]{:S(2)}) async-start(bf16[16,8,1377]{2,1,0:T(8,128)(2,1)} %concatenate.146), calls=%async_computation.1 | async-start | bytes 720896 | tf_op jit(solution)/shard_map/all_to_all | solution.py:12
  179.6 23.7 %all-to-all-start.18 = ((bf16[16,4,128]{2,1,0:T(4,128)(2,1)}), bf16[16,4,128]{2,1,0:T(4,128)(2,1)S(1)}, u32[]{:S(2)}, u32[]{:S(2)}) async-start(bf16[16,4,128]{2,1,0:T(4,128)(2,1)} %broadcast_in_dim.33), calls=%async_computation.18 | async-start | bytes 32768 | tf_op jit(solution)/shard_map/all_to_all | solution.py:12
  204.0 13.2 %all-to-all-start.19 = ((bf16[16,4,256]{2,1,0:T(4,128)(2,1)}), bf16[16,4,256]{2,1,0:T(4,128)(2,1)S(1)}, u32[]{:S(2)}, u32[]{:S(2)}) async-start(bf16[16,4,256]{2,1,0:T(4,128)(2,1)} %reshape.672), calls=%async_computation.19 | async-start | bytes 65536 | tf_op jit(solution)/shard_map/all_to_all | solution.py:12
  217.9 16.9 %all-to-all-start.2 = ((bf16[16,8,688]{2,1,0:T(8,128)(2,1)}), bf16[16,8,688]{2,1,0:T(8,128)(2,1)S(1)}, u32[]{:S(2)}, u32[]{:S(2)}) async-start(bf16[16,8,688]{2,1,0:T(8,128)(2,1)} %broadcast_in_dim.25), calls=%async_computation.2 | async-start | bytes 393216 | tf_op jit(solution)/shard_map/all_to_all | solution.py:12
  235.6 14.5 %all-to-all-start.3 = ((bf16[16,8,256]{2,1,0:T(8,128)(2,1)}), bf16[16,8,256]{2,1,0:T(8,128)(2,1)S(1)}, u32[]{:S(2)}, u32[]{:S(2)}) async-start(bf16[16,8,256]{2,1,0:T(8,128)(2,1)} %fusion.1), calls=%async_computation.3 | async-start | bytes 131072 | tf_op jit(solution)/shard_map/all_to_all | solution.py:12
  250.7 11.3 %all-to-all-start.20 = ((bf16[16,4,256]{2,1,0:T(4,128)(2,1)}), bf16[16,4,256]{2,1,0:T(4,128)(2,1)S(1)}, u32[]{:S(2)}, u32[]{:S(2)}) async-start(bf16[16,4,256]{2,1,0:T(4,128)(2,1)} %broadcast_in_dim.34), calls=%async_computation.20 | async-start | bytes 65536 | tf_op jit(solution)/shard_map/all_to_all | solution.py:12
  262.6 11.6 %all-to-all-start.4 = ((bf16[16,8,256]{2,1,0:T(8,128)(2,1)}), bf16[16,8,256]{2,1,0:T(8,128)(2,1)S(1)}, u32[]{:S(2)}, u32[]{:S(2)}) async-start(bf16[16,8,256]{2,1,0:T(8,128)(2,1)} %broadcast_in_dim.26), calls=%async_computation.4 | async-start | bytes 131072 | tf_op jit(solution)/shard_map/all_to_all | solution.py:12
  278.3 17.9 %all-to-all-start.5 = ((bf16[16,8,513]{2,1,0:T(8,128)(2,1)}), bf16[16,8,513]{2,1,0:T(8,128)(2,1)S(1)}, u32[]{:S(2)}, u32[]{:S(2)}) async-start(bf16[16,8,513]{2,1,0:T(8,128)(2,1)} %constant_dynamic-update-slice_fusion), calls=%async_computation.5 | async-start | bytes 327680 | tf_op jit(solution)/shard_map/all_to_all | solution.py:12
  298.3 19.2 %all-to-all-start.6 = ((bf16[16,8,128]{2,1,0:T(8,128)(2,1)}), bf16[16,8,128]{2,1,0:T(8,128)(2,1)S(1)}, u32[]{:S(2)}, u32[]{:S(2)}) async-start(bf16[16,8,128]{2,1,0:T(8,128)(2,1)} %broadcast_in_dim.27), calls=%async_computation.6 | async-start | bytes 65536 | tf_op jit(solution)/shard_map/all_to_all | solution.py:12
  317.6 16.0 %all-to-all-start.21 = ((bf16[16,8,689]{2,1,0:T(8,128)(2,1)}), bf16[16,8,689]{2,1,0:T(8,128)(2,1)S(1)}, u32[]{:S(2)}, u32[]{:S(2)}) async-start(bf16[16,8,689]{2,1,0:T(8,128)(2,1)} %bitcast.62), calls=%async_computation.21 | async-start | bytes 393216 | tf_op jit(solution)/shard_map/all_to_all | solution.py:12
  333.6 16.5 %all-to-all-start.7 = ((bf16[16,8,256]{2,1,0:T(8,128)(2,1)}), bf16[16,8,256]{2,1,0:T(8,128)(2,1)S(1)}, u32[]{:S(2)}, u32[]{:S(2)}) async-start(bf16[16,8,256]{2,1,0:T(8,128)(2,1)} %fusion), calls=%async_computation.7 | async-start | bytes 131072 | tf_op jit(solution)/shard_map/all_to_all | solution.py:12
  350.8 11.6 %all-to-all-start.8 = ((bf16[16,8,256]{2,1,0:T(8,128)(2,1)}), bf16[16,8,256]{2,1,0:T(8,128)(2,1)S(1)}, u32[]{:S(2)}, u32[]{:S(2)}) async-start(bf16[16,8,256]{2,1,0:T(8,128)(2,1)} %broadcast_in_dim.28), calls=%async_computation.8 | async-start | bytes 131072 | tf_op jit(solution)/shard_map/all_to_all | solution.py:12
  363.0 16.4 %all-to-all-start.22 = ((bf16[16,8,344]{2,1,0:T(8,128)(2,1)}), bf16[16,8,344]{2,1,0:T(8,128)(2,1)S(1)}, u32[]{:S(2)}, u32[]{:S(2)}) async-start(bf16[16,8,344]{2,1,0:T(8,128)(2,1)} %broadcast_in_dim.35), calls=%async_computation.22 | async-start | bytes 196608 | tf_op jit(solution)/shard_map/all_to_all | solution.py:12
  379.3 21.4 %all-to-all-start.9 = ((bf16[16,8,1377]{2,1,0:T(8,128)(2,1)}), bf16[16,8,1377]{2,1,0:T(8,128)(2,1)S(1)}, u32[]{:S(2)}, u32[]{:S(2)}) async-start(bf16[16,8,1377]{2,1,0:T(8,128)(2,1)} %concatenate.156), calls=%async_computation.9 | async-start | bytes 720896 | tf_op jit(solution)/shard_map/all_to_all | solution.py:12
  400.7 17.5 %all-to-all-start.23 = ((bf16[16,4,256]{2,1,0:T(4,128)(2,1)}), bf16[16,4,256]{2,1,0:T(4,128)(2,1)S(1)}, u32[]{:S(2)}, u32[]{:S(2)}) async-start(bf16[16,4,256]{2,1,0:T(4,128)(2,1)} %reshape.675), calls=%async_computation.23 | async-start | bytes 65536 | tf_op jit(solution)/shard_map/all_to_all | solution.py:12
  418.9 18.8 %all-to-all-start.10 = ((bf16[16,8,688]{2,1,0:T(8,128)(2,1)}), bf16[16,8,688]{2,1,0:T(8,128)(2,1)S(1)}, u32[]{:S(2)}, u32[]{:S(2)}) async-start(bf16[16,8,688]{2,1,0:T(8,128)(2,1)} %broadcast_in_dim.29), calls=%async_computation.10 | async-start | bytes 393216 | tf_op jit(solution)/shard_map/all_to_all | solution.py:12
  438.6 15.2 %all-to-all-start.11 = ((bf16[16,8,256]{2,1,0:T(8,128)(2,1)}), bf16[16,8,256]{2,1,0:T(8,128)(2,1)S(1)}, u32[]{:S(2)}, u32[]{:S(2)}) async-start(bf16[16,8,256]{2,1,0:T(8,128)(2,1)} %fusion.2), calls=%async_computation.11 | async-start | bytes 131072 | tf_op jit(solution)/shard_map/all_to_all | solution.py:12
  (18 other events, 103.0 us)

commit v2 on v1

--- a/solution.py
+++ b/solution.py
@@ -5,7 +5,7 @@
 
 EPS_NORM = 1e-06
 EPS_GROUP = 1e-05
-CHAINS = ((0, 8), (8, 4))
+CHAINS = ((0, 12),)
 
 
 def exchange(x, axis):

time: 456 us -> 303 us (0.66)
  waiting for transfers between devices: 210 us -> 38.8 us
  blocking collectives: 71.6 us -> 225 us
  starting transfers between devices: 131 us -> 20.1 us
  local copies, waits for them, and re-layouts: 22.3 us -> 6.69 us
  matrix products: 11.1 us -> 4.22 us
    all_to_all x22 -> x3, waiting for transfers between devices: 210 us -> 38.8 us  [exchange(): return lax.all_to_all(x, axis, split_axis=0, concat_axis=0, tiled=True)]
    all_to_all x2 -> x9, blocking collectives: 71.6 us -> 225 us  [exchange(): return lax.all_to_all(x, axis, split_axis=0, concat_axis=0, tiled=True)]
    all_to_all x22 -> x3, starting transfers between devices: 131 us -> 20.1 us  [exchange(): return lax.all_to_all(x, axis, split_axis=0, concat_axis=0, tiled=True)]
    dot_general x28 -> x17, matrix products: 10.3 us -> 3.43 us  [dot(): return jnp.dot(a, b, preferred_element_type=jnp.float32)]
    broadcast_in_dim x12 -> x6, local copies, waits for them, and re-layouts: 7.07 us -> 1.56 us  [spread(): jnp.broadcast_to(x[None], (lax.axis_size(axis), *x.shape))]
    unnamed x41 -> x38, local copies, waits for them, and re-layouts: 7.95 us -> 3.09 us
  transfers between devices with their start and end apart: 22 -> 3, of which waited for: 22 -> 3; matrix products, arithmetic and copies ran while one was open for 2% -> 0% of each run, Pallas kernels for 0% -> 0%
where the time goes in v2:
time: 303 us; the launch traced here: 302 us
  blocking collectives  225 us (74%)
  waiting for transfers between devices  38.8 us (13%)
  starting transfers between devices  20.1 us (7%)
  local copies, waits for them, and re-layouts  6.69 us (2%)
  other arithmetic  5.37 us (2%)
  matrix products  4.22 us (1%)
    all_to_all x9, blocking collectives, exchange(): return lax.all_to_all(x, axis, split_axis=0, concat_axis=0, tiled=True)  225 us
    all_to_all x3, waiting for transfers between devices, exchange(): return lax.all_to_all(x, axis, split_axis=0, concat_axis=0, tiled=True)  38.8 us
    all_to_all x3, starting transfers between devices, exchange(): return lax.all_to_all(x, axis, split_axis=0, concat_axis=0, tiled=True)  20.1 us
  transfers between devices with their start and end apart: 3, of which 3 were waited for; matrix products, arithmetic and copies ran while one was open for 0% of the time, Pallas kernels for 0%

profile of v2, /device:TPU:65, one launch (start us, length us, event | category | flops | bytes accessed | tf_op | source)
XLA Modules:
  0.0 302.0 jit_solution(1914079426905999210)
XLA Ops:
  0.7 0.8 broadcast_in_dim.12
  1.4 53.1 %all_to_all.60 = bf16[16,12,256]{2,1,0:T(8,128)(2,1)S(1)} all-to-all(bf16[16,12,256]{2,1,0:T(8,128)(2,1)S(1)} %broadcast_in_dim.12), channel_id=1, replica_groups=mesh['grp'=2,'kv'=16,'tp'=16] {'tp'}, dimensions={0} | all-to-all | bytes 196608 | tf_op jit(solution)/shard_map/all_to_all | solution.py:12
  54.5 0.7 multiply_convert_fusion.2
  56.7 41.5 %all_to_all.61 = bf16[16,24,689]{2,1,0:T(8,128)(2,1)S(1)} all-to-all(bf16[16,24,689]{2,1,0:T(8,128)(2,1)S(1)} %bitcast.79), channel_id=1, replica_groups=mesh['grp'=2,'kv'=16,'tp'=16] {'kv'}, dimensions={0} | all-to-all | bytes 1058304 | tf_op jit(solution)/shard_map/all_to_all | solution.py:12
  98.7 18.0 %all_to_all.62 = bf16[16,24,344]{2,1,0:T(8,128)(2,1)S(1)} all-to-all(bf16[16,24,344]{2,1,0:T(8,128)(2,1)S(1)} %broadcast_in_dim.13), channel_id=1, replica_groups=mesh['grp'=2,'kv'=16,'tp'=16] {'kv'}, dimensions={0} | all-to-all | bytes 528384 | tf_op jit(solution)/shard_map/all_to_all | solution.py:12
  117.2 18.0 %all_to_all.63 = bf16[16,12,256]{2,1,0:T(8,128)(2,1)S(1)} all-to-all(bf16[16,12,256]{2,1,0:T(8,128)(2,1)S(1)} %reshape.355), channel_id=1, replica_groups=mesh['grp'=2,'kv'=16,'tp'=16] {'tp'}, dimensions={0} | all-to-all | bytes 196608 | tf_op jit(solution)/shard_map/all_to_all | solution.py:12
  135.3 11.3 %all_to_all.64 = bf16[16,12,256]{2,1,0:T(8,128)(2,1)S(1)} all-to-all(bf16[16,12,256]{2,1,0:T(8,128)(2,1)S(1)} %broadcast_in_dim.14), channel_id=1, replica_groups=mesh['grp'=2,'kv'=16,'tp'=16] {'tp'}, dimensions={0} | all-to-all | bytes 196608 | tf_op jit(solution)/shard_map/all_to_all | solution.py:12
  147.8 0.6 constant_dynamic-update-slice_fusion.4
  148.5 0.6 constant_dynamic-update-slice_fusion.3
  149.1 0.6 constant_dynamic-update-slice_fusion.2
  151.0 6.1 %all-to-all-start.5 = ((bf16[16,12,513]{2,1,0:T(8,128)(2,1)}), bf16[16,12,513]{2,1,0:T(8,128)(2,1)S(1)}, u32[]{:S(2)}, u32[]{:S(2)}) async-start(bf16[16,12,513]{2,1,0:T(8,128)(2,1)} %constant_dynamic-update-slice_fusion), calls=%async_computation.5 | async-start | bytes 655360 | tf_op jit(solution)/shard_map/all_to_all | solution.py:12
  157.3 16.8 %all-to-all-done.5 = bf16[16,12,513]{2,1,0:T(8,128)(2,1)S(1)} async-done(((bf16[16,12,513]{2,1,0:T(8,128)(2,1)}), bf16[16,12,513]{2,1,0:T(8,128)(2,1)S(1)}, u32[]{:S(2)}, u32[]{:S(2)}) %all-to-all-start.5) | async-done | bytes 197024 | tf_op jit(solution)/shard_map/all_to_all | solution.py:12
  174.5 0.8 fusion.2
  176.1 21.4 %all_to_all.65 = bf16[16,12,128]{2,1,0:T(8,128)(2,1)S(1)} all-to-all(bf16[16,12,128]{2,1,0:T(8,128)(2,1)S(1)} %broadcast_in_dim.15), channel_id=1, replica_groups=mesh['grp'=2,'kv'=16,'tp'=16] {'kv'}, dimensions={0} | all-to-all | bytes 98304 | tf_op jit(solution)/shard_map/all_to_all | solution.py:12
  197.7 14.1 %all_to_all.66 = bf16[16,12,256]{2,1,0:T(8,128)(2,1)S(1)} all-to-all(bf16[16,12,256]{2,1,0:T(8,128)(2,1)S(1)} %reshape.361), channel_id=1, replica_groups=mesh['grp'=2,'kv'=16,'tp'=16] {'tp'}, dimensions={0} | all-to-all | bytes 196608 | tf_op jit(solution)/shard_map/all_to_all | solution.py:12
  211.9 11.3 %all_to_all.67 = bf16[16,12,256]{2,1,0:T(8,128)(2,1)S(1)} all-to-all(bf16[16,12,256]{2,1,0:T(8,128)(2,1)S(1)} %broadcast_in_dim.16), channel_id=1, replica_groups=mesh['grp'=2,'kv'=16,'tp'=16] {'tp'}, dimensions={0} | all-to-all | bytes 196608 | tf_op jit(solution)/shard_map/all_to_all | solution.py:12
  225.1 36.7 %all_to_all.68 = bf16[16,24,689]{2,1,0:T(8,128)(2,1)S(1)} all-to-all(bf16[16,24,689]{2,1,0:T(8,128)(2,1)S(1)} %bitcast.80), channel_id=1, replica_groups=mesh['grp'=2,'kv'=16,'tp'=16] {'kv'}, dimensions={0} | all-to-all | bytes 1058304 | tf_op jit(solution)/shard_map/all_to_all | solution.py:12
  262.2 0.7 broadcast_in_dim.17
  263.0 4.5 %all-to-all-start.10 = ((bf16[16,24,344]{2,1,0:T(8,128)(2,1)}), bf16[16,24,344]{2,1,0:T(8,128)(2,1)S(1)}, u32[]{:S(2)}, u32[]{:S(2)}) async-start(bf16[16,24,344]{2,1,0:T(8,128)(2,1)} %broadcast_in_dim.17), calls=%async_computation.10 | async-start | bytes 589824 | tf_op jit(solution)/shard_map/all_to_all | solution.py:12
  267.6 14.0 %all-to-all-done.10 = bf16[16,24,344]{2,1,0:T(8,128)(2,1)S(1)} async-done(((bf16[16,24,344]{2,1,0:T(8,128)(2,1)}), bf16[16,24,344]{2,1,0:T(8,128)(2,1)S(1)}, u32[]{:S(2)}, u32[]{:S(2)}) %all-to-all-start.10) | async-done | bytes 264224 | tf_op jit(solution)/shard_map/all_to_all | solution.py:12
  282.0 0.7 reshape.364
  282.7 9.4 %all-to-all-start.11 = ((bf16[16,12,256]{2,1,0:T(8,128)(2,1)}), bf16[16,12,256]{2,1,0:T(8,128)(2,1)S(1)}, u32[]{:S(2)}, u32[]{:S(2)}) async-start(bf16[16,12,256]{2,1,0:T(8,128)(2,1)} %reshape.364), calls=%async_computation.11 | async-start | bytes 262144 | tf_op jit(solution)/shard_map/all_to_all | solution.py:12
  292.1 1.2 multiply_add_fusion
  293.3 8.1 %all-to-all-done.11 = bf16[16,12,256]{2,1,0:T(8,128)(2,1)S(1)} async-done(((bf16[16,12,256]{2,1,0:T(8,128)(2,1)}), bf16[16,12,256]{2,1,0:T(8,128)(2,1)S(1)}, u32[]{:S(2)}, u32[]{:S(2)}) %all-to-all-start.11) | async-done | bytes 98336 | tf_op jit(solution)/shard_map/all_to_all | solution.py:12
  (108 shorter events, 9.5 us)
Async XLA Ops:
  0.6 196.9 %copy-start = (bf16[128,256]{1,0:T(8,128)(2,1)S(1)}, bf16[128,256]{1,0:T(8,128)(2,1)}, u32[]{:S(2)}) copy-start(bf16[128,256]{1,0:T(8,128)(2,1)} %param.30) | copy-start | bytes 196612
  0.6 54.7 %copy-start.2 = (bf16[256,688]{0,1:T(8,128)(2,1)S(1)}, bf16[256,688]{0,1:T(8,128)(2,1)}, u32[]{:S(2)}) copy-start(bf16[256,688]{0,1:T(8,128)(2,1)} %param.23) | copy-start | bytes 1056772
  54.5 1.3 copy-start.3
  98.5 18.2 %copy-start.6 = (bf16[688,256]{1,0:T(8,128)(2,1)S(1)}, bf16[688,256]{1,0:T(8,128)(2,1)}, u32[]{:S(2)}) copy-start(bf16[688,256]{1,0:T(8,128)(2,1)} %param.24) | copy-start | bytes 1056772
  116.7 18.5 %copy-start.12 = (bf16[12,256]{1,0:T(8,128)(2,1)S(1)}, bf16[12,256]{1,0:T(8,128)(2,1)}, u32[]{:S(2)}) copy-start(bf16[12,256]{1,0:T(8,128)(2,1)} %param.18) | copy-start | bytes 18436
  117.2 29.8 %copy-start.13 = (f32[256]{0:T(256)S(1)}, f32[256]{0:T(256)}, u32[]{:S(2)}) copy-start(f32[256]{0:T(256)} %param.25) | copy-start | bytes 3076
  117.2 29.8 %copy-start.8 = (bf16[256,128]{1,0:T(8,128)(2,1)S(1)}, bf16[256,128]{1,0:T(8,128)(2,1)}, u32[]{:S(2)}) copy-start(bf16[256,128]{1,0:T(8,128)(2,1)} %param.29) | copy-start | bytes 196612
  135.3 12.0 %copy-start.9 = (bf16[256,128]{1,0:T(8,128)(2,1)S(1)}, bf16[256,128]{1,0:T(8,128)(2,1)}, u32[]{:S(2)}) copy-start(bf16[256,128]{1,0:T(8,128)(2,1)} %param.28) | copy-start | bytes 196612
  146.6 0.8 copy-start.10
  146.7 0.9 copy-start.11
  147.8 9.5 %copy-start.16 = (s32[12]{0:T(128)S(1)}, s32[12]{0:T(128)}, u32[]{:S(2)}) copy-start(s32[12]{0:T(128)} %param.19) | copy-start | bytes 148
  149.1 25.4 %copy-start.1 = (f32[12,1,128,128]{3,2,1,0:T(8,128)S(1)}, f32[12,1,128,128]{3,2,1,0:T(8,128)}, u32[]{:S(2)}) copy-start(f32[12,1,128,128]{3,2,1,0:T(8,128)} %param.20) | copy-start | bytes 2359300
  151.0 23.0 %all-to-all-start.5 = ((bf16[16,12,513]{2,1,0:T(8,128)(2,1)}), bf16[16,12,513]{2,1,0:T(8,128)(2,1)S(1)}, u32[]{:S(2)}, u32[]{:S(2)}) async-start(bf16[16,12,513]{2,1,0:T(8,128)(2,1)} %constant_dynamic-update-slice_fusion), calls=%async_computation.5 | async-start | bytes 655360 | tf_op jit(solution)/shard_map/all_to_all | solution.py:12
  157.1 18.8 %copy-start.15 = (f32[128]{0:T(128)S(1)}, f32[128]{0:T(128)}, u32[]{:S(2)}) copy-start(f32[128]{0:T(128)} %param.31) | copy-start | bytes 1540
  197.5 25.7 %copy-start.14 = (f32[256]{0:T(256)S(1)}, f32[256]{0:T(256)}, u32[]{:S(2)}) copy-start(f32[256]{0:T(256)} %param.32) | copy-start | bytes 3076
  197.7 25.5 %copy-start.4 = (bf16[256,688]{0,1:T(8,128)(2,1)S(1)}, bf16[256,688]{0,1:T(8,128)(2,1)}, u32[]{:S(2)}) copy-start(bf16[256,688]{0,1:T(8,128)(2,1)} %param.34) | copy-start | bytes 1056772
  223.2 1.0 copy-start.5
  262.2 19.4 %copy-start.7 = (bf16[688,256]{1,0:T(8,128)(2,1)S(1)}, bf16[688,256]{1,0:T(8,128)(2,1)}, u32[]{:S(2)}) copy-start(bf16[688,256]{1,0:T(8,128)(2,1)} %param.35) | copy-start | bytes 1056772
  263.0 18.6 %all-to-all-start.10 = ((bf16[16,24,344]{2,1,0:T(8,128)(2,1)}), bf16[16,24,344]{2,1,0:T(8,128)(2,1)S(1)}, u32[]{:S(2)}, u32[]{:S(2)}) async-start(bf16[16,24,344]{2,1,0:T(8,128)(2,1)} %broadcast_in_dim.17), calls=%async_computation.10 | async-start | bytes 589824 | tf_op jit(solution)/shard_map/all_to_all | solution.py:12
  282.7 18.7 %all-to-all-start.11 = ((bf16[16,12,256]{2,1,0:T(8,128)(2,1)}), bf16[16,12,256]{2,1,0:T(8,128)(2,1)S(1)}, u32[]{:S(2)}, u32[]{:S(2)}) async-start(bf16[16,12,256]{2,1,0:T(8,128)(2,1)} %reshape.364), calls=%async_computation.11 | async-start | bytes 262144 | tf_op jit(solution)/shard_map/all_to_all | solution.py:12

commit v3 on v2

v3 whole, which is shorter than its diff:
```python
import functools

import jax
import jax.numpy as jnp
import numpy as np
from jax import lax
from jax.experimental import pallas as pl
from jax.experimental.pallas import tpu as pltpu
from jax.sharding import Mesh
from jax.sharding import PartitionSpec as P

EPS_NORM = 1e-06
EPS_GROUP = 1e-05
KV = ("kvh", "kvp")
BOTH = ("kvp", "tp")
VMEM = pl.BlockSpec(memory_space=pltpu.VMEM)
NT = (((1,), (1,)), ((), ()))


def local_call(kernel, out_shape, *args, scratch=(), flops=0):
    return pl.pallas_call(
        kernel,
        out_shape=out_shape,
        in_specs=[VMEM] * len(args),
        out_specs=jax.tree.map(lambda _: VMEM, out_shape),
        scratch_shapes=scratch,
        cost_estimate=pl.CostEstimate(flops=flops, bytes_accessed=2**20, transcendentals=0),
        compiler_params=pltpu.CompilerParams(vmem_limit_bytes=16 * 2**20),
    )(*args)


def exchange(x, axis):
    return lax.all_to_all(x, axis, split_axis=0, concat_axis=0, tiled=True)


def spread(x, axis):
    return exchange(jnp.broadcast_to(x[None], (lax.axis_size(axis), *x.shape)), axis)


def mine(x, index):
    return lax.dynamic_index_in_dim(x, index, 0, keepdims=False)


def fill_rows(x, y_ref, p):
    if len(y_ref.shape) == 3:
        x[0] = y_ref[p]
        x[1] = y_ref[1 - p]
        return
    _, chunks, tall, wide = y_ref.shape
    across = x.shape[2] // wide
    for n in range(chunks):
        r, c = divmod(n, across)
        place = (slice(r * tall, (r + 1) * tall), slice(c * wide, (c + 1) * wide))
        x[(0, *place)] = y_ref[p, n]
        x[(1, *place)] = y_ref[1 - p, n]


def up_kernel(y_ref, own_ref, got_ref, out_ref, x):
    fill_rows(x, y_ref, lax.axis_index("kvp"))
    groups, tall, lanes = out_ref.shape
    part = own_ref.shape[1]
    half = lanes // 2
    squares = sum(jnp.sum(jnp.square(x[j].astype(jnp.float32)), axis=1, keepdims=True) for j in range(2))
    for i in range(2):
        value = sum(
            lax.dot_general(x[j], w[i], NT, preferred_element_type=jnp.float32)
            for j, w in enumerate((own_ref, got_ref))
        )
        rows = jnp.concatenate([value, jnp.broadcast_to(squares, (value.shape[0], half - part))], axis=1)
        rows = rows.astype(jnp.bfloat16)
        for r in range(groups):
            out_ref[r, :, i * half : (i + 1) * half] = rows[r * tall : (r + 1) * tall]


def down_kernel(h_ref, w_ref, out_ref, h):
    groups, tall, part = h_ref.shape
    cuts = w_ref.shape[0] // part
    value = 0.0
    for c in range(cuts):
        for r in range(groups // cuts):
            h[r * tall : (r + 1) * tall] = h_ref[r * cuts + c]
        value += jnp.dot(h[...], w_ref[c * part : (c + 1) * part], preferred_element_type=jnp.float32)
    value = value.astype(jnp.bfloat16)
    if len(out_ref.shape) == 2:
        out_ref[...] = value
        return
    chunks, high, wide = out_ref.shape
    across = value.shape[1] // wide
    for n in range(chunks):
        r, c = divmod(n, across)
        out_ref[n] = value[r * high : (r + 1) * high, c * wide : (c + 1) * wide]


def heads_kernel(y_ref, w_ref, out_ref, x, scr):
    chunks, tall, wide = y_ref.shape
    across = x.shape[1] // wide
    for n in range(chunks):
        r, c = divmod(n, across)
        x[r * tall : (r + 1) * tall, c * wide : (c + 1) * wide] = y_ref[n]
    members, high, lanes = out_ref.shape
    rows = x.shape[0]
    each = rows // members
    squares = jnp.sum(jnp.square(x[...].astype(jnp.float32)), axis=1, keepdims=True)
    scr[:rows, :lanes] = jnp.dot(x[...], w_ref[...], preferred_element_type=jnp.float32)
    scr[:rows, lanes:] = jnp.broadcast_to(squares, (rows, 128))
    row = lax.broadcasted_iota(jnp.int32, (high, 128), 0)
    lane = lax.broadcasted_iota(jnp.int32, (high, 128), 1)
    for k in range(members):
        piece = scr[k * each : k * each + high, :]
        line = jnp.sum(jnp.where((row == lane) & (row < each), piece[:, lanes:], 0.0), axis=0, keepdims=True)
        out_ref[k, :, :128] = jnp.where(row < each, piece[:, :128], line).astype(jnp.bfloat16)
        out_ref[k, :, 128:] = piece[:, 128:lanes].astype(jnp.bfloat16)


def paired_weights(norm_gain, w_gate, w_up):
    p = lax.axis_index("kvp")
    both = jnp.stack([w.T.reshape(2, -1, w.shape[0]) for w in (w_gate, w_up)], axis=1)
    both = (both.astype(jnp.float32) * norm_gain).astype(jnp.bfloat16)
    got = lax.ppermute(mine(both, 1 - p), "kvp", [(0, 1), (1, 0)])
    return mine(both, p), got


def feed_forward(gathered, weights, w_down, flat):
    own_w, got_w = weights
    members = lax.axis_size("kvh")
    wide, part = own_w.shape[2], own_w.shape[1]
    rows = gathered.size // (2 * wide)
    tall, half = rows // members, -(-(part + 1) // 128) * 128
    sent = local_call(
        up_kernel,
        jax.ShapeDtypeStruct((members, tall, 2 * half), jnp.bfloat16),
        gathered,
        own_w,
        got_w,
        scratch=(pltpu.VMEM((2, rows, wide), jnp.bfloat16),),
        flops=8 * rows * wide * part,
    )
    total = exchange(sent, "kvh").astype(jnp.float32).sum(axis=0)
    features = wide * lax.axis_size(KV)
    factor = lax.rsqrt(total[:, part : part + 1] / features + EPS_NORM)
    hidden = jax.nn.silu(factor * total[:, :part]) * (factor * total[:, half : half + part])
    everyone = spread(hidden.astype(jnp.bfloat16), KV)
    width = w_down.shape[1]
    shape = (rows, width) if flat else (lax.axis_size("tp"), tall, 2 * rows * width // (lax.axis_size("tp") * 2 * tall))
    return local_call(
        down_kernel,
        jax.ShapeDtypeStruct(shape, jnp.bfloat16),
        everyone,
        w_down,
        scratch=(pltpu.VMEM((rows, part), jnp.bfloat16),),
        flops=4 * rows * part * width,
    )


def advance(own, back, branch):
    share = exchange(back, "tp").astype(jnp.float32).sum(axis=0)
    return (own.astype(jnp.float32) + branch * share).astype(jnp.bfloat16)


def rotate(values_in, cosine, sine):
    half = values_in.shape[-1] // 2
    low, high = values_in[..., :half], values_in[..., half:]
    return jnp.concatenate([low * cosine - high * sine, low * sine + high * cosine], axis=-1)


def retention(gathered, w_heads, features, head_gain, state, tables):
    cosine, sine, decays = tables
    count, heads, width, _ = state.shape
    members = lax.axis_size(KV)
    chunks, tall, wide = gathered.shape
    block, lanes = w_heads.shape
    rows = members * count
    high = -(-(count + 1) // 8) * 8
    sent = local_call(
        heads_kernel,
        jax.ShapeDtypeStruct((members, high, lanes), jnp.bfloat16),
        gathered,
        w_heads,
        scratch=(
            pltpu.VMEM((rows, block), jnp.bfloat16),
            pltpu.VMEM((rows + 8, lanes + 128), jnp.float32),
        ),
        flops=2 * rows * block * lanes,
    )
    total = exchange(sent, KV).astype(jnp.float32).sum(axis=0)
    factor = lax.rsqrt(total[count, :count] / features + EPS_NORM)[:, None]
    total = factor * total[:count]
    q, k, v, o = (total[:, i * heads * width : (i + 1) * heads * width].reshape(count, heads, width) for i in range(4))
    q = rotate(q, cosine, sine)
    k = rotate(k, cosine, sine) * width ** (-0.5)
    carried = jnp.einsum("shd,shde->she", q, state, precision=lax.Precision.HIGHEST)
    within = jnp.sum(q * k, axis=-1, keepdims=True)
    mixture = decays[None, :, None] * carried + within * v
    centered = mixture - jnp.mean(mixture, axis=-1, keepdims=True)
    variance = jnp.mean(centered * centered, axis=-1, keepdims=True)
    normed = centered * lax.rsqrt(variance + EPS_GROUP) * head_gain.reshape(heads, width)
    ret_out = (jax.nn.silu(o) * normed).astype(jnp.bfloat16).reshape(count, heads * width)
    new_state = decays[None, :, None, None] * state + k[..., :, None] * v[..., None, :]
    return spread(ret_out, KV).reshape(rows, heads * width), new_state


def per_device(
    stream_in,
    positions,
    ret_state,
    first_gain,
    first_gate,
    first_up,
    first_down,
    mix_gain,
    w_query,
    w_key,
    w_value,
    w_outgate,
    w_out,
    head_gain,
    second_gain,
    second_gate,
    second_up,
    second_down,
):
    few, block = stream_in.shape
    tp, t, p = lax.axis_size("tp"), lax.axis_index("tp"), lax.axis_index("kvp")
    features = block * lax.axis_size(KV)
    rows = few * tp
    groups = lax.axis_size("kvh")
    tall, across = rows // groups, tp // groups
    wide = block // across

    half = ret_state.shape[-1] // 2
    inverse = 10000.0 ** (-jnp.arange(half, dtype=jnp.float32) / half)
    angles = positions.astype(jnp.float32)[:, None] * inverse[None, :]
    cosine, sine = jnp.cos(angles)[:, None, :], jnp.sin(angles)[:, None, :]
    heads = ret_state.shape[1]
    head_ids = (t * heads + jnp.arange(heads)).astype(jnp.float32)
    decays = jnp.exp(jnp.log1p(-(2.0 ** (-5.0 - head_ids))))

    first_pair = paired_weights(first_gain, first_gate, first_up)
    second_pair = paired_weights(second_gain, second_gate, second_up)
    w_heads = jnp.concatenate([w_query, w_key, w_value, w_outgate], axis=1)
    w_heads = (w_heads.astype(jnp.float32) * mix_gain[:, None]).astype(jnp.bfloat16)

    gathered = spread(stream_in, BOTH).reshape(2, rows, block)
    own = lax.dynamic_slice(gathered, (p, (t // across) * tall, (t % across) * wide), (1, tall, wide))[0]
    back = feed_forward(gathered, first_pair, first_down, False)
    own = advance(own, back, 0.5)
    gathered = spread(own, "tp")
    ret_out, new_state = retention(
        gathered, w_heads, features, head_gain, ret_state, (cosine, sine, decays)
    )
    back = jnp.dot(ret_out, w_out, preferred_element_type=jnp.float32).astype(jnp.bfloat16)
    back = back.reshape(groups, tall, across, wide).transpose(0, 2, 1, 3).reshape(tp, tall, wide)
    own = advance(own, back, 1.0)
    gathered = spread(own, BOTH).reshape(2, tp, tall, wide)
    place = (t * few) // tall
    own = lax.dynamic_slice(
        gathered, (p, place * across, t * few - place * tall, 0), (1, across, few, wide)
    )[0]
    own = jnp.concatenate([own[c] for c in range(across)], axis=1)
    back = feed_forward(gathered, second_pair, second_down, True)
    return advance(own, back.reshape(tp, few, block), 0.5), new_state


def solution(mesh):
    sizes = dict(mesh.shape)
    shape = (sizes["grp"], sizes["kv"] // 2, 2, sizes["tp"])
    fine = Mesh(np.asarray(mesh.devices).reshape(shape), ("grp", *KV, "tp"))
    rows, tall, flat = P(("grp", "tp"), KV), P(KV, "tp"), P("tp", KV)
    in_specs = (
        rows,
        P(("grp", *KV)),
        P(("grp", *KV), "tp", None, None),
        P(KV),
        tall,
        tall,
        flat,
        P(KV),
        tall,
        tall,
        tall,
        tall,
        flat,
        P("tp"),
        P(KV),
        tall,
        tall,
        flat,
    )
    out_specs = (rows, P(("grp", *KV), "tp", None, None))
    return jax.shard_map(
        per_device, mesh=fine, in_specs=in_specs, out_specs=out_specs, check_vma=False
    )
```

time: 303 us -> 285 us (0.941)
  blocking collectives: 225 us -> 99.5 us
  starting transfers between devices: 20.1 us -> 104 us
  waiting for transfers between devices: 38.8 us -> 67.4 us
  matrix products: 4.22 us -> 0.91 us
    all_to_all x9 -> x5, blocking collectives: 225 us -> 99.5 us  [exchange(): return lax.all_to_all(x, axis, split_axis=0, concat_axis=0, tiled=True)]
    all_to_all x3 -> x7, starting transfers between devices: 20.1 us -> 96.9 us  [exchange(): return lax.all_to_all(x, axis, split_axis=0, concat_axis=0, tiled=True)]
    all_to_all x3 -> x7, waiting for transfers between devices: 38.8 us -> 57.9 us  [exchange(): return lax.all_to_all(x, axis, split_axis=0, concat_axis=0, tiled=True)]
    ppermute x0 -> x2, waiting for transfers between devices: none -> 9.54 us  [paired_weights(): got = lax.ppermute(mine(both, 1 - p), 'kvp', [(0, 1), (1, 0)])]
    ppermute x0 -> x2, starting transfers between devices: none -> 6.64 us  [paired_weights(): got = lax.ppermute(mine(both, 1 - p), 'kvp', [(0, 1), (1, 0)])]
    dot_general x17 -> x1, matrix products: 3.43 us -> 0.15 us  [per_device(): jnp.dot(ret_out, w_out, preferred_element_type=jnp.float32)]
  transfers between devices with their start and end apart: 3 -> 9, of which waited for: 3 -> 8; matrix products, arithmetic and copies ran while one was open for 0% -> 1% of each run, Pallas kernels for 0% -> 0%
where the time goes in v3:
time: 285 us; the launch traced here: 284 us
  starting transfers between devices  104 us (36%)
  blocking collectives  99.5 us (35%)
  waiting for transfers between devices  67.4 us (24%)
  local copies, waits for them, and re-layouts  4.68 us (2%)
  other arithmetic  3.89 us (1%)
  Pallas kernels  2.95 us (1%)
    all_to_all x5, blocking collectives, exchange(): return lax.all_to_all(x, axis, split_axis=0, concat_axis=0, tiled=True)  99.5 us
    all_to_all x7, starting transfers between devices, exchange(): return lax.all_to_all(x, axis, split_axis=0, concat_axis=0, tiled=True)  96.9 us
    all_to_all x7, waiting for transfers between devices, exchange(): return lax.all_to_all(x, axis, split_axis=0, concat_axis=0, tiled=True)  57.9 us
    ppermute x2, waiting for transfers between devices, paired_weights(): got = lax.ppermute(mine(both, 1 - p), 'kvp', [(0, 1), (1, 0)])  9.54 us
    ppermute x2, starting transfers between devices, paired_weights(): got = lax.ppermute(mine(both, 1 - p), 'kvp', [(0, 1), (1, 0)])  6.64 us
  transfers between devices with their start and end apart: 9, of which 8 were waited for; matrix products, arithmetic and copies ran while one was open for 1% of the time, Pallas kernels for 0%

profile of v3, /device:TPU:65, one launch (start us, length us, event | category | flops | bytes accessed | tf_op | source)
XLA Modules:
  0.0 284.1 jit_solution(2057019259070050714)
XLA Ops:
  0.7 1.5 broadcast_in_dim.16
  2.2 45.2 %all-to-all-start = ((bf16[32,12,256]{2,1,0:T(8,128)(2,1)}), bf16[32,12,256]{2,1,0:T(8,128)(2,1)S(1)}, u32[]{:S(2)}, u32[]{:S(2)}) async-start(bf16[32,12,256]{2,1,0:T(8,128)(2,1)} %broadcast_in_dim.16), calls=%async_computation | async-start | bytes 524288 | tf_op jit(solution)/shard_map/all_to_all | solution.py:33
  47.6 3.6 %collective-permute-start = (bf16[2,344,256]{2,1,0:T(8,128)(2,1)S(1)}, bf16[2,344,256]{2,1,0:T(8,128)(2,1)S(1)}, u32[]{:S(2)}, u32[]{:S(2)}) collective-permute-start(bf16[2,344,256]{2,1,0:T(8,128)(2,1)S(1)} %get-tuple-element.4), channel_id=1, source_target_pairs={{0,16},{16,0},{1,17},{17,1},{2,18},{18,2},{3,19},{19,3},{4,20},{20... | collective-permute-start | bytes 1056776 | tf_op jit(solution)/shard_map/ppermute | solution.py:119
  51.2 7.1 %all-to-all-done = bf16[32,12,256]{2,1,0:T(8,128)(2,1)S(1)} async-done(((bf16[32,12,256]{2,1,0:T(8,128)(2,1)}), bf16[32,12,256]{2,1,0:T(8,128)(2,1)S(1)}, u32[]{:S(2)}, u32[]{:S(2)}) %all-to-all-start) | async-done | bytes 196640 | tf_op jit(solution)/shard_map/all_to_all | solution.py:33
  58.4 1.3 collective-permute-done.got_ref
  60.1 24.6 %all_to_all.60 = bf16[8,24,768]{2,1,0:T(8,128)(2,1)S(1)} all-to-all(bf16[8,24,768]{2,1,0:T(8,128)(2,1)S(1)} %shard_map.185), channel_id=1, replica_groups=mesh['grp'=2,'kvh'=8,'kvp'=2,'tp'=16] {'kvh'}, dimensions={0} | all-to-all | bytes 589824 | tf_op jit(solution)/shard_map/all_to_all | solution.py:33
  85.1 21.1 %all_to_all.61.h_ref = bf16[16,24,344]{2,1,0:T(8,128)(2,1)S(1)} all-to-all(bf16[16,24,344]{2,1,0:T(8,128)(2,1)S(1)} %broadcast_in_dim.17), channel_id=1, replica_groups=mesh['grp'=2,'kvh'=8,'kvp'=2,'tp'=16] {'kvh','kvp'}, dimensions={0} | all-to-all | bytes 528384 | tf_op jit(solution)/shard_map/all_to_all | solution.py:33
  107.1 14.8 %all-to-all-start.3 = ((bf16[16,24,128]{2,1,0:T(8,128)(2,1)}), bf16[16,24,128]{2,1,0:T(8,128)(2,1)S(1)}, u32[]{:S(2)}, u32[]{:S(2)}) async-start(bf16[16,24,128]{2,1,0:T(8,128)(2,1)} %shard_map.186), calls=%async_computation.3 | async-start | bytes 196608 | tf_op jit(solution)/shard_map/all_to_all | solution.py:33
  121.9 8.5 %all-to-all-done.3 = bf16[16,24,128]{2,1,0:T(8,128)(2,1)S(1)} async-done(((bf16[16,24,128]{2,1,0:T(8,128)(2,1)}), bf16[16,24,128]{2,1,0:T(8,128)(2,1)S(1)}, u32[]{:S(2)}, u32[]{:S(2)}) %all-to-all-start.3) | async-done | bytes 98336 | tf_op jit(solution)/shard_map/all_to_all | solution.py:33
  131.1 3.7 %all-to-all-start.4 = ((bf16[16,24,128]{2,1,0:T(8,128)(2,1)}), bf16[16,24,128]{2,1,0:T(8,128)(2,1)S(1)}, u32[]{:S(2)}, u32[]{:S(2)}) async-start(bf16[16,24,128]{2,1,0:T(8,128)(2,1)} %broadcast_in_dim.19), calls=%async_computation.4 | async-start | bytes 196608 | tf_op jit(solution)/shard_map/all_to_all | solution.py:33
  135.0 8.0 %all-to-all-done.4.y_ref = bf16[16,24,128]{2,1,0:T(8,128)(2,1)S(1)} async-done(((bf16[16,24,128]{2,1,0:T(8,128)(2,1)}), bf16[16,24,128]{2,1,0:T(8,128)(2,1)S(1)}, u32[]{:S(2)}, u32[]{:S(2)}) %all-to-all-start.4) | async-done | bytes 98336 | tf_op jit(solution)/shard_map/all_to_all | solution.py:33
  143.9 5.6 %all-to-all-start.5 = ((bf16[16,16,512]{2,1,0:T(8,128)(2,1)}), bf16[16,16,512]{2,1,0:T(8,128)(2,1)S(1)}, u32[]{:S(2)}, u32[]{:S(2)}) async-start(bf16[16,16,512]{2,1,0:T(8,128)(2,1)} %shard_map.187), calls=%async_computation.5 | async-start | bytes 524288 | tf_op jit(solution)/shard_map/all_to_all | solution.py:33
  149.6 14.0 %all-to-all-done.5 = bf16[16,16,512]{2,1,0:T(8,128)(2,1)S(1)} async-done(((bf16[16,16,512]{2,1,0:T(8,128)(2,1)}), bf16[16,16,512]{2,1,0:T(8,128)(2,1)S(1)}, u32[]{:S(2)}, u32[]{:S(2)}) %all-to-all-start.5) | async-done | bytes 262176 | tf_op jit(solution)/shard_map/all_to_all | solution.py:33
  165.3 21.4 %all_to_all.62 = bf16[16,12,128]{2,1,0:T(8,128)(2,1)S(1)} all-to-all(bf16[16,12,128]{2,1,0:T(8,128)(2,1)S(1)} %broadcast_in_dim.20), channel_id=1, replica_groups=mesh['grp'=2,'kvh'=8,'kvp'=2,'tp'=16] {'kvh','kvp'}, dimensions={0} | all-to-all | bytes 98304 | tf_op jit(solution)/shard_map/all_to_all | solution.py:33
  186.9 13.3 %all_to_all.63 = bf16[16,24,128]{2,1,0:T(8,128)(2,1)S(1)} all-to-all(bf16[16,24,128]{2,1,0:T(8,128)(2,1)S(1)} %bitcast.77), channel_id=1, replica_groups=mesh['grp'=2,'kvh'=8,'kvp'=2,'tp'=16] {'tp'}, dimensions={0} | all-to-all | bytes 196608 | tf_op jit(solution)/shard_map/all_to_all | solution.py:33
  201.0 4.2 %all-to-all-start.8 = ((bf16[32,24,128]{2,1,0:T(8,128)(2,1)}), bf16[32,24,128]{2,1,0:T(8,128)(2,1)S(1)}, u32[]{:S(2)}, u32[]{:S(2)}) async-start(bf16[32,24,128]{2,1,0:T(8,128)(2,1)} %broadcast_in_dim.22), calls=%async_computation.8 | async-start | bytes 393216 | tf_op jit(solution)/shard_map/all_to_all | solution.py:33
  205.5 3.0 %collective-permute-start.1 = (bf16[2,344,256]{2,1,0:T(8,128)(2,1)S(1)}, bf16[2,344,256]{2,1,0:T(8,128)(2,1)S(1)}, u32[]{:S(2)}, u32[]{:S(2)}) collective-permute-start(bf16[2,344,256]{2,1,0:T(8,128)(2,1)S(1)} %get-tuple-element.2), channel_id=1, source_target_pairs={{0,16},{16,0},{1,17},{17,1},{2,18},{18,2},{3,19},{19,3},{4,20},{20... | collective-permute-start | bytes 1056776 | tf_op jit(solution)/shard_map/ppermute | solution.py:119
  208.5 8.2 %collective-permute-done.1.got_ref = bf16[2,344,256]{2,1,0:T(8,128)(2,1)S(1)} collective-permute-done((bf16[2,344,256]{2,1,0:T(8,128)(2,1)S(1)}, bf16[2,344,256]{2,1,0:T(8,128)(2,1)S(1)}, u32[]{:S(2)}, u32[]{:S(2)}) %collective-permute-start.1) | collective-permute-done | bytes 352288 | tf_op jit(solution)/shard_map/ppermute | solution.py:119
  217.2 19.1 %all_to_all.64 = bf16[8,24,768]{2,1,0:T(8,128)(2,1)S(1)} all-to-all(bf16[8,24,768]{2,1,0:T(8,128)(2,1)S(1)} %shard_map.188), channel_id=1, replica_groups=mesh['grp'=2,'kvh'=8,'kvp'=2,'tp'=16] {'kvh'}, dimensions={0} | all-to-all | bytes 589824 | tf_op jit(solution)/shard_map/all_to_all | solution.py:33
  237.3 9.2 %all-to-all-start.10 = ((bf16[16,24,344]{2,1,0:T(8,128)(2,1)}), bf16[16,24,344]{2,1,0:T(8,128)(2,1)S(1)}, u32[]{:S(2)}, u32[]{:S(2)}) async-start(bf16[16,24,344]{2,1,0:T(8,128)(2,1)} %broadcast_in_dim.23), calls=%async_computation.10 | async-start | bytes 589824 | tf_op jit(solution)/shard_map/all_to_all | solution.py:33
  246.6 12.7 %all-to-all-done.10.h_ref = bf16[16,24,344]{2,1,0:T(8,128)(2,1)S(1)} async-done(((bf16[16,24,344]{2,1,0:T(8,128)(2,1)}), bf16[16,24,344]{2,1,0:T(8,128)(2,1)S(1)}, u32[]{:S(2)}, u32[]{:S(2)}) %all-to-all-start.10) | async-done | bytes 264224 | tf_op jit(solution)/shard_map/all_to_all | solution.py:33
  260.2 14.4 %all-to-all-start.11 = ((bf16[16,12,256]{2,1,0:T(8,128)(2,1)}), bf16[16,12,256]{2,1,0:T(8,128)(2,1)S(1)}, u32[]{:S(2)}, u32[]{:S(2)}) async-start(bf16[16,12,256]{2,1,0:T(8,128)(2,1)} %reshape.308), calls=%async_computation.11 | async-start | bytes 262144 | tf_op jit(solution)/shard_map/all_to_all | solution.py:33
  274.6 1.2 multiply_add_fusion
  275.8 7.7 %all-to-all-done.11 = bf16[16,12,256]{2,1,0:T(8,128)(2,1)S(1)} async-done(((bf16[16,12,256]{2,1,0:T(8,128)(2,1)}), bf16[16,12,256]{2,1,0:T(8,128)(2,1)S(1)}, u32[]{:S(2)}, u32[]{:S(2)}) %all-to-all-start.11) | async-done | bytes 98336 | tf_op jit(solution)/shard_map/all_to_all | solution.py:33
  (84 shorter events, 9.8 us)
Async XLA Ops:
  0.6 186.0 %copy-start = (bf16[128,256]{1,0:T(8,128)(2,1)S(1)}, bf16[128,256]{1,0:T(8,128)(2,1)}, u32[]{:S(2)}) copy-start(bf16[128,256]{1,0:T(8,128)(2,1)} %param.30) | copy-start | bytes 196612
  0.6 46.7 %copy-start.4 = (bf16[256,688]{0,1:T(8,128)(2,1)S(1)}, bf16[256,688]{0,1:T(8,128)(2,1)}, u32[]{:S(2)}) copy-start(bf16[256,688]{0,1:T(8,128)(2,1)} %param.23) | copy-start | bytes 1056772
  0.7 46.7 %copy-start.5 = (bf16[256,688]{0,1:T(8,128)(2,1)S(1)}, bf16[256,688]{0,1:T(8,128)(2,1)}, u32[]{:S(2)}) copy-start(bf16[256,688]{0,1:T(8,128)(2,1)} %param.22) | copy-start | bytes 1056772
  0.7 46.7 %copy-start.12 = (f32[256]{0:T(256)S(1)}, f32[256]{0:T(256)}, u32[]{:S(2)}) copy-start(f32[256]{0:T(256)} %param.21) | copy-start | bytes 3076
  2.2 56.1 %all-to-all-start = ((bf16[32,12,256]{2,1,0:T(8,128)(2,1)}), bf16[32,12,256]{2,1,0:T(8,128)(2,1)S(1)}, u32[]{:S(2)}, u32[]{:S(2)}) async-start(bf16[32,12,256]{2,1,0:T(8,128)(2,1)} %broadcast_in_dim.16), calls=%async_computation | async-start | bytes 524288 | tf_op jit(solution)/shard_map/all_to_all | solution.py:33
  47.6 12.1 %collective-permute-start = (bf16[2,344,256]{2,1,0:T(8,128)(2,1)S(1)}, bf16[2,344,256]{2,1,0:T(8,128)(2,1)S(1)}, u32[]{:S(2)}, u32[]{:S(2)}) collective-permute-start(bf16[2,344,256]{2,1,0:T(8,128)(2,1)S(1)} %get-tuple-element.4), channel_id=1, source_target_pairs={{0,16},{16,0},{1,17},{17,1},{2,18},{18,2},{3,19},{19,3},{4,20},{20... | collective-permute-start | bytes 1056776 | tf_op jit(solution)/shard_map/ppermute | solution.py:119
  84.8 21.4 %copy-start.1 = (bf16[688,256]{1,0:T(8,128)(2,1)S(1)}, bf16[688,256]{1,0:T(8,128)(2,1)}, u32[]{:S(2)}) copy-start(bf16[688,256]{1,0:T(8,128)(2,1)} %w_ref.2) | copy-start | bytes 1056772
  106.2 28.6 %copy-start.8 = (bf16[256,128]{1,0:T(8,128)(2,1)S(1)}, bf16[256,128]{1,0:T(8,128)(2,1)}, u32[]{:S(2)}) copy-start(bf16[256,128]{1,0:T(8,128)(2,1)} %param.29) | copy-start | bytes 196612
  106.2 28.6 %copy-start.9 = (bf16[256,128]{1,0:T(8,128)(2,1)S(1)}, bf16[256,128]{1,0:T(8,128)(2,1)}, u32[]{:S(2)}) copy-start(bf16[256,128]{1,0:T(8,128)(2,1)} %param.28) | copy-start | bytes 196612
  106.2 28.6 %copy-start.10 = (bf16[256,128]{1,0:T(8,128)(2,1)S(1)}, bf16[256,128]{1,0:T(8,128)(2,1)}, u32[]{:S(2)}) copy-start(bf16[256,128]{1,0:T(8,128)(2,1)} %param.27) | copy-start | bytes 196612
  106.2 28.6 %copy-start.11 = (bf16[256,128]{1,0:T(8,128)(2,1)S(1)}, bf16[256,128]{1,0:T(8,128)(2,1)}, u32[]{:S(2)}) copy-start(bf16[256,128]{1,0:T(8,128)(2,1)} %param.26) | copy-start | bytes 196612
  106.2 28.6 %copy-start.13 = (f32[256]{0:T(256)S(1)}, f32[256]{0:T(256)}, u32[]{:S(2)}) copy-start(f32[256]{0:T(256)} %param.25) | copy-start | bytes 3076
  107.1 23.2 %all-to-all-start.3 = ((bf16[16,24,128]{2,1,0:T(8,128)(2,1)}), bf16[16,24,128]{2,1,0:T(8,128)(2,1)S(1)}, u32[]{:S(2)}, u32[]{:S(2)}) async-start(bf16[16,24,128]{2,1,0:T(8,128)(2,1)} %shard_map.186), calls=%async_computation.3 | async-start | bytes 196608 | tf_op jit(solution)/shard_map/all_to_all | solution.py:33
  131.1 11.8 %all-to-all-start.4 = ((bf16[16,24,128]{2,1,0:T(8,128)(2,1)}), bf16[16,24,128]{2,1,0:T(8,128)(2,1)S(1)}, u32[]{:S(2)}, u32[]{:S(2)}) async-start(bf16[16,24,128]{2,1,0:T(8,128)(2,1)} %broadcast_in_dim.19), calls=%async_computation.4 | async-start | bytes 196608 | tf_op jit(solution)/shard_map/all_to_all | solution.py:33
  134.9 29.1 %copy-start.3 = (f32[12,1,128,128]{3,2,1,0:T(8,128)S(1)}, f32[12,1,128,128]{3,2,1,0:T(8,128)}, u32[]{:S(2)}) copy-start(f32[12,1,128,128]{3,2,1,0:T(8,128)} %param.20) | copy-start | bytes 2359300
  143.9 19.7 %all-to-all-start.5 = ((bf16[16,16,512]{2,1,0:T(8,128)(2,1)}), bf16[16,16,512]{2,1,0:T(8,128)(2,1)S(1)}, u32[]{:S(2)}, u32[]{:S(2)}) async-start(bf16[16,16,512]{2,1,0:T(8,128)(2,1)} %shard_map.187), calls=%async_computation.5 | async-start | bytes 524288 | tf_op jit(solution)/shard_map/all_to_all | solution.py:33
  186.7 18.5 %copy-start.6 = (bf16[256,688]{0,1:T(8,128)(2,1)S(1)}, bf16[256,688]{0,1:T(8,128)(2,1)}, u32[]{:S(2)}) copy-start(bf16[256,688]{0,1:T(8,128)(2,1)} %param.34) | copy-start | bytes 1056772
  186.7 18.5 %copy-start.7 = (bf16[256,688]{0,1:T(8,128)(2,1)S(1)}, bf16[256,688]{0,1:T(8,128)(2,1)}, u32[]{:S(2)}) copy-start(bf16[256,688]{0,1:T(8,128)(2,1)} %param.33) | copy-start | bytes 1056772
  186.7 18.5 %copy-start.14 = (f32[256]{0:T(256)S(1)}, f32[256]{0:T(256)}, u32[]{:S(2)}) copy-start(f32[256]{0:T(256)} %param.32) | copy-start | bytes 3076
  201.0 15.7 %all-to-all-start.8 = ((bf16[32,24,128]{2,1,0:T(8,128)(2,1)}), bf16[32,24,128]{2,1,0:T(8,128)(2,1)S(1)}, u32[]{:S(2)}, u32[]{:S(2)}) async-start(bf16[32,24,128]{2,1,0:T(8,128)(2,1)} %broadcast_in_dim.22), calls=%async_computation.8 | async-start | bytes 393216 | tf_op jit(solution)/shard_map/all_to_all | solution.py:33
  205.5 11.3 %collective-permute-start.1 = (bf16[2,344,256]{2,1,0:T(8,128)(2,1)S(1)}, bf16[2,344,256]{2,1,0:T(8,128)(2,1)S(1)}, u32[]{:S(2)}, u32[]{:S(2)}) collective-permute-start(bf16[2,344,256]{2,1,0:T(8,128)(2,1)S(1)} %get-tuple-element.2), channel_id=1, source_target_pairs={{0,16},{16,0},{1,17},{17,1},{2,18},{18,2},{3,19},{19,3},{4,20},{20... | collective-permute-start | bytes 1056776 | tf_op jit(solution)/shard_map/ppermute | solution.py:119
  236.2 23.1 %copy-start.2 = (bf16[688,256]{1,0:T(8,128)(2,1)S(1)}, bf16[688,256]{1,0:T(8,128)(2,1)}, u32[]{:S(2)}) copy-start(bf16[688,256]{1,0:T(8,128)(2,1)} %w_ref.3) | copy-start | bytes 1056772
  237.3 22.0 %all-to-all-start.10 = ((bf16[16,24,344]{2,1,0:T(8,128)(2,1)}), bf16[16,24,344]{2,1,0:T(8,128)(2,1)S(1)}, u32[]{:S(2)}, u32[]{:S(2)}) async-start(bf16[16,24,344]{2,1,0:T(8,128)(2,1)} %broadcast_in_dim.23), calls=%async_computation.10 | async-start | bytes 589824 | tf_op jit(solution)/shard_map/all_to_all | solution.py:33
  260.2 23.2 %all-to-all-start.11 = ((bf16[16,12,256]{2,1,0:T(8,128)(2,1)}), bf16[16,12,256]{2,1,0:T(8,128)(2,1)S(1)}, u32[]{:S(2)}, u32[]{:S(2)}) async-start(bf16[16,12,256]{2,1,0:T(8,128)(2,1)} %reshape.308), calls=%async_computation.11 | async-start | bytes 262144 | tf_op jit(solution)/shard_map/all_to_all | solution.py:33
  (2 other events, 30.4 us)

commit v4 on v3

--- a/solution.py
+++ b/solution.py
@@ -1,5 +1,3 @@
-import functools
-
 import jax
 import jax.numpy as jnp
 import numpy as np
@@ -72,37 +70,34 @@
             out_ref[r, :, i * half : (i + 1) * half] = rows[r * tall : (r + 1) * tall]
 
 
-def down_kernel(h_ref, w_ref, out_ref, h):
-    groups, tall, part = h_ref.shape
-    cuts = w_ref.shape[0] // part
-    value = 0.0
-    for c in range(cuts):
-        for r in range(groups // cuts):
-            h[r * tall : (r + 1) * tall] = h_ref[r * cuts + c]
-        value += jnp.dot(h[...], w_ref[c * part : (c + 1) * part], preferred_element_type=jnp.float32)
-    value = value.astype(jnp.bfloat16)
-    if len(out_ref.shape) == 2:
-        out_ref[...] = value
-        return
-    chunks, high, wide = out_ref.shape
-    across = value.shape[1] // wide
-    for n in range(chunks):
-        r, c = divmod(n, across)
-        out_ref[n] = value[r * high : (r + 1) * high, c * wide : (c + 1) * wide]
-
-
-def heads_kernel(y_ref, w_ref, out_ref, x, scr):
-    chunks, tall, wide = y_ref.shape
-    across = x.shape[1] // wide
-    for n in range(chunks):
-        r, c = divmod(n, across)
-        x[r * tall : (r + 1) * tall, c * wide : (c + 1) * wide] = y_ref[n]
+def down_kernel(h_ref, own_ref, got_ref, out_ref, h):
+    groups, tall, _ = h_ref.shape
+    p = lax.axis_index("kvp")
+    for r in range(groups):
+        h[r * tall : (r + 1) * tall] = h_ref[r]
+    for place, w in ((p, own_ref), (1 - p, got_ref)):
+        value = jnp.dot(h[...], w[2], preferred_element_type=jnp.float32).astype(jnp.bfloat16)
+        if len(out_ref.shape) == 3:
+            out_ref[place] = value
+            continue
+        _, chunks, high, wide = out_ref.shape
+        across = value.shape[1] // wide
+        for n in range(chunks):
+            r, c = divmod(n, across)
+            out_ref[place, n] = value[r * high : (r + 1) * high, c * wide : (c + 1) * wide]
+
+
+def heads_kernel(y_ref, own_ref, got_ref, out_ref, x, scr):
+    fill_rows(x, y_ref, lax.axis_index("kvp"))
     members, high, lanes = out_ref.shape
-    rows = x.shape[0]
+    rows = x.shape[1]
     each = rows // members
-    squares = jnp.sum(jnp.square(x[...].astype(jnp.float32)), axis=1, keepdims=True)
-    scr[:rows, :lanes] = jnp.dot(x[...], w_ref[...], preferred_element_type=jnp.float32)
+    squares = sum(jnp.sum(jnp.square(x[j].astype(jnp.float32)), axis=1, keepdims=True) for j in range(2))
+    scr[:rows, :lanes] = sum(
+        jnp.dot(x[j], w[...], preferred_element_type=jnp.float32) for j, w in enumerate((own_ref, got_ref))
+    )
     scr[:rows, lanes:] = jnp.broadcast_to(squares, (rows, 128))
+    scr[rows:] = jnp.zeros((scr.shape[0] - rows, scr.shape[1]), jnp.float32)
     row = lax.broadcasted_iota(jnp.int32, (high, 128), 0)
     lane = lax.broadcasted_iota(jnp.int32, (high, 128), 1)
     for k in range(members):
@@ -112,17 +107,20 @@
         out_ref[k, :, 128:] = piece[:, 128:lanes].astype(jnp.bfloat16)
 
 
-def paired_weights(norm_gain, w_gate, w_up):
+def swapped(both):
     p = lax.axis_index("kvp")
-    both = jnp.stack([w.T.reshape(2, -1, w.shape[0]) for w in (w_gate, w_up)], axis=1)
-    both = (both.astype(jnp.float32) * norm_gain).astype(jnp.bfloat16)
-    got = lax.ppermute(mine(both, 1 - p), "kvp", [(0, 1), (1, 0)])
-    return mine(both, p), got
-
-
-def feed_forward(gathered, weights, w_down, flat):
+    return mine(both, p), lax.ppermute(mine(both, 1 - p), "kvp", [(0, 1), (1, 0)])
+
+
+def paired_weights(norm_gain, w_gate, w_up, w_down):
+    width = w_gate.shape[0]
+    scaled = [(w.T.astype(jnp.float32) * norm_gain).astype(jnp.bfloat16) for w in (w_gate, w_up)]
+    return swapped(jnp.stack([w.reshape(2, -1, width) for w in (*scaled, w_down)], axis=1))
+
+
+def feed_forward(gathered, weights, flat):
     own_w, got_w = weights
-    members = lax.axis_size("kvh")
+    members, tp = lax.axis_size("kvh"), lax.axis_size("tp")
     wide, part = own_w.shape[2], own_w.shape[1]
     rows = gathered.size // (2 * wide)
     tall, half = rows // members, -(-(part + 1) // 128) * 128
@@ -139,21 +137,21 @@
     features = wide * lax.axis_size(KV)
     factor = lax.rsqrt(total[:, part : part + 1] / features + EPS_NORM)
     hidden = jax.nn.silu(factor * total[:, :part]) * (factor * total[:, half : half + part])
-    everyone = spread(hidden.astype(jnp.bfloat16), KV)
-    width = w_down.shape[1]
-    shape = (rows, width) if flat else (lax.axis_size("tp"), tall, 2 * rows * width // (lax.axis_size("tp") * 2 * tall))
+    everyone = spread(hidden.astype(jnp.bfloat16), "kvh")
+    shape = (2, rows, wide) if flat else (2, tp, tall, rows * wide // (tp * tall))
     return local_call(
         down_kernel,
         jax.ShapeDtypeStruct(shape, jnp.bfloat16),
         everyone,
-        w_down,
+        own_w,
+        got_w,
         scratch=(pltpu.VMEM((rows, part), jnp.bfloat16),),
-        flops=4 * rows * part * width,
-    )
-
-
-def advance(own, back, branch):
-    share = exchange(back, "tp").astype(jnp.float32).sum(axis=0)
+        flops=4 * rows * part * wide,
+    )
+
+
+def advance(own, back, branch, axis):
+    share = exchange(back, axis).astype(jnp.float32).sum(axis=0)
     return (own.astype(jnp.float32) + branch * share).astype(jnp.bfloat16)
 
 
@@ -163,29 +161,31 @@
     return jnp.concatenate([low * cosine - high * sine, low * sine + high * cosine], axis=-1)
 
 
-def retention(gathered, w_heads, features, head_gain, state, tables):
+def retention(gathered, weights, features, head_gain, state, tables):
     cosine, sine, decays = tables
     count, heads, width, _ = state.shape
     members = lax.axis_size(KV)
-    chunks, tall, wide = gathered.shape
-    block, lanes = w_heads.shape
+    block, lanes = weights[0].shape
     rows = members * count
     high = -(-(count + 1) // 8) * 8
     sent = local_call(
         heads_kernel,
         jax.ShapeDtypeStruct((members, high, lanes), jnp.bfloat16),
         gathered,
-        w_heads,
+        *weights,
         scratch=(
-            pltpu.VMEM((rows, block), jnp.bfloat16),
+            pltpu.VMEM((2, rows, block), jnp.bfloat16),
             pltpu.VMEM((rows + 8, lanes + 128), jnp.float32),
         ),
-        flops=2 * rows * block * lanes,
-    )
-    total = exchange(sent, KV).astype(jnp.float32).sum(axis=0)
-    factor = lax.rsqrt(total[count, :count] / features + EPS_NORM)[:, None]
-    total = factor * total[:count]
-    q, k, v, o = (total[:, i * heads * width : (i + 1) * heads * width].reshape(count, heads, width) for i in range(4))
+        flops=4 * rows * block * lanes,
+    )
+    total = exchange(sent, KV).reshape(members // 2, 2, high, lanes).astype(jnp.float32).sum(axis=0)
+    factor = lax.rsqrt(total[0, count, :count] / features + EPS_NORM)[:, None]
+    total = factor * total[:, :count]
+    wide = heads * width
+    q, k, v, o = (
+        total[i // 2, :, i % 2 * wide : (i % 2 + 1) * wide].reshape(count, heads, width) for i in range(4)
+    )
     q = rotate(q, cosine, sine)
     k = rotate(k, cosine, sine) * width ** (-0.5)
     carried = jnp.einsum("shd,shde->she", q, state, precision=lax.Precision.HIGHEST)
@@ -226,6 +226,7 @@
     groups = lax.axis_size("kvh")
     tall, across = rows // groups, tp // groups
     wide = block // across
+    r, c = lax.div(t, across), lax.rem(t, across)
 
     half = ret_state.shape[-1] // 2
     inverse = 10000.0 ** (-jnp.arange(half, dtype=jnp.float32) / half)
@@ -234,31 +235,31 @@
     heads = ret_state.shape[1]
     head_ids = (t * heads + jnp.arange(heads)).astype(jnp.float32)
     decays = jnp.exp(jnp.log1p(-(2.0 ** (-5.0 - head_ids))))
-
-    first_pair = paired_weights(first_gain, first_gate, first_up)
-    second_pair = paired_weights(second_gain, second_gate, second_up)
-    w_heads = jnp.concatenate([w_query, w_key, w_value, w_outgate], axis=1)
-    w_heads = (w_heads.astype(jnp.float32) * mix_gain[:, None]).astype(jnp.bfloat16)
+    tables = (cosine, sine, decays)
+
+    first_pair = paired_weights(first_gain, first_gate, first_up, first_down)
+    second_pair = paired_weights(second_gain, second_gate, second_up, second_down)
+    halves = [jnp.concatenate(w, axis=1) for w in ((w_query, w_key), (w_value, w_outgate))]
+    halves = jnp.stack(halves).astype(jnp.float32) * mix_gain[:, None]
+    heads_pair = swapped(halves.astype(jnp.bfloat16))
 
     gathered = spread(stream_in, BOTH).reshape(2, rows, block)
-    own = lax.dynamic_slice(gathered, (p, (t // across) * tall, (t % across) * wide), (1, tall, wide))[0]
-    back = feed_forward(gathered, first_pair, first_down, False)
-    own = advance(own, back, 0.5)
-    gathered = spread(own, "tp")
-    ret_out, new_state = retention(
-        gathered, w_heads, features, head_gain, ret_state, (cosine, sine, decays)
-    )
+    own = lax.dynamic_slice(gathered, (p, r * tall, c * wide), (1, tall, wide))[0]
+    gathered, own, tables = lax.optimization_barrier((gathered, own, tables))
+    back = feed_forward(gathered, first_pair, False)
+    own = advance(own, back.reshape(2 * tp, tall, wide), 0.5, BOTH)
+    gathered = spread(own, BOTH).reshape(2, tp, tall, wide)
+    ret_out, new_state = retention(gathered, heads_pair, features, head_gain, ret_state, tables)
     back = jnp.dot(ret_out, w_out, preferred_element_type=jnp.float32).astype(jnp.bfloat16)
     back = back.reshape(groups, tall, across, wide).transpose(0, 2, 1, 3).reshape(tp, tall, wide)
-    own = advance(own, back, 1.0)
+    own = advance(own, back, 1.0, "tp")
     gathered = spread(own, BOTH).reshape(2, tp, tall, wide)
-    place = (t * few) // tall
-    own = lax.dynamic_slice(
-        gathered, (p, place * across, t * few - place * tall, 0), (1, across, few, wide)
-    )[0]
-    own = jnp.concatenate([own[c] for c in range(across)], axis=1)
-    back = feed_forward(gathered, second_pair, second_down, True)
-    return advance(own, back.reshape(tp, few, block), 0.5), new_state
+    place = lax.div(t * few, tall)
+    own = lax.dynamic_slice(gathered, (p, place * across, t * few - place * tall, 0), (1, across, few, wide))[0]
+    own = jnp.concatenate([own[i] for i in range(across)], axis=1)
+    gathered, own = lax.optimization_barrier((gathered, own))
+    back = feed_forward(gathered, second_pair, True)
+    return advance(own, back.reshape(2 * tp, few, block), 0.5, BOTH), new_state
 
 
 def solution(mesh):
@@ -287,6 +288,4 @@
         flat,
     )
     out_specs = (rows, P(("grp", *KV), "tp", None, None))
-    return jax.shard_map(
-        per_device, mesh=fine, in_specs=in_specs, out_specs=out_specs, check_vma=False
-    )
+    return jax.shard_map(per_device, mesh=fine, in_specs=in_specs, out_specs=out_specs, check_vma=False)

time: 285 us -> 283 us (level)
  blocking collectives: 99.5 us -> 154 us
  waiting for transfers between devices: 67.4 us -> 38.3 us
  starting transfers between devices: 104 us -> 76.4 us
    all_to_all x5 -> x8, blocking collectives: 99.5 us -> 154 us  [exchange(): return lax.all_to_all(x, axis, split_axis=0, concat_axis=0, tiled=True)]
    all_to_all x7 -> x4, waiting for transfers between devices: 57.9 us -> 24.1 us  [exchange(): return lax.all_to_all(x, axis, split_axis=0, concat_axis=0, tiled=True)]
    all_to_all x7 -> x4, starting transfers between devices: 96.9 us -> 66.4 us  [exchange(): return lax.all_to_all(x, axis, split_axis=0, concat_axis=0, tiled=True)]
    ppermute x2 -> x3, waiting for transfers between devices: 9.54 us -> 14.1 us  [swapped(): lax.ppermute(mine(both, 1 - p), 'kvp', [(0, 1), (1, 0)])]
    ppermute x2 -> x3, starting transfers between devices: 6.64 us -> 10 us  [swapped(): lax.ppermute(mine(both, 1 - p), 'kvp', [(0, 1), (1, 0)])]
  transfers between devices with their start and end apart: 9 -> 7, of which waited for: 8 -> 7; matrix products, arithmetic and copies ran while one was open for 1% -> 1% of each run, Pallas kernels for 0% -> 0%
where the time goes in v4:
time: 283 us; the launch traced here: 282 us
  blocking collectives  154 us (54%)
  starting transfers between devices  76.4 us (27%)
  waiting for transfers between devices  38.3 us (14%)
  other arithmetic  5.36 us (2%)
  local copies, waits for them, and re-layouts  4.18 us (1%)
    all_to_all x8, blocking collectives, exchange(): return lax.all_to_all(x, axis, split_axis=0, concat_axis=0, tiled=True)  154 us
    all_to_all x4, starting transfers between devices, exchange(): return lax.all_to_all(x, axis, split_axis=0, concat_axis=0, tiled=True)  66.4 us
    all_to_all x4, waiting for transfers between devices, exchange(): return lax.all_to_all(x, axis, split_axis=0, concat_axis=0, tiled=True)  24.1 us
    ppermute x3, waiting for transfers between devices, swapped(): lax.ppermute(mine(both, 1 - p), 'kvp', [(0, 1), (1, 0)])  14.1 us
    ppermute x3, starting transfers between devices, swapped(): lax.ppermute(mine(both, 1 - p), 'kvp', [(0, 1), (1, 0)])  10 us
  transfers between devices with their start and end apart: 7, of which 7 were waited for; matrix products, arithmetic and copies ran while one was open for 1% of the time, Pallas kernels for 0%

profile of v4, /device:TPU:65, one launch (start us, length us, event | category | flops | bytes accessed | tf_op | source)
XLA Modules:
  0.0 282.2 jit_solution(11510592095220262585)
XLA Ops:
  0.7 1.5 broadcast_in_dim.12
  2.1 45.2 %all-to-all-start = ((bf16[32,12,256]{2,1,0:T(8,128)(2,1)}), bf16[32,12,256]{2,1,0:T(8,128)(2,1)S(1)}, u32[]{:S(2)}, u32[]{:S(2)}) async-start(bf16[32,12,256]{2,1,0:T(8,128)(2,1)} %broadcast_in_dim.12), calls=%async_computation | async-start | bytes 524288 | tf_op jit(solution)/shard_map/all_to_all | solution.py:31
  47.3 1.2 multiply_convert_fusion.3
  48.9 3.5 %collective-permute-start = (bf16[3,344,256]{2,1,0:T(8,128)(2,1)S(1)}, bf16[3,344,256]{2,1,0:T(8,128)(2,1)S(1)}, u32[]{:S(2)}, u32[]{:S(2)}) collective-permute-start(bf16[3,344,256]{2,1,0:T(8,128)(2,1)S(1)} %get-tuple-element.18), channel_id=1, source_target_pairs={{0,16},{16,0},{1,17},{17,1},{2,18},{18,2},{3,19},{19,3},{4,20},{20... | collective-permute-start | bytes 1585160 | tf_op jit(solution)/shard_map/ppermute | solution.py:112
  52.7 5.5 %all-to-all-done = bf16[32,12,256]{2,1,0:T(8,128)(2,1)S(1)} async-done(((bf16[32,12,256]{2,1,0:T(8,128)(2,1)}), bf16[32,12,256]{2,1,0:T(8,128)(2,1)S(1)}, u32[]{:S(2)}, u32[]{:S(2)}) %all-to-all-start) | async-done | bytes 196640 | tf_op jit(solution)/shard_map/all_to_all | solution.py:31
  58.3 5.3 %collective-permute-done.got_ref = bf16[3,344,256]{2,1,0:T(8,128)(2,1)S(1)} collective-permute-done((bf16[3,344,256]{2,1,0:T(8,128)(2,1)S(1)}, bf16[3,344,256]{2,1,0:T(8,128)(2,1)S(1)}, u32[]{:S(2)}, u32[]{:S(2)}) %collective-permute-start) | collective-permute-done | bytes 528416 | tf_op jit(solution)/shard_map/ppermute | solution.py:112
  64.1 24.2 %all_to_all.60 = bf16[8,24,768]{2,1,0:T(8,128)(2,1)S(1)} all-to-all(bf16[8,24,768]{2,1,0:T(8,128)(2,1)S(1)} %shard_map.185), channel_id=1, replica_groups=mesh['grp'=2,'kvh'=8,'kvp'=2,'tp'=16] {'kvh'}, dimensions={0} | all-to-all | bytes 589824 | tf_op jit(solution)/shard_map/all_to_all | solution.py:31
  88.6 19.7 %all_to_all.61.h_ref = bf16[8,24,344]{2,1,0:T(8,128)(2,1)S(1)} all-to-all(bf16[8,24,344]{2,1,0:T(8,128)(2,1)S(1)} %broadcast_in_dim.13), channel_id=1, replica_groups=mesh['grp'=2,'kvh'=8,'kvp'=2,'tp'=16] {'kvh'}, dimensions={0} | all-to-all | bytes 264192 | tf_op jit(solution)/shard_map/all_to_all | solution.py:31
  108.6 23.9 %all_to_all.62 = bf16[32,24,128]{2,1,0:T(8,128)(2,1)S(1)} all-to-all(bf16[32,24,128]{2,1,0:T(8,128)(2,1)S(1)} %bitcast.101), channel_id=1, replica_groups=mesh['grp'=2,'kvh'=8,'kvp'=2,'tp'=16] {'kvp','tp'}, dimensions={0} | all-to-all | bytes 393216 | tf_op jit(solution)/shard_map/all_to_all | solution.py:31
  133.2 4.4 %all-to-all-start.4 = ((bf16[32,24,128]{2,1,0:T(8,128)(2,1)}), bf16[32,24,128]{2,1,0:T(8,128)(2,1)S(1)}, u32[]{:S(2)}, u32[]{:S(2)}) async-start(bf16[32,24,128]{2,1,0:T(8,128)(2,1)} %broadcast_in_dim.14), calls=%async_computation.4 | async-start | bytes 393216 | tf_op jit(solution)/shard_map/all_to_all | solution.py:31
  137.9 3.4 %collective-permute-start.1 = (bf16[256,256]{1,0:T(8,128)(2,1)S(1)}, bf16[256,256]{1,0:T(8,128)(2,1)S(1)}, u32[]{:S(2)}, u32[]{:S(2)}) collective-permute-start(bf16[256,256]{1,0:T(8,128)(2,1)S(1)} %get-tuple-element.20), channel_id=1, source_target_pairs={{0,16},{16,0},{1,17},{17,1},{2,18},{18,2},{3,19},{19,3},{4,20},{20... | collective-permute-start | bytes 393224 | tf_op jit(solution)/shard_map/ppermute | solution.py:112
  141.4 3.0 %collective-permute-done.1.got_ref = bf16[256,256]{1,0:T(8,128)(2,1)S(1)} collective-permute-done((bf16[256,256]{1,0:T(8,128)(2,1)S(1)}, bf16[256,256]{1,0:T(8,128)(2,1)S(1)}, u32[]{:S(2)}, u32[]{:S(2)}) %collective-permute-start.1) | collective-permute-done | bytes 131104 | tf_op jit(solution)/shard_map/ppermute | solution.py:112
  144.3 3.1 %all-to-all-done.4 = bf16[32,24,128]{2,1,0:T(8,128)(2,1)S(1)} async-done(((bf16[32,24,128]{2,1,0:T(8,128)(2,1)}), bf16[32,24,128]{2,1,0:T(8,128)(2,1)S(1)}, u32[]{:S(2)}, u32[]{:S(2)}) %all-to-all-start.4) | async-done | bytes 196640 | tf_op jit(solution)/shard_map/all_to_all | solution.py:31
  147.7 14.7 %all_to_all.63 = bf16[16,16,256]{2,1,0:T(8,128)(2,1)S(1)} all-to-all(bf16[16,16,256]{2,1,0:T(8,128)(2,1)S(1)} %shard_map.187), channel_id=1, replica_groups=mesh['grp'=2,'kvh'=8,'kvp'=2,'tp'=16] {'kvh','kvp'}, dimensions={0} | all-to-all | bytes 262144 | tf_op jit(solution)/shard_map/all_to_all | solution.py:31
  164.0 17.2 %all_to_all.64 = bf16[16,12,128]{2,1,0:T(8,128)(2,1)S(1)} all-to-all(bf16[16,12,128]{2,1,0:T(8,128)(2,1)S(1)} %broadcast_in_dim.15), channel_id=1, replica_groups=mesh['grp'=2,'kvh'=8,'kvp'=2,'tp'=16] {'kvh','kvp'}, dimensions={0} | all-to-all | bytes 98304 | tf_op jit(solution)/shard_map/all_to_all | solution.py:31
  181.5 15.5 %all_to_all.65 = bf16[16,24,128]{2,1,0:T(8,128)(2,1)S(1)} all-to-all(bf16[16,24,128]{2,1,0:T(8,128)(2,1)S(1)} %bitcast.107), channel_id=1, replica_groups=mesh['grp'=2,'kvh'=8,'kvp'=2,'tp'=16] {'tp'}, dimensions={0} | all-to-all | bytes 196608 | tf_op jit(solution)/shard_map/all_to_all | solution.py:31
  197.8 4.2 %all-to-all-start.8 = ((bf16[32,24,128]{2,1,0:T(8,128)(2,1)}), bf16[32,24,128]{2,1,0:T(8,128)(2,1)S(1)}, u32[]{:S(2)}, u32[]{:S(2)}) async-start(bf16[32,24,128]{2,1,0:T(8,128)(2,1)} %broadcast_in_dim.16), calls=%async_computation.8 | async-start | bytes 393216 | tf_op jit(solution)/shard_map/all_to_all | solution.py:31
  202.4 3.1 %collective-permute-start.2 = (bf16[3,344,256]{2,1,0:T(8,128)(2,1)S(1)}, bf16[3,344,256]{2,1,0:T(8,128)(2,1)S(1)}, u32[]{:S(2)}, u32[]{:S(2)}) collective-permute-start(bf16[3,344,256]{2,1,0:T(8,128)(2,1)S(1)} %get-tuple-element.16), channel_id=1, source_target_pairs={{0,16},{16,0},{1,17},{17,1},{2,18},{18,2},{3,19},{19,3},{4,20},{20... | collective-permute-start | bytes 1585160 | tf_op jit(solution)/shard_map/ppermute | solution.py:112
  205.5 6.0 %all-to-all-done.8 = bf16[32,24,128]{2,1,0:T(8,128)(2,1)S(1)} async-done(((bf16[32,24,128]{2,1,0:T(8,128)(2,1)}), bf16[32,24,128]{2,1,0:T(8,128)(2,1)S(1)}, u32[]{:S(2)}, u32[]{:S(2)}) %all-to-all-start.8) | async-done | bytes 196640 | tf_op jit(solution)/shard_map/all_to_all | solution.py:31
  211.5 5.9 %collective-permute-done.2.got_ref = bf16[3,344,256]{2,1,0:T(8,128)(2,1)S(1)} collective-permute-done((bf16[3,344,256]{2,1,0:T(8,128)(2,1)S(1)}, bf16[3,344,256]{2,1,0:T(8,128)(2,1)S(1)}, u32[]{:S(2)}, u32[]{:S(2)}) %collective-permute-start.2) | collective-permute-done | bytes 528416 | tf_op jit(solution)/shard_map/ppermute | solution.py:112
  217.8 19.5 %all_to_all.66 = bf16[8,24,768]{2,1,0:T(8,128)(2,1)S(1)} all-to-all(bf16[8,24,768]{2,1,0:T(8,128)(2,1)S(1)} %shard_map.188), channel_id=1, replica_groups=mesh['grp'=2,'kvh'=8,'kvp'=2,'tp'=16] {'kvh'}, dimensions={0} | all-to-all | bytes 589824 | tf_op jit(solution)/shard_map/all_to_all | solution.py:31
  237.7 19.5 %all_to_all.67.h_ref = bf16[8,24,344]{2,1,0:T(8,128)(2,1)S(1)} all-to-all(bf16[8,24,344]{2,1,0:T(8,128)(2,1)S(1)} %broadcast_in_dim.17), channel_id=1, replica_groups=mesh['grp'=2,'kvh'=8,'kvp'=2,'tp'=16] {'kvh'}, dimensions={0} | all-to-all | bytes 264192 | tf_op jit(solution)/shard_map/all_to_all | solution.py:31
  258.1 12.6 %all-to-all-start.11 = ((bf16[32,12,256]{2,1,0:T(8,128)(2,1)}), bf16[32,12,256]{2,1,0:T(8,128)(2,1)S(1)}, u32[]{:S(2)}, u32[]{:S(2)}) async-start(bf16[32,12,256]{2,1,0:T(8,128)(2,1)} %reshape.303), calls=%async_computation.11 | async-start | bytes 524288 | tf_op jit(solution)/shard_map/all_to_all | solution.py:31
  272.0 9.6 %all-to-all-done.11 = bf16[32,12,256]{2,1,0:T(8,128)(2,1)S(1)} async-done(((bf16[32,12,256]{2,1,0:T(8,128)(2,1)}), bf16[32,12,256]{2,1,0:T(8,128)(2,1)S(1)}, u32[]{:S(2)}, u32[]{:S(2)}) %all-to-all-start.11) | async-done | bytes 196640 | tf_op jit(solution)/shard_map/all_to_all | solution.py:31
  (84 shorter events, 9.4 us)
Async XLA Ops:
  0.6 180.7 %copy-start = (bf16[128,256]{1,0:T(8,128)(2,1)S(1)}, bf16[128,256]{1,0:T(8,128)(2,1)}, u32[]{:S(2)}) copy-start(bf16[128,256]{1,0:T(8,128)(2,1)} %param.30) | copy-start | bytes 196612
  0.6 47.9 %copy-start.4 = (bf16[688,256]{1,0:T(8,128)(2,1)S(1)}, bf16[688,256]{1,0:T(8,128)(2,1)}, u32[]{:S(2)}) copy-start(bf16[688,256]{1,0:T(8,128)(2,1)} %param.24) | copy-start | bytes 1056772
  2.1 56.1 %all-to-all-start = ((bf16[32,12,256]{2,1,0:T(8,128)(2,1)}), bf16[32,12,256]{2,1,0:T(8,128)(2,1)S(1)}, u32[]{:S(2)}, u32[]{:S(2)}) async-start(bf16[32,12,256]{2,1,0:T(8,128)(2,1)} %broadcast_in_dim.12), calls=%async_computation | async-start | bytes 524288 | tf_op jit(solution)/shard_map/all_to_all | solution.py:31
  48.7 3.7 %copy-start.13 = (s32[12]{0:T(128)S(1)}, s32[12]{0:T(128)}, u32[]{:S(2)}) copy-start(s32[12]{0:T(128)} %param.19) | copy-start | bytes 148
  48.9 14.8 %collective-permute-start = (bf16[3,344,256]{2,1,0:T(8,128)(2,1)S(1)}, bf16[3,344,256]{2,1,0:T(8,128)(2,1)S(1)}, u32[]{:S(2)}, u32[]{:S(2)}) collective-permute-start(bf16[3,344,256]{2,1,0:T(8,128)(2,1)S(1)} %get-tuple-element.18), channel_id=1, source_target_pairs={{0,16},{16,0},{1,17},{17,1},{2,18},{18,2},{3,19},{19,3},{4,20},{20... | collective-permute-start | bytes 1585160 | tf_op jit(solution)/shard_map/ppermute | solution.py:112
  108.3 29.4 %copy-start.6 = (bf16[256,128]{1,0:T(8,128)(2,1)S(1)}, bf16[256,128]{1,0:T(8,128)(2,1)}, u32[]{:S(2)}) copy-start(bf16[256,128]{1,0:T(8,128)(2,1)} %param.27) | copy-start | bytes 196612
  108.3 29.4 %copy-start.7 = (bf16[256,128]{1,0:T(8,128)(2,1)S(1)}, bf16[256,128]{1,0:T(8,128)(2,1)}, u32[]{:S(2)}) copy-start(bf16[256,128]{1,0:T(8,128)(2,1)} %param.26) | copy-start | bytes 196612
  108.3 29.4 %copy-start.8 = (bf16[256,128]{1,0:T(8,128)(2,1)S(1)}, bf16[256,128]{1,0:T(8,128)(2,1)}, u32[]{:S(2)}) copy-start(bf16[256,128]{1,0:T(8,128)(2,1)} %param.29) | copy-start | bytes 196612
  108.3 29.4 %copy-start.9 = (bf16[256,128]{1,0:T(8,128)(2,1)S(1)}, bf16[256,128]{1,0:T(8,128)(2,1)}, u32[]{:S(2)}) copy-start(bf16[256,128]{1,0:T(8,128)(2,1)} %param.28) | copy-start | bytes 196612
  108.6 29.2 %copy-start.10 = (f32[256]{0:T(256)S(1)}, f32[256]{0:T(256)}, u32[]{:S(2)}) copy-start(f32[256]{0:T(256)} %param.25) | copy-start | bytes 3076
  133.2 14.2 %all-to-all-start.4 = ((bf16[32,24,128]{2,1,0:T(8,128)(2,1)}), bf16[32,24,128]{2,1,0:T(8,128)(2,1)S(1)}, u32[]{:S(2)}, u32[]{:S(2)}) async-start(bf16[32,24,128]{2,1,0:T(8,128)(2,1)} %broadcast_in_dim.14), calls=%async_computation.4 | async-start | bytes 393216 | tf_op jit(solution)/shard_map/all_to_all | solution.py:31
  137.8 25.0 %copy-start.1 = (f32[12,1,128,128]{3,2,1,0:T(8,128)S(1)}, f32[12,1,128,128]{3,2,1,0:T(8,128)}, u32[]{:S(2)}) copy-start(f32[12,1,128,128]{3,2,1,0:T(8,128)} %param.20) | copy-start | bytes 2359300
  137.9 26.0 %copy-start.12 = (f32[128]{0:T(128)S(1)}, f32[128]{0:T(128)}, u32[]{:S(2)}) copy-start(f32[128]{0:T(128)} %param.31) | copy-start | bytes 1540
  137.9 6.4 %collective-permute-start.1 = (bf16[256,256]{1,0:T(8,128)(2,1)S(1)}, bf16[256,256]{1,0:T(8,128)(2,1)S(1)}, u32[]{:S(2)}, u32[]{:S(2)}) collective-permute-start(bf16[256,256]{1,0:T(8,128)(2,1)S(1)} %get-tuple-element.20), channel_id=1, source_target_pairs={{0,16},{16,0},{1,17},{17,1},{2,18},{18,2},{3,19},{19,3},{4,20},{20... | collective-permute-start | bytes 393224 | tf_op jit(solution)/shard_map/ppermute | solution.py:112
  163.5 38.4 %copy-start.2 = (bf16[256,688]{0,1:T(8,128)(2,1)S(1)}, bf16[256,688]{0,1:T(8,128)(2,1)}, u32[]{:S(2)}) copy-start(bf16[256,688]{0,1:T(8,128)(2,1)} %param.33) | copy-start | bytes 1056772
  163.5 38.4 %copy-start.3 = (bf16[256,688]{0,1:T(8,128)(2,1)S(1)}, bf16[256,688]{0,1:T(8,128)(2,1)}, u32[]{:S(2)}) copy-start(bf16[256,688]{0,1:T(8,128)(2,1)} %param.34) | copy-start | bytes 1056772
  163.5 38.4 %copy-start.11 = (f32[256]{0:T(256)S(1)}, f32[256]{0:T(256)}, u32[]{:S(2)}) copy-start(f32[256]{0:T(256)} %param.32) | copy-start | bytes 3076
  197.0 5.1 %copy-start.5 = (bf16[688,256]{1,0:T(8,128)(2,1)S(1)}, bf16[688,256]{1,0:T(8,128)(2,1)}, u32[]{:S(2)}) copy-start(bf16[688,256]{1,0:T(8,128)(2,1)} %param.35) | copy-start | bytes 1056772
  197.8 13.7 %all-to-all-start.8 = ((bf16[32,24,128]{2,1,0:T(8,128)(2,1)}), bf16[32,24,128]{2,1,0:T(8,128)(2,1)S(1)}, u32[]{:S(2)}, u32[]{:S(2)}) async-start(bf16[32,24,128]{2,1,0:T(8,128)(2,1)} %broadcast_in_dim.16), calls=%async_computation.8 | async-start | bytes 393216 | tf_op jit(solution)/shard_map/all_to_all | solution.py:31
  202.4 14.9 %collective-permute-start.2 = (bf16[3,344,256]{2,1,0:T(8,128)(2,1)S(1)}, bf16[3,344,256]{2,1,0:T(8,128)(2,1)S(1)}, u32[]{:S(2)}, u32[]{:S(2)}) collective-permute-start(bf16[3,344,256]{2,1,0:T(8,128)(2,1)S(1)} %get-tuple-element.16), channel_id=1, source_target_pairs={{0,16},{16,0},{1,17},{17,1},{2,18},{18,2},{3,19},{19,3},{4,20},{20... | collective-permute-start | bytes 1585160 | tf_op jit(solution)/shard_map/ppermute | solution.py:112
  258.1 23.4 %all-to-all-start.11 = ((bf16[32,12,256]{2,1,0:T(8,128)(2,1)}), bf16[32,12,256]{2,1,0:T(8,128)(2,1)S(1)}, u32[]{:S(2)}, u32[]{:S(2)}) async-start(bf16[32,12,256]{2,1,0:T(8,128)(2,1)} %reshape.303), calls=%async_computation.11 | async-start | bytes 524288 | tf_op jit(solution)/shard_map/all_to_all | solution.py:31

commit v5 on v4

--- a/solution.py
+++ b/solution.py
@@ -1,3 +1,5 @@
+import functools
+
 import jax
 import jax.numpy as jnp
 import numpy as np
@@ -70,21 +72,19 @@
             out_ref[r, :, i * half : (i + 1) * half] = rows[r * tall : (r + 1) * tall]
 
 
-def down_kernel(h_ref, own_ref, got_ref, out_ref, h):
+def down_kernel(h_ref, own_ref, got_ref, out_ref, h, scr):
     groups, tall, _ = h_ref.shape
     p = lax.axis_index("kvp")
     for r in range(groups):
         h[r * tall : (r + 1) * tall] = h_ref[r]
+    _, chunks, high, wide = out_ref.shape
+    across = scr.shape[1] // wide
     for place, w in ((p, own_ref), (1 - p, got_ref)):
-        value = jnp.dot(h[...], w[2], preferred_element_type=jnp.float32).astype(jnp.bfloat16)
-        if len(out_ref.shape) == 3:
-            out_ref[place] = value
-            continue
-        _, chunks, high, wide = out_ref.shape
-        across = value.shape[1] // wide
+        scr[...] = jnp.dot(h[...], w[...], preferred_element_type=jnp.float32)
         for n in range(chunks):
             r, c = divmod(n, across)
-            out_ref[place, n] = value[r * high : (r + 1) * high, c * wide : (c + 1) * wide]
+            piece = scr[r * high : (r + 1) * high, c * wide : (c + 1) * wide]
+            out_ref[place, n] = piece.astype(jnp.bfloat16)
 
 
 def heads_kernel(y_ref, own_ref, got_ref, out_ref, x, scr):
@@ -107,18 +107,54 @@
         out_ref[k, :, 128:] = piece[:, 128:lanes].astype(jnp.bfloat16)
 
 
+def retention_kernel(features, z_ref, state_ref, cos_ref, sin_ref, decay_ref, gain_ref, out_ref, k_ref, v_ref):
+    members, high, _ = z_ref.shape
+    count, width = k_ref.shape
+    left, right = (
+        sum(z_ref[n].astype(jnp.float32) for n in range(start, members, 2)) for start in range(2)
+    )
+    row = lax.broadcasted_iota(jnp.int32, (high, width), 0)
+    lane = lax.broadcasted_iota(jnp.int32, (high, width), 1)
+    line = jnp.broadcast_to(left[count : count + 1, :width], (high, width))
+    squares = jnp.sum(jnp.where((row == lane) & (row < count), line, 0.0), axis=1, keepdims=True)
+    factor = lax.rsqrt(squares / features + EPS_NORM)
+    q, k, v, o = (factor * part for part in (left[:, :width], left[:, width:], right[:, :width], right[:, width:]))
+    q, k, v, o = (part[:count] for part in (q, k, v, o))
+    cosine, sine = cos_ref[...], sin_ref[...]
+    q = q * cosine + pltpu.roll(q, width // 2, 1) * sine
+    k = (k * cosine + pltpu.roll(k, width // 2, 1) * sine) * width ** (-0.5)
+    k_ref[...] = k
+    v_ref[...] = v
+    square = jnp.concatenate([q, jnp.zeros((width - count, width), jnp.float32)], axis=0).T
+    carried = jnp.concatenate(
+        [jnp.sum(square[:, s : s + 1] * state_ref[s], axis=0, keepdims=True) for s in range(count)], axis=0
+    )
+    within = jnp.sum(q * k, axis=1, keepdims=True)
+    mixture = decay_ref[...] * carried + within * v
+    centered = mixture - jnp.mean(mixture, axis=1, keepdims=True)
+    variance = jnp.mean(centered * centered, axis=1, keepdims=True)
+    normed = centered * lax.rsqrt(variance + EPS_GROUP) * gain_ref[...]
+    value = (o / (1.0 + jnp.exp(-o)) * normed).astype(jnp.bfloat16)
+    for n in range(members):
+        out_ref[n] = value
+
+
 def swapped(both):
     p = lax.axis_index("kvp")
     return mine(both, p), lax.ppermute(mine(both, 1 - p), "kvp", [(0, 1), (1, 0)])
 
 
-def paired_weights(norm_gain, w_gate, w_up, w_down):
+def paired_weights(norm_gain, w_gate, w_up):
     width = w_gate.shape[0]
     scaled = [(w.T.astype(jnp.float32) * norm_gain).astype(jnp.bfloat16) for w in (w_gate, w_up)]
-    return swapped(jnp.stack([w.reshape(2, -1, width) for w in (*scaled, w_down)], axis=1))
-
-
-def feed_forward(gathered, weights, flat):
+    return swapped(jnp.stack([w.reshape(2, -1, width) for w in scaled], axis=1))
+
+
+def paired_rows(w_down):
+    return swapped(w_down.reshape(2, -1, w_down.shape[1]))
+
+
+def feed_forward(gathered, weights, back_weights, flat):
     own_w, got_w = weights
     members, tp = lax.axis_size("kvh"), lax.axis_size("tp")
     wide, part = own_w.shape[2], own_w.shape[1]
@@ -137,15 +173,15 @@
     features = wide * lax.axis_size(KV)
     factor = lax.rsqrt(total[:, part : part + 1] / features + EPS_NORM)
     hidden = jax.nn.silu(factor * total[:, :part]) * (factor * total[:, half : half + part])
-    everyone = spread(hidden.astype(jnp.bfloat16), "kvh")
-    shape = (2, rows, wide) if flat else (2, tp, tall, rows * wide // (tp * tall))
+    hidden, back_weights = lax.optimization_barrier((hidden.astype(jnp.bfloat16), back_weights))
+    everyone = spread(hidden, "kvh")
+    shape = (2, tp, rows // tp, wide) if flat else (2, tp, tall, rows * wide // (tp * tall))
     return local_call(
         down_kernel,
         jax.ShapeDtypeStruct(shape, jnp.bfloat16),
         everyone,
-        own_w,
-        got_w,
-        scratch=(pltpu.VMEM((rows, part), jnp.bfloat16),),
+        *back_weights,
+        scratch=(pltpu.VMEM((rows, part), jnp.bfloat16), pltpu.VMEM((rows, wide), jnp.float32)),
         flops=4 * rows * part * wide,
     )
 
@@ -155,15 +191,9 @@
     return (own.astype(jnp.float32) + branch * share).astype(jnp.bfloat16)
 
 
-def rotate(values_in, cosine, sine):
-    half = values_in.shape[-1] // 2
-    low, high = values_in[..., :half], values_in[..., half:]
-    return jnp.concatenate([low * cosine - high * sine, low * sine + high * cosine], axis=-1)
-
-
 def retention(gathered, weights, features, head_gain, state, tables):
-    cosine, sine, decays = tables
-    count, heads, width, _ = state.shape
+    cosine, sine, decay = tables
+    count, _, width, _ = state.shape
     members = lax.axis_size(KV)
     block, lanes = weights[0].shape
     rows = members * count
@@ -179,24 +209,24 @@
         ),
         flops=4 * rows * block * lanes,
     )
-    total = exchange(sent, KV).reshape(members // 2, 2, high, lanes).astype(jnp.float32).sum(axis=0)
-    factor = lax.rsqrt(total[0, count, :count] / features + EPS_NORM)[:, None]
-    total = factor * total[:, :count]
-    wide = heads * width
-    q, k, v, o = (
-        total[i // 2, :, i % 2 * wide : (i % 2 + 1) * wide].reshape(count, heads, width) for i in range(4)
-    )
-    q = rotate(q, cosine, sine)
-    k = rotate(k, cosine, sine) * width ** (-0.5)
-    carried = jnp.einsum("shd,shde->she", q, state, precision=lax.Precision.HIGHEST)
-    within = jnp.sum(q * k, axis=-1, keepdims=True)
-    mixture = decays[None, :, None] * carried + within * v
-    centered = mixture - jnp.mean(mixture, axis=-1, keepdims=True)
-    variance = jnp.mean(centered * centered, axis=-1, keepdims=True)
-    normed = centered * lax.rsqrt(variance + EPS_GROUP) * head_gain.reshape(heads, width)
-    ret_out = (jax.nn.silu(o) * normed).astype(jnp.bfloat16).reshape(count, heads * width)
-    new_state = decays[None, :, None, None] * state + k[..., :, None] * v[..., None, :]
-    return spread(ret_out, KV).reshape(rows, heads * width), new_state
+    received = exchange(sent, KV)
+    ret_out, k, v = local_call(
+        functools.partial(retention_kernel, features),
+        (
+            jax.ShapeDtypeStruct((members, count, width), jnp.bfloat16),
+            jax.ShapeDtypeStruct((count, width), jnp.float32),
+            jax.ShapeDtypeStruct((count, width), jnp.float32),
+        ),
+        received,
+        state.reshape(count, width, width),
+        cosine,
+        sine,
+        decay,
+        head_gain.reshape(1, width),
+        flops=4 * count * width * width,
+    )
+    new_state = decay[:, :, None] * state.reshape(count, width, width) + k[:, :, None] * v[:, None, :]
+    return exchange(ret_out, KV).reshape(rows, width), new_state.reshape(state.shape)
 
 
 def per_device(
@@ -231,34 +261,36 @@
     half = ret_state.shape[-1] // 2
     inverse = 10000.0 ** (-jnp.arange(half, dtype=jnp.float32) / half)
     angles = positions.astype(jnp.float32)[:, None] * inverse[None, :]
-    cosine, sine = jnp.cos(angles)[:, None, :], jnp.sin(angles)[:, None, :]
-    heads = ret_state.shape[1]
-    head_ids = (t * heads + jnp.arange(heads)).astype(jnp.float32)
-    decays = jnp.exp(jnp.log1p(-(2.0 ** (-5.0 - head_ids))))
-    tables = (cosine, sine, decays)
-
-    first_pair = paired_weights(first_gain, first_gate, first_up, first_down)
-    second_pair = paired_weights(second_gain, second_gate, second_up, second_down)
+    cosine, sine = jnp.cos(angles), jnp.sin(angles)
+    cosine, sine = jnp.concatenate([cosine, cosine], axis=1), jnp.concatenate([-sine, sine], axis=1)
+    decay = jnp.exp(jnp.log1p(-(2.0 ** (-5.0 - t.astype(jnp.float32))))) * jnp.ones((1, 2 * half), jnp.float32)
+    place = lax.div(t * few, tall)
+    ready = (cosine, sine, decay, place, t * few - place * tall)
+
+    first_pair = paired_weights(first_gain, first_gate, first_up)
+    first_back = paired_rows(first_down)
+    second_pair = paired_weights(second_gain, second_gate, second_up)
+    second_back = paired_rows(second_down)
     halves = [jnp.concatenate(w, axis=1) for w in ((w_query, w_key), (w_value, w_outgate))]
     halves = jnp.stack(halves).astype(jnp.float32) * mix_gain[:, None]
     heads_pair = swapped(halves.astype(jnp.bfloat16))
 
     gathered = spread(stream_in, BOTH).reshape(2, rows, block)
     own = lax.dynamic_slice(gathered, (p, r * tall, c * wide), (1, tall, wide))[0]
-    gathered, own, tables = lax.optimization_barrier((gathered, own, tables))
-    back = feed_forward(gathered, first_pair, False)
+    gathered, own, ready = lax.optimization_barrier((gathered, own, ready))
+    cosine, sine, decay, place, offset = ready
+    back = feed_forward(gathered, first_pair, first_back, False)
     own = advance(own, back.reshape(2 * tp, tall, wide), 0.5, BOTH)
     gathered = spread(own, BOTH).reshape(2, tp, tall, wide)
-    ret_out, new_state = retention(gathered, heads_pair, features, head_gain, ret_state, tables)
+    ret_out, new_state = retention(gathered, heads_pair, features, head_gain, ret_state, (cosine, sine, decay))
     back = jnp.dot(ret_out, w_out, preferred_element_type=jnp.float32).astype(jnp.bfloat16)
     back = back.reshape(groups, tall, across, wide).transpose(0, 2, 1, 3).reshape(tp, tall, wide)
     own = advance(own, back, 1.0, "tp")
     gathered = spread(own, BOTH).reshape(2, tp, tall, wide)
-    place = lax.div(t * few, tall)
-    own = lax.dynamic_slice(gathered, (p, place * across, t * few - place * tall, 0), (1, across, few, wide))[0]
+    own = lax.dynamic_slice(gathered, (p, place * across, offset, 0), (1, across, few, wide))[0]
     own = jnp.concatenate([own[i] for i in range(across)], axis=1)
     gathered, own = lax.optimization_barrier((gathered, own))
-    back = feed_forward(gathered, second_pair, True)
+    back = feed_forward(gathered, second_pair, second_back, True)
     return advance(own, back.reshape(2 * tp, few, block), 0.5, BOTH), new_state
 
 

time: 283 us -> 286 us (1.011)
  blocking collectives: 154 us -> 117 us
  waiting for transfers between devices: 38.3 us -> 57.6 us
  starting transfers between devices: 76.4 us -> 94.8 us
  Pallas kernels: 1.63 us -> 4.54 us
    all_to_all x8 -> x6, blocking collectives: 154 us -> 117 us  [exchange(): return lax.all_to_all(x, axis, split_axis=0, concat_axis=0, tiled=True)]
    all_to_all x4 -> x6, waiting for transfers between devices: 24.1 us -> 50 us  [exchange(): return lax.all_to_all(x, axis, split_axis=0, concat_axis=0, tiled=True)]
    all_to_all x4 -> x6, starting transfers between devices: 66.4 us -> 77.8 us  [exchange(): return lax.all_to_all(x, axis, split_axis=0, concat_axis=0, tiled=True)]
    ppermute x3 -> x5, starting transfers between devices: 10 us -> 16.9 us  [swapped(): lax.ppermute(mine(both, 1 - p), 'kvp', [(0, 1), (1, 0)])]
    ppermute x3 -> x5, waiting for transfers between devices: 14.1 us -> 7.6 us  [swapped(): lax.ppermute(mine(both, 1 - p), 'kvp', [(0, 1), (1, 0)])]
    pallas_call x5 -> x6, Pallas kernels: 1.63 us -> 4.54 us  [local_call(): pl.pallas_call(kernel, out_shape=out_shape, in_specs=[VMEM] * len(args),...]
  transfers between devices with their start and end apart: 7 -> 11, of which waited for: 7 -> 11; matrix products, arithmetic and copies ran while one was open for 1% -> 1% of each run, Pallas kernels for 0% -> 0%
where the time goes in v5:
time: 286 us; the launch traced here: 285 us
  blocking collectives  117 us (41%)
  starting transfers between devices  94.8 us (33%)
  waiting for transfers between devices  57.6 us (20%)
  local copies, waits for them, and re-layouts  5.89 us (2%)
  Pallas kernels  4.54 us (2%)
  other arithmetic  3.42 us (1%)
    all_to_all x6, blocking collectives, exchange(): return lax.all_to_all(x, axis, split_axis=0, concat_axis=0, tiled=True)  117 us
    all_to_all x6, starting transfers between devices, exchange(): return lax.all_to_all(x, axis, split_axis=0, concat_axis=0, tiled=True)  77.8 us
    all_to_all x6, waiting for transfers between devices, exchange(): return lax.all_to_all(x, axis, split_axis=0, concat_axis=0, tiled=True)  50 us
    ppermute x5, starting transfers between devices, swapped(): lax.ppermute(mine(both, 1 - p), 'kvp', [(0, 1), (1, 0)])  16.9 us
    ppermute x5, waiting for transfers between devices, swapped(): lax.ppermute(mine(both, 1 - p), 'kvp', [(0, 1), (1, 0)])  7.6 us
  transfers between devices with their start and end apart: 11, of which 11 were waited for; matrix products, arithmetic and copies ran while one was open for 1% of the time, Pallas kernels for 0%

profile of v5, /device:TPU:65, one launch (start us, length us, event | category | flops | bytes accessed | tf_op | source)
XLA Modules:
  0.0 285.0 jit_solution(14858895359458352770)
XLA Ops:
  2.2 45.2 %all-to-all-start = ((bf16[32,12,256]{2,1,0:T(8,128)(2,1)}), bf16[32,12,256]{2,1,0:T(8,128)(2,1)S(1)}, u32[]{:S(2)}, u32[]{:S(2)}) async-start(bf16[32,12,256]{2,1,0:T(8,128)(2,1)} %broadcast_in_dim.10), calls=%async_computation | async-start | bytes 524288 | tf_op jit(solution)/shard_map/all_to_all | solution.py:33
  48.3 3.6 %collective-permute-start = (bf16[2,344,256]{2,1,0:T(8,128)(2,1)S(1)}, bf16[2,344,256]{2,1,0:T(8,128)(2,1)S(1)}, u32[]{:S(2)}, u32[]{:S(2)}) collective-permute-start(bf16[2,344,256]{2,1,0:T(8,128)(2,1)S(1)} %get-tuple-element.40), channel_id=1, source_target_pairs={{0,16},{16,0},{1,17},{17,1},{2,18},{18,2},{3,19},{19,3},{4,20},{20... | collective-permute-start | bytes 1056776 | tf_op jit(solution)/shard_map/ppermute | solution.py:144
  52.9 5.4 %all-to-all-done = bf16[32,12,256]{2,1,0:T(8,128)(2,1)S(1)} async-done(((bf16[32,12,256]{2,1,0:T(8,128)(2,1)}), bf16[32,12,256]{2,1,0:T(8,128)(2,1)S(1)}, u32[]{:S(2)}, u32[]{:S(2)}) %all-to-all-start) | async-done | bytes 196640 | tf_op jit(solution)/shard_map/all_to_all | solution.py:33
  60.5 8.0 %all-to-all-start.1 = ((bf16[8,24,768]{2,1,0:T(8,128)(2,1)}), bf16[8,24,768]{2,1,0:T(8,128)(2,1)S(1)}, u32[]{:S(2)}, u32[]{:S(2)}) async-start(bf16[8,24,768]{2,1,0:T(8,128)(2,1)} %shard_map.185), calls=%async_computation.1 | async-start | bytes 589824 | tf_op jit(solution)/shard_map/all_to_all | solution.py:33
  68.6 3.6 %collective-permute-start.1 = (bf16[344,256]{1,0:T(8,128)(2,1)S(1)}, bf16[344,256]{1,0:T(8,128)(2,1)S(1)}, u32[]{:S(2)}, u32[]{:S(2)}) collective-permute-start(bf16[344,256]{1,0:T(8,128)(2,1)S(1)} %get-tuple-element.44), channel_id=1, source_target_pairs={{0,16},{16,0},{1,17},{17,1},{2,18},{18,2},{3,19},{19,3},{4,20},{20... | collective-permute-start | bytes 528392 | tf_op jit(solution)/shard_map/ppermute | solution.py:144
  72.1 13.4 %all-to-all-done.1 = bf16[8,24,768]{2,1,0:T(8,128)(2,1)S(1)} async-done(((bf16[8,24,768]{2,1,0:T(8,128)(2,1)}), bf16[8,24,768]{2,1,0:T(8,128)(2,1)S(1)}, u32[]{:S(2)}, u32[]{:S(2)}) %all-to-all-start.1) | async-done | bytes 294944 | tf_op jit(solution)/shard_map/all_to_all | solution.py:33
  86.7 23.8 %all_to_all.60.h_ref = bf16[8,24,344]{2,1,0:T(8,128)(2,1)S(1)} all-to-all(bf16[8,24,344]{2,1,0:T(8,128)(2,1)S(1)} %broadcast_in_dim.11), channel_id=1, replica_groups=mesh['grp'=2,'kvh'=8,'kvp'=2,'tp'=16] {'kvh'}, dimensions={0} | all-to-all | bytes 264192 | tf_op jit(solution)/shard_map/all_to_all | solution.py:33
  110.8 21.8 %all_to_all.61 = bf16[32,24,128]{2,1,0:T(8,128)(2,1)S(1)} all-to-all(bf16[32,24,128]{2,1,0:T(8,128)(2,1)S(1)} %bitcast.68), channel_id=1, replica_groups=mesh['grp'=2,'kvh'=8,'kvp'=2,'tp'=16] {'kvp','tp'}, dimensions={0} | all-to-all | bytes 393216 | tf_op jit(solution)/shard_map/all_to_all | solution.py:33
  133.4 4.6 %all-to-all-start.4 = ((bf16[32,24,128]{2,1,0:T(8,128)(2,1)}), bf16[32,24,128]{2,1,0:T(8,128)(2,1)S(1)}, u32[]{:S(2)}, u32[]{:S(2)}) async-start(bf16[32,24,128]{2,1,0:T(8,128)(2,1)} %broadcast_in_dim.12), calls=%async_computation.4 | async-start | bytes 393216 | tf_op jit(solution)/shard_map/all_to_all | solution.py:33
  138.8 3.4 %collective-permute-start.2 = (bf16[256,256]{1,0:T(8,128)(2,1)S(1)}, bf16[256,256]{1,0:T(8,128)(2,1)S(1)}, u32[]{:S(2)}, u32[]{:S(2)}) collective-permute-start(bf16[256,256]{1,0:T(8,128)(2,1)S(1)} %get-tuple-element.46), channel_id=1, source_target_pairs={{0,16},{16,0},{1,17},{17,1},{2,18},{18,2},{3,19},{19,3},{4,20},{20... | collective-permute-start | bytes 393224 | tf_op jit(solution)/shard_map/ppermute | solution.py:144
  142.3 3.0 %collective-permute-done.2.got_ref = bf16[256,256]{1,0:T(8,128)(2,1)S(1)} collective-permute-done((bf16[256,256]{1,0:T(8,128)(2,1)S(1)}, bf16[256,256]{1,0:T(8,128)(2,1)S(1)}, u32[]{:S(2)}, u32[]{:S(2)}) %collective-permute-start.2) | collective-permute-done | bytes 131104 | tf_op jit(solution)/shard_map/ppermute | solution.py:144
  145.3 2.4 all-to-all-done.4
  147.9 14.8 %all_to_all.62.z_ref = bf16[16,16,256]{2,1,0:T(8,128)(2,1)S(1)} all-to-all(bf16[16,16,256]{2,1,0:T(8,128)(2,1)S(1)} %shard_map.187), channel_id=1, replica_groups=mesh['grp'=2,'kvh'=8,'kvp'=2,'tp'=16] {'kvh','kvp'}, dimensions={0} | all-to-all | bytes 262144 | tf_op jit(solution)/shard_map/all_to_all | solution.py:33
  164.1 17.7 %all_to_all.63 = bf16[16,12,128]{2,1,0:T(8,128)(2,1)S(1)} all-to-all(bf16[16,12,128]{2,1,0:T(8,128)(2,1)S(1)} %get-tuple-element.28), channel_id=1, replica_groups=mesh['grp'=2,'kvh'=8,'kvp'=2,'tp'=16] {'kvh','kvp'}, dimensions={0} | all-to-all | bytes 98304 | tf_op jit(solution)/shard_map/all_to_all | solution.py:33
  182.0 15.4 %all_to_all.64 = bf16[16,24,128]{2,1,0:T(8,128)(2,1)S(1)} all-to-all(bf16[16,24,128]{2,1,0:T(8,128)(2,1)S(1)} %bitcast.75), channel_id=1, replica_groups=mesh['grp'=2,'kvh'=8,'kvp'=2,'tp'=16] {'tp'}, dimensions={0} | all-to-all | bytes 196608 | tf_op jit(solution)/shard_map/all_to_all | solution.py:33
  198.2 4.3 %all-to-all-start.8 = ((bf16[32,24,128]{2,1,0:T(8,128)(2,1)}), bf16[32,24,128]{2,1,0:T(8,128)(2,1)S(1)}, u32[]{:S(2)}, u32[]{:S(2)}) async-start(bf16[32,24,128]{2,1,0:T(8,128)(2,1)} %broadcast_in_dim.13), calls=%async_computation.8 | async-start | bytes 393216 | tf_op jit(solution)/shard_map/all_to_all | solution.py:33
  202.8 3.1 %collective-permute-start.3 = (bf16[2,344,256]{2,1,0:T(8,128)(2,1)S(1)}, bf16[2,344,256]{2,1,0:T(8,128)(2,1)S(1)}, u32[]{:S(2)}, u32[]{:S(2)}) collective-permute-start(bf16[2,344,256]{2,1,0:T(8,128)(2,1)S(1)} %get-tuple-element.38), channel_id=1, source_target_pairs={{0,16},{16,0},{1,17},{17,1},{2,18},{18,2},{3,19},{19,3},{4,20},{20... | collective-permute-start | bytes 1056776 | tf_op jit(solution)/shard_map/ppermute | solution.py:144
  206.0 6.1 %all-to-all-done.8 = bf16[32,24,128]{2,1,0:T(8,128)(2,1)S(1)} async-done(((bf16[32,24,128]{2,1,0:T(8,128)(2,1)}), bf16[32,24,128]{2,1,0:T(8,128)(2,1)S(1)}, u32[]{:S(2)}, u32[]{:S(2)}) %all-to-all-start.8) | async-done | bytes 196640 | tf_op jit(solution)/shard_map/all_to_all | solution.py:33
  215.2 3.8 %all-to-all-start.9 = ((bf16[8,24,768]{2,1,0:T(8,128)(2,1)}), bf16[8,24,768]{2,1,0:T(8,128)(2,1)S(1)}, u32[]{:S(2)}, u32[]{:S(2)}) async-start(bf16[8,24,768]{2,1,0:T(8,128)(2,1)} %shard_map.189), calls=%async_computation.9 | async-start | bytes 589824 | tf_op jit(solution)/shard_map/all_to_all | solution.py:33
  219.0 3.3 %collective-permute-start.4 = (bf16[344,256]{1,0:T(8,128)(2,1)S(1)}, bf16[344,256]{1,0:T(8,128)(2,1)S(1)}, u32[]{:S(2)}, u32[]{:S(2)}) collective-permute-start(bf16[344,256]{1,0:T(8,128)(2,1)S(1)} %get-tuple-element.42), channel_id=1, source_target_pairs={{0,16},{16,0},{1,17},{17,1},{2,18},{18,2},{3,19},{19,3},{4,20},{20... | collective-permute-start | bytes 528392 | tf_op jit(solution)/shard_map/ppermute | solution.py:144
  222.3 13.0 %all-to-all-done.9 = bf16[8,24,768]{2,1,0:T(8,128)(2,1)S(1)} async-done(((bf16[8,24,768]{2,1,0:T(8,128)(2,1)}), bf16[8,24,768]{2,1,0:T(8,128)(2,1)S(1)}, u32[]{:S(2)}, u32[]{:S(2)}) %all-to-all-start.9) | async-done | bytes 294944 | tf_op jit(solution)/shard_map/all_to_all | solution.py:33
  236.6 24.0 %all_to_all.65.h_ref = bf16[8,24,344]{2,1,0:T(8,128)(2,1)S(1)} all-to-all(bf16[8,24,344]{2,1,0:T(8,128)(2,1)S(1)} %broadcast_in_dim.14), channel_id=1, replica_groups=mesh['grp'=2,'kvh'=8,'kvp'=2,'tp'=16] {'kvh'}, dimensions={0} | all-to-all | bytes 264192 | tf_op jit(solution)/shard_map/all_to_all | solution.py:33
  261.6 12.0 %all-to-all-start.11 = ((bf16[32,12,256]{2,1,0:T(8,128)(2,1)}), bf16[32,12,256]{2,1,0:T(8,128)(2,1)S(1)}, u32[]{:S(2)}, u32[]{:S(2)}) async-start(bf16[32,12,256]{2,1,0:T(8,128)(2,1)} %bitcast.36), calls=%async_computation.11 | async-start | bytes 524288 | tf_op jit(solution)/shard_map/all_to_all | solution.py:33
  274.7 9.6 %all-to-all-done.11 = bf16[32,12,256]{2,1,0:T(8,128)(2,1)S(1)} async-done(((bf16[32,12,256]{2,1,0:T(8,128)(2,1)}), bf16[32,12,256]{2,1,0:T(8,128)(2,1)S(1)}, u32[]{:S(2)}, u32[]{:S(2)}) %all-to-all-start.11) | async-done | bytes 196640 | tf_op jit(solution)/shard_map/all_to_all | solution.py:33
  (84 shorter events, 18.6 us)
Async XLA Ops:
  0.6 181.2 %copy-start = (bf16[128,256]{1,0:T(8,128)(2,1)S(1)}, bf16[128,256]{1,0:T(8,128)(2,1)}, u32[]{:S(2)}) copy-start(bf16[128,256]{1,0:T(8,128)(2,1)} %param.30) | copy-start | bytes 196612
  0.6 46.7 %copy-start.3 = (bf16[256,688]{0,1:T(8,128)(2,1)S(1)}, bf16[256,688]{0,1:T(8,128)(2,1)}, u32[]{:S(2)}) copy-start(bf16[256,688]{0,1:T(8,128)(2,1)} %param.23) | copy-start | bytes 1056772
  0.7 46.7 %copy-start.4 = (bf16[256,688]{0,1:T(8,128)(2,1)S(1)}, bf16[256,688]{0,1:T(8,128)(2,1)}, u32[]{:S(2)}) copy-start(bf16[256,688]{0,1:T(8,128)(2,1)} %param.22) | copy-start | bytes 1056772
  2.2 56.1 %all-to-all-start = ((bf16[32,12,256]{2,1,0:T(8,128)(2,1)}), bf16[32,12,256]{2,1,0:T(8,128)(2,1)S(1)}, u32[]{:S(2)}, u32[]{:S(2)}) async-start(bf16[32,12,256]{2,1,0:T(8,128)(2,1)} %broadcast_in_dim.10), calls=%async_computation | async-start | bytes 524288 | tf_op jit(solution)/shard_map/all_to_all | solution.py:33
  48.3 11.1 %collective-permute-start = (bf16[2,344,256]{2,1,0:T(8,128)(2,1)S(1)}, bf16[2,344,256]{2,1,0:T(8,128)(2,1)S(1)}, u32[]{:S(2)}, u32[]{:S(2)}) collective-permute-start(bf16[2,344,256]{2,1,0:T(8,128)(2,1)S(1)} %get-tuple-element.40), channel_id=1, source_target_pairs={{0,16},{16,0},{1,17},{17,1},{2,18},{18,2},{3,19},{19,3},{4,20},{20... | collective-permute-start | bytes 1056776 | tf_op jit(solution)/shard_map/ppermute | solution.py:144
  60.5 8.0 %copy-start.7 = (bf16[688,256]{1,0:T(8,128)(2,1)S(1)}, bf16[688,256]{1,0:T(8,128)(2,1)}, u32[]{:S(2)}) copy-start(bf16[688,256]{1,0:T(8,128)(2,1)} %param.24) | copy-start | bytes 1056772
  60.5 25.0 %all-to-all-start.1 = ((bf16[8,24,768]{2,1,0:T(8,128)(2,1)}), bf16[8,24,768]{2,1,0:T(8,128)(2,1)S(1)}, u32[]{:S(2)}, u32[]{:S(2)}) async-start(bf16[8,24,768]{2,1,0:T(8,128)(2,1)} %shard_map.185), calls=%async_computation.1 | async-start | bytes 589824 | tf_op jit(solution)/shard_map/all_to_all | solution.py:33
  68.6 18.1 %collective-permute-start.1 = (bf16[344,256]{1,0:T(8,128)(2,1)S(1)}, bf16[344,256]{1,0:T(8,128)(2,1)S(1)}, u32[]{:S(2)}, u32[]{:S(2)}) collective-permute-start(bf16[344,256]{1,0:T(8,128)(2,1)S(1)} %get-tuple-element.44), channel_id=1, source_target_pairs={{0,16},{16,0},{1,17},{17,1},{2,18},{18,2},{3,19},{19,3},{4,20},{20... | collective-permute-start | bytes 528392 | tf_op jit(solution)/shard_map/ppermute | solution.py:144
  133.3 4.6 %copy-start.9 = (bf16[256,128]{1,0:T(8,128)(2,1)S(1)}, bf16[256,128]{1,0:T(8,128)(2,1)}, u32[]{:S(2)}) copy-start(bf16[256,128]{1,0:T(8,128)(2,1)} %param.27) | copy-start | bytes 196612
  133.3 4.6 %copy-start.10 = (bf16[256,128]{1,0:T(8,128)(2,1)S(1)}, bf16[256,128]{1,0:T(8,128)(2,1)}, u32[]{:S(2)}) copy-start(bf16[256,128]{1,0:T(8,128)(2,1)} %param.26) | copy-start | bytes 196612
  133.3 4.6 %copy-start.11 = (bf16[256,128]{1,0:T(8,128)(2,1)S(1)}, bf16[256,128]{1,0:T(8,128)(2,1)}, u32[]{:S(2)}) copy-start(bf16[256,128]{1,0:T(8,128)(2,1)} %param.29) | copy-start | bytes 196612
  133.3 4.6 %copy-start.12 = (bf16[256,128]{1,0:T(8,128)(2,1)S(1)}, bf16[256,128]{1,0:T(8,128)(2,1)}, u32[]{:S(2)}) copy-start(bf16[256,128]{1,0:T(8,128)(2,1)} %param.28) | copy-start | bytes 196612
  133.4 14.3 %all-to-all-start.4 = ((bf16[32,24,128]{2,1,0:T(8,128)(2,1)}), bf16[32,24,128]{2,1,0:T(8,128)(2,1)S(1)}, u32[]{:S(2)}, u32[]{:S(2)}) async-start(bf16[32,24,128]{2,1,0:T(8,128)(2,1)} %broadcast_in_dim.12), calls=%async_computation.4 | async-start | bytes 393216 | tf_op jit(solution)/shard_map/all_to_all | solution.py:33
  138.8 23.9 %copy-start.1 = (f32[12,1,128,128]{3,2,1,0:T(8,128)S(1)}, f32[12,1,128,128]{3,2,1,0:T(8,128)}, u32[]{:S(2)}) copy-start(f32[12,1,128,128]{3,2,1,0:T(8,128)} %param.20) | copy-start | bytes 2359300
  138.8 6.4 %collective-permute-start.2 = (bf16[256,256]{1,0:T(8,128)(2,1)S(1)}, bf16[256,256]{1,0:T(8,128)(2,1)S(1)}, u32[]{:S(2)}, u32[]{:S(2)}) collective-permute-start(bf16[256,256]{1,0:T(8,128)(2,1)S(1)} %get-tuple-element.46), channel_id=1, source_target_pairs={{0,16},{16,0},{1,17},{17,1},{2,18},{18,2},{3,19},{19,3},{4,20},{20... | collective-permute-start | bytes 393224 | tf_op jit(solution)/shard_map/ppermute | solution.py:144
  197.5 5.1 %copy-start.5 = (bf16[256,688]{0,1:T(8,128)(2,1)S(1)}, bf16[256,688]{0,1:T(8,128)(2,1)}, u32[]{:S(2)}) copy-start(bf16[256,688]{0,1:T(8,128)(2,1)} %param.34) | copy-start | bytes 1056772
  197.5 5.1 %copy-start.6 = (bf16[256,688]{0,1:T(8,128)(2,1)S(1)}, bf16[256,688]{0,1:T(8,128)(2,1)}, u32[]{:S(2)}) copy-start(bf16[256,688]{0,1:T(8,128)(2,1)} %param.33) | copy-start | bytes 1056772
  198.2 4.3 %copy-start.15 = (f32[256]{0:T(256)S(1)}, f32[256]{0:T(256)}, u32[]{:S(2)}) copy-start(f32[256]{0:T(256)} %param.32) | copy-start | bytes 3076
  198.2 13.9 %all-to-all-start.8 = ((bf16[32,24,128]{2,1,0:T(8,128)(2,1)}), bf16[32,24,128]{2,1,0:T(8,128)(2,1)S(1)}, u32[]{:S(2)}, u32[]{:S(2)}) async-start(bf16[32,24,128]{2,1,0:T(8,128)(2,1)} %broadcast_in_dim.13), calls=%async_computation.8 | async-start | bytes 393216 | tf_op jit(solution)/shard_map/all_to_all | solution.py:33
  202.8 11.2 %collective-permute-start.3 = (bf16[2,344,256]{2,1,0:T(8,128)(2,1)S(1)}, bf16[2,344,256]{2,1,0:T(8,128)(2,1)S(1)}, u32[]{:S(2)}, u32[]{:S(2)}) collective-permute-start(bf16[2,344,256]{2,1,0:T(8,128)(2,1)S(1)} %get-tuple-element.38), channel_id=1, source_target_pairs={{0,16},{16,0},{1,17},{17,1},{2,18},{18,2},{3,19},{19,3},{4,20},{20... | collective-permute-start | bytes 1056776 | tf_op jit(solution)/shard_map/ppermute | solution.py:144
  215.2 3.8 %copy-start.8 = (bf16[688,256]{1,0:T(8,128)(2,1)S(1)}, bf16[688,256]{1,0:T(8,128)(2,1)}, u32[]{:S(2)}) copy-start(bf16[688,256]{1,0:T(8,128)(2,1)} %param.35) | copy-start | bytes 1056772
  215.2 20.1 %all-to-all-start.9 = ((bf16[8,24,768]{2,1,0:T(8,128)(2,1)}), bf16[8,24,768]{2,1,0:T(8,128)(2,1)S(1)}, u32[]{:S(2)}, u32[]{:S(2)}) async-start(bf16[8,24,768]{2,1,0:T(8,128)(2,1)} %shard_map.189), calls=%async_computation.9 | async-start | bytes 589824 | tf_op jit(solution)/shard_map/all_to_all | solution.py:33
  219.0 17.6 %collective-permute-start.4 = (bf16[344,256]{1,0:T(8,128)(2,1)S(1)}, bf16[344,256]{1,0:T(8,128)(2,1)S(1)}, u32[]{:S(2)}, u32[]{:S(2)}) collective-permute-start(bf16[344,256]{1,0:T(8,128)(2,1)S(1)} %get-tuple-element.42), channel_id=1, source_target_pairs={{0,16},{16,0},{1,17},{17,1},{2,18},{18,2},{3,19},{19,3},{4,20},{20... | collective-permute-start | bytes 528392 | tf_op jit(solution)/shard_map/ppermute | solution.py:144
  261.6 22.8 %all-to-all-start.11 = ((bf16[32,12,256]{2,1,0:T(8,128)(2,1)}), bf16[32,12,256]{2,1,0:T(8,128)(2,1)S(1)}, u32[]{:S(2)}, u32[]{:S(2)}) async-start(bf16[32,12,256]{2,1,0:T(8,128)(2,1)} %bitcast.36), calls=%async_computation.11 | async-start | bytes 524288 | tf_op jit(solution)/shard_map/all_to_all | solution.py:33
  (4 other events, 2.7 us)

commit v6 on v5

--- a/solution.py
+++ b/solution.py
@@ -87,6 +87,23 @@
             out_ref[place, n] = piece.astype(jnp.bfloat16)
 
 
+def whole_down_kernel(h_ref, w_ref, out_ref, h, scr):
+    groups, tall, part = h_ref.shape
+    cuts = w_ref.shape[0] // part
+    for c in range(cuts):
+        for r in range(groups // cuts):
+            h[c, r * tall : (r + 1) * tall] = h_ref[r * cuts + c]
+    scr[...] = sum(
+        jnp.dot(h[c], w_ref[c * part : (c + 1) * part], preferred_element_type=jnp.float32) for c in range(cuts)
+    )
+    chunks, high, wide = out_ref.shape
+    across = scr.shape[1] // wide
+    for n in range(chunks):
+        r, c = divmod(n, across)
+        piece = scr[r * high : (r + 1) * high, c * wide : (c + 1) * wide]
+        out_ref[n] = piece.astype(jnp.bfloat16)
+
+
 def heads_kernel(y_ref, own_ref, got_ref, out_ref, x, scr):
     fill_rows(x, y_ref, lax.axis_index("kvp"))
     members, high, lanes = out_ref.shape
@@ -173,15 +190,26 @@
     features = wide * lax.axis_size(KV)
     factor = lax.rsqrt(total[:, part : part + 1] / features + EPS_NORM)
     hidden = jax.nn.silu(factor * total[:, :part]) * (factor * total[:, half : half + part])
-    hidden, back_weights = lax.optimization_barrier((hidden.astype(jnp.bfloat16), back_weights))
+    hidden = hidden.astype(jnp.bfloat16)
+    scratch = (pltpu.VMEM((rows, part), jnp.bfloat16), pltpu.VMEM((rows, wide), jnp.float32))
+    if not flat:
+        everyone = spread(hidden, KV)
+        return local_call(
+            whole_down_kernel,
+            jax.ShapeDtypeStruct((tp, tall, rows * wide // (tp * tall)), jnp.bfloat16),
+            everyone,
+            back_weights,
+            scratch=(pltpu.VMEM((2, rows, part), jnp.bfloat16), scratch[1]),
+            flops=4 * rows * part * wide,
+        )
+    hidden, back_weights = lax.optimization_barrier((hidden, back_weights))
     everyone = spread(hidden, "kvh")
-    shape = (2, tp, rows // tp, wide) if flat else (2, tp, tall, rows * wide // (tp * tall))
     return local_call(
         down_kernel,
-        jax.ShapeDtypeStruct(shape, jnp.bfloat16),
+        jax.ShapeDtypeStruct((2, tp, rows // tp, wide), jnp.bfloat16),
         everyone,
         *back_weights,
-        scratch=(pltpu.VMEM((rows, part), jnp.bfloat16), pltpu.VMEM((rows, wide), jnp.float32)),
+        scratch=scratch,
         flops=4 * rows * part * wide,
     )
 
@@ -268,7 +296,6 @@
     ready = (cosine, sine, decay, place, t * few - place * tall)
 
     first_pair = paired_weights(first_gain, first_gate, first_up)
-    first_back = paired_rows(first_down)
     second_pair = paired_weights(second_gain, second_gate, second_up)
     second_back = paired_rows(second_down)
     halves = [jnp.concatenate(w, axis=1) for w in ((w_query, w_key), (w_value, w_outgate))]
@@ -279,8 +306,8 @@
     own = lax.dynamic_slice(gathered, (p, r * tall, c * wide), (1, tall, wide))[0]
     gathered, own, ready = lax.optimization_barrier((gathered, own, ready))
     cosine, sine, decay, place, offset = ready
-    back = feed_forward(gathered, first_pair, first_back, False)
-    own = advance(own, back.reshape(2 * tp, tall, wide), 0.5, BOTH)
+    back = feed_forward(gathered, first_pair, first_down, False)
+    own = advance(own, back, 0.5, "tp")
     gathered = spread(own, BOTH).reshape(2, tp, tall, wide)
     ret_out, new_state = retention(gathered, heads_pair, features, head_gain, ret_state, (cosine, sine, decay))
     back = jnp.dot(ret_out, w_out, preferred_element_type=jnp.float32).astype(jnp.bfloat16)

time: 286 us -> 286 us (level)
  blocking collectives: 117 us -> 144 us
  waiting for transfers between devices: 57.6 us -> 43.2 us
  starting transfers between devices: 94.8 us -> 82.9 us
    all_to_all x6 -> x7, blocking collectives: 117 us -> 144 us  [exchange(): return lax.all_to_all(x, axis, split_axis=0, concat_axis=0, tiled=True)]
    all_to_all x6 -> x5, waiting for transfers between devices: 50 us -> 36.2 us  [exchange(): return lax.all_to_all(x, axis, split_axis=0, concat_axis=0, tiled=True)]
    all_to_all x6 -> x5, starting transfers between devices: 77.8 us -> 69.6 us  [exchange(): return lax.all_to_all(x, axis, split_axis=0, concat_axis=0, tiled=True)]
    ppermute x5 -> x4, starting transfers between devices: 16.9 us -> 13.3 us  [swapped(): lax.ppermute(mine(both, 1 - p), 'kvp', [(0, 1), (1, 0)])]
    ppermute x5 -> x4, waiting for transfers between devices: 7.6 us -> 6.99 us  [swapped(): lax.ppermute(mine(both, 1 - p), 'kvp', [(0, 1), (1, 0)])]
  transfers between devices with their start and end apart: 11 -> 9, of which waited for: 11 -> 9; matrix products, arithmetic and copies ran while one was open for 1% -> 1% of each run, Pallas kernels for 0% -> 0%
where the time goes in v6:
time: 286 us; the launch traced here: 285 us
  blocking collectives  144 us (50%)
  starting transfers between devices  82.9 us (29%)
  waiting for transfers between devices  43.2 us (15%)
  local copies, waits for them, and re-layouts  5.85 us (2%)
  Pallas kernels  3.79 us (1%)
  other arithmetic  3.41 us (1%)
    all_to_all x7, blocking collectives, exchange(): return lax.all_to_all(x, axis, split_axis=0, concat_axis=0, tiled=True)  144 us
    all_to_all x5, starting transfers between devices, exchange(): return lax.all_to_all(x, axis, split_axis=0, concat_axis=0, tiled=True)  69.6 us
    all_to_all x5, waiting for transfers between devices, exchange(): return lax.all_to_all(x, axis, split_axis=0, concat_axis=0, tiled=True)  36.2 us
    ppermute x4, starting transfers between devices, swapped(): lax.ppermute(mine(both, 1 - p), 'kvp', [(0, 1), (1, 0)])  13.3 us
    ppermute x4, waiting for transfers between devices, swapped(): lax.ppermute(mine(both, 1 - p), 'kvp', [(0, 1), (1, 0)])  6.99 us
  transfers between devices with their start and end apart: 9, of which 9 were waited for; matrix products, arithmetic and copies ran while one was open for 1% of the time, Pallas kernels for 0%

profile of v6, /device:TPU:65, one launch (start us, length us, event | category | flops | bytes accessed | tf_op | source)
XLA Modules:
  0.0 284.9 jit_solution(5716205792622954467)
XLA Ops:
  0.7 1.5 broadcast_in_dim.10
  2.2 45.2 %all-to-all-start = ((bf16[32,12,256]{2,1,0:T(8,128)(2,1)}), bf16[32,12,256]{2,1,0:T(8,128)(2,1)S(1)}, u32[]{:S(2)}, u32[]{:S(2)}) async-start(bf16[32,12,256]{2,1,0:T(8,128)(2,1)} %broadcast_in_dim.10), calls=%async_computation | async-start | bytes 524288 | tf_op jit(solution)/shard_map/all_to_all | solution.py:33
  48.3 3.6 %collective-permute-start = (bf16[2,344,256]{2,1,0:T(8,128)(2,1)S(1)}, bf16[2,344,256]{2,1,0:T(8,128)(2,1)S(1)}, u32[]{:S(2)}, u32[]{:S(2)}) collective-permute-start(bf16[2,344,256]{2,1,0:T(8,128)(2,1)S(1)} %get-tuple-element.34), channel_id=1, source_target_pairs={{0,16},{16,0},{1,17},{17,1},{2,18},{18,2},{3,19},{19,3},{4,20},{20... | collective-permute-start | bytes 1056776 | tf_op jit(solution)/shard_map/ppermute | solution.py:161
  52.9 5.4 %all-to-all-done = bf16[32,12,256]{2,1,0:T(8,128)(2,1)S(1)} async-done(((bf16[32,12,256]{2,1,0:T(8,128)(2,1)}), bf16[32,12,256]{2,1,0:T(8,128)(2,1)S(1)}, u32[]{:S(2)}, u32[]{:S(2)}) %all-to-all-start) | async-done | bytes 196640 | tf_op jit(solution)/shard_map/all_to_all | solution.py:33
  59.8 24.1 %all_to_all.60 = bf16[8,24,768]{2,1,0:T(8,128)(2,1)S(1)} all-to-all(bf16[8,24,768]{2,1,0:T(8,128)(2,1)S(1)} %shard_map.185), channel_id=1, replica_groups=mesh['grp'=2,'kvh'=8,'kvp'=2,'tp'=16] {'kvh'}, dimensions={0} | all-to-all | bytes 589824 | tf_op jit(solution)/shard_map/all_to_all | solution.py:33
  84.3 22.1 %all_to_all.61.h_ref = bf16[16,24,344]{2,1,0:T(8,128)(2,1)S(1)} all-to-all(bf16[16,24,344]{2,1,0:T(8,128)(2,1)S(1)} %broadcast_in_dim.11), channel_id=1, replica_groups=mesh['grp'=2,'kvh'=8,'kvp'=2,'tp'=16] {'kvh','kvp'}, dimensions={0} | all-to-all | bytes 528384 | tf_op jit(solution)/shard_map/all_to_all | solution.py:33
  106.6 23.1 %all_to_all.62 = bf16[16,24,128]{2,1,0:T(8,128)(2,1)S(1)} all-to-all(bf16[16,24,128]{2,1,0:T(8,128)(2,1)S(1)} %shard_map.186), channel_id=1, replica_groups=mesh['grp'=2,'kvh'=8,'kvp'=2,'tp'=16] {'tp'}, dimensions={0} | all-to-all | bytes 196608 | tf_op jit(solution)/shard_map/all_to_all | solution.py:33
  130.5 4.3 %all-to-all-start.4 = ((bf16[32,24,128]{2,1,0:T(8,128)(2,1)}), bf16[32,24,128]{2,1,0:T(8,128)(2,1)S(1)}, u32[]{:S(2)}, u32[]{:S(2)}) async-start(bf16[32,24,128]{2,1,0:T(8,128)(2,1)} %broadcast_in_dim.12), calls=%async_computation.4 | async-start | bytes 393216 | tf_op jit(solution)/shard_map/all_to_all | solution.py:33
  135.7 3.4 %collective-permute-start.1 = (bf16[256,256]{1,0:T(8,128)(2,1)S(1)}, bf16[256,256]{1,0:T(8,128)(2,1)S(1)}, u32[]{:S(2)}, u32[]{:S(2)}) collective-permute-start(bf16[256,256]{1,0:T(8,128)(2,1)S(1)} %get-tuple-element.38), channel_id=1, source_target_pairs={{0,16},{16,0},{1,17},{17,1},{2,18},{18,2},{3,19},{19,3},{4,20},{20... | collective-permute-start | bytes 393224 | tf_op jit(solution)/shard_map/ppermute | solution.py:161
  139.1 3.2 %collective-permute-done.1.got_ref = bf16[256,256]{1,0:T(8,128)(2,1)S(1)} collective-permute-done((bf16[256,256]{1,0:T(8,128)(2,1)S(1)}, bf16[256,256]{1,0:T(8,128)(2,1)S(1)}, u32[]{:S(2)}, u32[]{:S(2)}) %collective-permute-start.1) | collective-permute-done | bytes 131104 | tf_op jit(solution)/shard_map/ppermute | solution.py:161
  142.3 2.1 all-to-all-done.4
  144.6 17.2 %all_to_all.63.z_ref = bf16[16,16,256]{2,1,0:T(8,128)(2,1)S(1)} all-to-all(bf16[16,16,256]{2,1,0:T(8,128)(2,1)S(1)} %shard_map.187), channel_id=1, replica_groups=mesh['grp'=2,'kvh'=8,'kvp'=2,'tp'=16] {'kvh','kvp'}, dimensions={0} | all-to-all | bytes 262144 | tf_op jit(solution)/shard_map/all_to_all | solution.py:33
  163.2 17.0 %all_to_all.64 = bf16[16,12,128]{2,1,0:T(8,128)(2,1)S(1)} all-to-all(bf16[16,12,128]{2,1,0:T(8,128)(2,1)S(1)} %get-tuple-element.22), channel_id=1, replica_groups=mesh['grp'=2,'kvh'=8,'kvp'=2,'tp'=16] {'kvh','kvp'}, dimensions={0} | all-to-all | bytes 98304 | tf_op jit(solution)/shard_map/all_to_all | solution.py:33
  180.5 16.9 %all_to_all.65 = bf16[16,24,128]{2,1,0:T(8,128)(2,1)S(1)} all-to-all(bf16[16,24,128]{2,1,0:T(8,128)(2,1)S(1)} %bitcast.68), channel_id=1, replica_groups=mesh['grp'=2,'kvh'=8,'kvp'=2,'tp'=16] {'tp'}, dimensions={0} | all-to-all | bytes 196608 | tf_op jit(solution)/shard_map/all_to_all | solution.py:33
  198.1 4.3 %all-to-all-start.8 = ((bf16[32,24,128]{2,1,0:T(8,128)(2,1)}), bf16[32,24,128]{2,1,0:T(8,128)(2,1)S(1)}, u32[]{:S(2)}, u32[]{:S(2)}) async-start(bf16[32,24,128]{2,1,0:T(8,128)(2,1)} %broadcast_in_dim.13), calls=%async_computation.8 | async-start | bytes 393216 | tf_op jit(solution)/shard_map/all_to_all | solution.py:33
  202.7 3.1 %collective-permute-start.2 = (bf16[2,344,256]{2,1,0:T(8,128)(2,1)S(1)}, bf16[2,344,256]{2,1,0:T(8,128)(2,1)S(1)}, u32[]{:S(2)}, u32[]{:S(2)}) collective-permute-start(bf16[2,344,256]{2,1,0:T(8,128)(2,1)S(1)} %get-tuple-element.32), channel_id=1, source_target_pairs={{0,16},{16,0},{1,17},{17,1},{2,18},{18,2},{3,19},{19,3},{4,20},{20... | collective-permute-start | bytes 1056776 | tf_op jit(solution)/shard_map/ppermute | solution.py:161
  205.8 6.1 %all-to-all-done.8 = bf16[32,24,128]{2,1,0:T(8,128)(2,1)S(1)} async-done(((bf16[32,24,128]{2,1,0:T(8,128)(2,1)}), bf16[32,24,128]{2,1,0:T(8,128)(2,1)S(1)}, u32[]{:S(2)}, u32[]{:S(2)}) %all-to-all-start.8) | async-done | bytes 196640 | tf_op jit(solution)/shard_map/all_to_all | solution.py:33
  212.0 1.9 collective-permute-done.2.got_ref
  215.0 3.8 %all-to-all-start.9 = ((bf16[8,24,768]{2,1,0:T(8,128)(2,1)}), bf16[8,24,768]{2,1,0:T(8,128)(2,1)S(1)}, u32[]{:S(2)}, u32[]{:S(2)}) async-start(bf16[8,24,768]{2,1,0:T(8,128)(2,1)} %shard_map.189), calls=%async_computation.9 | async-start | bytes 589824 | tf_op jit(solution)/shard_map/all_to_all | solution.py:33
  218.8 3.3 %collective-permute-start.3 = (bf16[344,256]{1,0:T(8,128)(2,1)S(1)}, bf16[344,256]{1,0:T(8,128)(2,1)S(1)}, u32[]{:S(2)}, u32[]{:S(2)}) collective-permute-start(bf16[344,256]{1,0:T(8,128)(2,1)S(1)} %get-tuple-element.36), channel_id=1, source_target_pairs={{0,16},{16,0},{1,17},{17,1},{2,18},{18,2},{3,19},{19,3},{4,20},{20... | collective-permute-start | bytes 528392 | tf_op jit(solution)/shard_map/ppermute | solution.py:161
  222.1 13.0 %all-to-all-done.9 = bf16[8,24,768]{2,1,0:T(8,128)(2,1)S(1)} async-done(((bf16[8,24,768]{2,1,0:T(8,128)(2,1)}), bf16[8,24,768]{2,1,0:T(8,128)(2,1)S(1)}, u32[]{:S(2)}, u32[]{:S(2)}) %all-to-all-start.9) | async-done | bytes 294944 | tf_op jit(solution)/shard_map/all_to_all | solution.py:33
  236.4 24.0 %all_to_all.66.h_ref = bf16[8,24,344]{2,1,0:T(8,128)(2,1)S(1)} all-to-all(bf16[8,24,344]{2,1,0:T(8,128)(2,1)S(1)} %broadcast_in_dim.14), channel_id=1, replica_groups=mesh['grp'=2,'kvh'=8,'kvp'=2,'tp'=16] {'kvh'}, dimensions={0} | all-to-all | bytes 264192 | tf_op jit(solution)/shard_map/all_to_all | solution.py:33
  261.4 12.0 %all-to-all-start.11 = ((bf16[32,12,256]{2,1,0:T(8,128)(2,1)}), bf16[32,12,256]{2,1,0:T(8,128)(2,1)S(1)}, u32[]{:S(2)}, u32[]{:S(2)}) async-start(bf16[32,12,256]{2,1,0:T(8,128)(2,1)} %bitcast.32), calls=%async_computation.11 | async-start | bytes 524288 | tf_op jit(solution)/shard_map/all_to_all | solution.py:33
  274.6 9.6 %all-to-all-done.11 = bf16[32,12,256]{2,1,0:T(8,128)(2,1)S(1)} async-done(((bf16[32,12,256]{2,1,0:T(8,128)(2,1)}), bf16[32,12,256]{2,1,0:T(8,128)(2,1)S(1)}, u32[]{:S(2)}, u32[]{:S(2)}) %all-to-all-start.11) | async-done | bytes 196640 | tf_op jit(solution)/shard_map/all_to_all | solution.py:33
  (80 shorter events, 13.6 us)
Async XLA Ops:
  0.6 179.6 %copy-start = (bf16[128,256]{1,0:T(8,128)(2,1)S(1)}, bf16[128,256]{1,0:T(8,128)(2,1)}, u32[]{:S(2)}) copy-start(bf16[128,256]{1,0:T(8,128)(2,1)} %param.30) | copy-start | bytes 196612
  0.6 46.7 %copy-start.4 = (bf16[256,688]{0,1:T(8,128)(2,1)S(1)}, bf16[256,688]{0,1:T(8,128)(2,1)}, u32[]{:S(2)}) copy-start(bf16[256,688]{0,1:T(8,128)(2,1)} %param.23) | copy-start | bytes 1056772
  0.7 46.7 %copy-start.5 = (bf16[256,688]{0,1:T(8,128)(2,1)S(1)}, bf16[256,688]{0,1:T(8,128)(2,1)}, u32[]{:S(2)}) copy-start(bf16[256,688]{0,1:T(8,128)(2,1)} %param.22) | copy-start | bytes 1056772
  2.2 56.1 %all-to-all-start = ((bf16[32,12,256]{2,1,0:T(8,128)(2,1)}), bf16[32,12,256]{2,1,0:T(8,128)(2,1)S(1)}, u32[]{:S(2)}, u32[]{:S(2)}) async-start(bf16[32,12,256]{2,1,0:T(8,128)(2,1)} %broadcast_in_dim.10), calls=%async_computation | async-start | bytes 524288 | tf_op jit(solution)/shard_map/all_to_all | solution.py:33
  47.4 0.7 copy-start.13
  48.3 11.1 %collective-permute-start = (bf16[2,344,256]{2,1,0:T(8,128)(2,1)S(1)}, bf16[2,344,256]{2,1,0:T(8,128)(2,1)S(1)}, u32[]{:S(2)}, u32[]{:S(2)}) collective-permute-start(bf16[2,344,256]{2,1,0:T(8,128)(2,1)S(1)} %get-tuple-element.34), channel_id=1, source_target_pairs={{0,16},{16,0},{1,17},{17,1},{2,18},{18,2},{3,19},{19,3},{4,20},{20... | collective-permute-start | bytes 1056776 | tf_op jit(solution)/shard_map/ppermute | solution.py:161
  84.3 22.1 %copy-start.2 = (bf16[688,256]{1,0:T(8,128)(2,1)S(1)}, bf16[688,256]{1,0:T(8,128)(2,1)}, u32[]{:S(2)}) copy-start(bf16[688,256]{1,0:T(8,128)(2,1)} %w_ref.1) | copy-start | bytes 1056772
  130.5 4.4 %copy-start.9 = (bf16[256,128]{1,0:T(8,128)(2,1)S(1)}, bf16[256,128]{1,0:T(8,128)(2,1)}, u32[]{:S(2)}) copy-start(bf16[256,128]{1,0:T(8,128)(2,1)} %param.27) | copy-start | bytes 196612
  130.5 4.4 %copy-start.10 = (bf16[256,128]{1,0:T(8,128)(2,1)S(1)}, bf16[256,128]{1,0:T(8,128)(2,1)}, u32[]{:S(2)}) copy-start(bf16[256,128]{1,0:T(8,128)(2,1)} %param.26) | copy-start | bytes 196612
  130.5 4.4 %copy-start.11 = (bf16[256,128]{1,0:T(8,128)(2,1)S(1)}, bf16[256,128]{1,0:T(8,128)(2,1)}, u32[]{:S(2)}) copy-start(bf16[256,128]{1,0:T(8,128)(2,1)} %param.29) | copy-start | bytes 196612
  130.5 4.4 %copy-start.12 = (bf16[256,128]{1,0:T(8,128)(2,1)S(1)}, bf16[256,128]{1,0:T(8,128)(2,1)}, u32[]{:S(2)}) copy-start(bf16[256,128]{1,0:T(8,128)(2,1)} %param.28) | copy-start | bytes 196612
  130.5 13.9 %all-to-all-start.4 = ((bf16[32,24,128]{2,1,0:T(8,128)(2,1)}), bf16[32,24,128]{2,1,0:T(8,128)(2,1)S(1)}, u32[]{:S(2)}, u32[]{:S(2)}) async-start(bf16[32,24,128]{2,1,0:T(8,128)(2,1)} %broadcast_in_dim.12), calls=%async_computation.4 | async-start | bytes 393216 | tf_op jit(solution)/shard_map/all_to_all | solution.py:33
  134.9 0.7 copy-start.14
  135.7 26.1 %copy-start.1 = (f32[12,1,128,128]{3,2,1,0:T(8,128)S(1)}, f32[12,1,128,128]{3,2,1,0:T(8,128)}, u32[]{:S(2)}) copy-start(f32[12,1,128,128]{3,2,1,0:T(8,128)} %param.20) | copy-start | bytes 2359300
  135.7 6.6 %collective-permute-start.1 = (bf16[256,256]{1,0:T(8,128)(2,1)S(1)}, bf16[256,256]{1,0:T(8,128)(2,1)S(1)}, u32[]{:S(2)}, u32[]{:S(2)}) collective-permute-start(bf16[256,256]{1,0:T(8,128)(2,1)S(1)} %get-tuple-element.38), channel_id=1, source_target_pairs={{0,16},{16,0},{1,17},{17,1},{2,18},{18,2},{3,19},{19,3},{4,20},{20... | collective-permute-start | bytes 393224 | tf_op jit(solution)/shard_map/ppermute | solution.py:161
  197.3 5.1 %copy-start.6 = (bf16[256,688]{0,1:T(8,128)(2,1)S(1)}, bf16[256,688]{0,1:T(8,128)(2,1)}, u32[]{:S(2)}) copy-start(bf16[256,688]{0,1:T(8,128)(2,1)} %param.34) | copy-start | bytes 1056772
  197.3 5.1 %copy-start.7 = (bf16[256,688]{0,1:T(8,128)(2,1)S(1)}, bf16[256,688]{0,1:T(8,128)(2,1)}, u32[]{:S(2)}) copy-start(bf16[256,688]{0,1:T(8,128)(2,1)} %param.33) | copy-start | bytes 1056772
  198.1 4.3 %copy-start.15 = (f32[256]{0:T(256)S(1)}, f32[256]{0:T(256)}, u32[]{:S(2)}) copy-start(f32[256]{0:T(256)} %param.32) | copy-start | bytes 3076
  198.1 13.9 %all-to-all-start.8 = ((bf16[32,24,128]{2,1,0:T(8,128)(2,1)}), bf16[32,24,128]{2,1,0:T(8,128)(2,1)S(1)}, u32[]{:S(2)}, u32[]{:S(2)}) async-start(bf16[32,24,128]{2,1,0:T(8,128)(2,1)} %broadcast_in_dim.13), calls=%async_computation.8 | async-start | bytes 393216 | tf_op jit(solution)/shard_map/all_to_all | solution.py:33
  202.7 11.2 %collective-permute-start.2 = (bf16[2,344,256]{2,1,0:T(8,128)(2,1)S(1)}, bf16[2,344,256]{2,1,0:T(8,128)(2,1)S(1)}, u32[]{:S(2)}, u32[]{:S(2)}) collective-permute-start(bf16[2,344,256]{2,1,0:T(8,128)(2,1)S(1)} %get-tuple-element.32), channel_id=1, source_target_pairs={{0,16},{16,0},{1,17},{17,1},{2,18},{18,2},{3,19},{19,3},{4,20},{20... | collective-permute-start | bytes 1056776 | tf_op jit(solution)/shard_map/ppermute | solution.py:161
  215.0 3.8 %copy-start.8 = (bf16[688,256]{1,0:T(8,128)(2,1)S(1)}, bf16[688,256]{1,0:T(8,128)(2,1)}, u32[]{:S(2)}) copy-start(bf16[688,256]{1,0:T(8,128)(2,1)} %param.35) | copy-start | bytes 1056772
  215.0 20.1 %all-to-all-start.9 = ((bf16[8,24,768]{2,1,0:T(8,128)(2,1)}), bf16[8,24,768]{2,1,0:T(8,128)(2,1)S(1)}, u32[]{:S(2)}, u32[]{:S(2)}) async-start(bf16[8,24,768]{2,1,0:T(8,128)(2,1)} %shard_map.189), calls=%async_computation.9 | async-start | bytes 589824 | tf_op jit(solution)/shard_map/all_to_all | solution.py:33
  218.8 17.6 %collective-permute-start.3 = (bf16[344,256]{1,0:T(8,128)(2,1)S(1)}, bf16[344,256]{1,0:T(8,128)(2,1)S(1)}, u32[]{:S(2)}, u32[]{:S(2)}) collective-permute-start(bf16[344,256]{1,0:T(8,128)(2,1)S(1)} %get-tuple-element.36), channel_id=1, source_target_pairs={{0,16},{16,0},{1,17},{17,1},{2,18},{18,2},{3,19},{19,3},{4,20},{20... | collective-permute-start | bytes 528392 | tf_op jit(solution)/shard_map/ppermute | solution.py:161
  261.4 22.8 %all-to-all-start.11 = ((bf16[32,12,256]{2,1,0:T(8,128)(2,1)}), bf16[32,12,256]{2,1,0:T(8,128)(2,1)S(1)}, u32[]{:S(2)}, u32[]{:S(2)}) async-start(bf16[32,12,256]{2,1,0:T(8,128)(2,1)} %bitcast.32), calls=%async_computation.11 | async-start | bytes 524288 | tf_op jit(solution)/shard_map/all_to_all | solution.py:33
  (2 other events, 1.3 us)

commit v7 on v5

--- a/solution.py
+++ b/solution.py
@@ -173,17 +173,19 @@
     features = wide * lax.axis_size(KV)
     factor = lax.rsqrt(total[:, part : part + 1] / features + EPS_NORM)
     hidden = jax.nn.silu(factor * total[:, :part]) * (factor * total[:, half : half + part])
-    hidden, back_weights = lax.optimization_barrier((hidden.astype(jnp.bfloat16), back_weights))
+    hidden = hidden.astype(jnp.bfloat16)
+    hidden, back_weights = lax.optimization_barrier((hidden, back_weights))
     everyone = spread(hidden, "kvh")
-    shape = (2, tp, rows // tp, wide) if flat else (2, tp, tall, rows * wide // (tp * tall))
-    return local_call(
+    chunk = (rows // tp, wide) if flat else (tall, rows * wide // (tp * tall))
+    back = local_call(
         down_kernel,
-        jax.ShapeDtypeStruct(shape, jnp.bfloat16),
+        jax.ShapeDtypeStruct((2, tp, *chunk), jnp.bfloat16),
         everyone,
         *back_weights,
         scratch=(pltpu.VMEM((rows, part), jnp.bfloat16), pltpu.VMEM((rows, wide), jnp.float32)),
         flops=4 * rows * part * wide,
     )
+    return back.reshape(2 * tp, *chunk)
 
 
 def advance(own, back, branch, axis):
@@ -280,7 +282,7 @@
     gathered, own, ready = lax.optimization_barrier((gathered, own, ready))
     cosine, sine, decay, place, offset = ready
     back = feed_forward(gathered, first_pair, first_back, False)
-    own = advance(own, back.reshape(2 * tp, tall, wide), 0.5, BOTH)
+    own = advance(own, back, 0.5, BOTH)
     gathered = spread(own, BOTH).reshape(2, tp, tall, wide)
     ret_out, new_state = retention(gathered, heads_pair, features, head_gain, ret_state, (cosine, sine, decay))
     back = jnp.dot(ret_out, w_out, preferred_element_type=jnp.float32).astype(jnp.bfloat16)
@@ -291,7 +293,7 @@
     own = jnp.concatenate([own[i] for i in range(across)], axis=1)
     gathered, own = lax.optimization_barrier((gathered, own))
     back = feed_forward(gathered, second_pair, second_back, True)
-    return advance(own, back.reshape(2 * tp, few, block), 0.5, BOTH), new_state
+    return advance(own, back, 0.5, BOTH), new_state
 
 
 def solution(mesh):

time: 286 us -> 286 us (level)
  no operation moved by 1% of the time
where the time goes in v7:
time: 286 us; the launch traced here: 285 us
  blocking collectives  117 us (41%)
  starting transfers between devices  94.8 us (33%)
  waiting for transfers between devices  57.6 us (20%)
  local copies, waits for them, and re-layouts  5.89 us (2%)
  Pallas kernels  4.54 us (2%)
  other arithmetic  3.42 us (1%)
    all_to_all x6, blocking collectives, exchange(): return lax.all_to_all(x, axis, split_axis=0, concat_axis=0, tiled=True)  117 us
    all_to_all x6, starting transfers between devices, exchange(): return lax.all_to_all(x, axis, split_axis=0, concat_axis=0, tiled=True)  77.8 us
    all_to_all x6, waiting for transfers between devices, exchange(): return lax.all_to_all(x, axis, split_axis=0, concat_axis=0, tiled=True)  50 us
    ppermute x5, starting transfers between devices, swapped(): lax.ppermute(mine(both, 1 - p), 'kvp', [(0, 1), (1, 0)])  16.9 us
    ppermute x5, waiting for transfers between devices, swapped(): lax.ppermute(mine(both, 1 - p), 'kvp', [(0, 1), (1, 0)])  7.6 us
  transfers between devices with their start and end apart: 11, of which 11 were waited for; matrix products, arithmetic and copies ran while one was open for 1% of the time, Pallas kernels for 0%

profile of v7, /device:TPU:65, one launch (start us, length us, event | category | flops | bytes accessed | tf_op | source)
XLA Modules:
  0.0 285.0 jit_solution(14858895359458352770)
XLA Ops:
  2.2 45.2 %all-to-all-start = ((bf16[32,12,256]{2,1,0:T(8,128)(2,1)}), bf16[32,12,256]{2,1,0:T(8,128)(2,1)S(1)}, u32[]{:S(2)}, u32[]{:S(2)}) async-start(bf16[32,12,256]{2,1,0:T(8,128)(2,1)} %broadcast_in_dim.10), calls=%async_computation | async-start | bytes 524288 | tf_op jit(solution)/shard_map/all_to_all | solution.py:33
  48.3 3.6 %collective-permute-start = (bf16[2,344,256]{2,1,0:T(8,128)(2,1)S(1)}, bf16[2,344,256]{2,1,0:T(8,128)(2,1)S(1)}, u32[]{:S(2)}, u32[]{:S(2)}) collective-permute-start(bf16[2,344,256]{2,1,0:T(8,128)(2,1)S(1)} %get-tuple-element.40), channel_id=1, source_target_pairs={{0,16},{16,0},{1,17},{17,1},{2,18},{18,2},{3,19},{19,3},{4,20},{20... | collective-permute-start | bytes 1056776 | tf_op jit(solution)/shard_map/ppermute | solution.py:144
  52.9 5.4 %all-to-all-done = bf16[32,12,256]{2,1,0:T(8,128)(2,1)S(1)} async-done(((bf16[32,12,256]{2,1,0:T(8,128)(2,1)}), bf16[32,12,256]{2,1,0:T(8,128)(2,1)S(1)}, u32[]{:S(2)}, u32[]{:S(2)}) %all-to-all-start) | async-done | bytes 196640 | tf_op jit(solution)/shard_map/all_to_all | solution.py:33
  60.5 8.0 %all-to-all-start.1 = ((bf16[8,24,768]{2,1,0:T(8,128)(2,1)}), bf16[8,24,768]{2,1,0:T(8,128)(2,1)S(1)}, u32[]{:S(2)}, u32[]{:S(2)}) async-start(bf16[8,24,768]{2,1,0:T(8,128)(2,1)} %shard_map.185), calls=%async_computation.1 | async-start | bytes 589824 | tf_op jit(solution)/shard_map/all_to_all | solution.py:33
  68.6 3.6 %collective-permute-start.1 = (bf16[344,256]{1,0:T(8,128)(2,1)S(1)}, bf16[344,256]{1,0:T(8,128)(2,1)S(1)}, u32[]{:S(2)}, u32[]{:S(2)}) collective-permute-start(bf16[344,256]{1,0:T(8,128)(2,1)S(1)} %get-tuple-element.44), channel_id=1, source_target_pairs={{0,16},{16,0},{1,17},{17,1},{2,18},{18,2},{3,19},{19,3},{4,20},{20... | collective-permute-start | bytes 528392 | tf_op jit(solution)/shard_map/ppermute | solution.py:144
  72.1 13.4 %all-to-all-done.1 = bf16[8,24,768]{2,1,0:T(8,128)(2,1)S(1)} async-done(((bf16[8,24,768]{2,1,0:T(8,128)(2,1)}), bf16[8,24,768]{2,1,0:T(8,128)(2,1)S(1)}, u32[]{:S(2)}, u32[]{:S(2)}) %all-to-all-start.1) | async-done | bytes 294944 | tf_op jit(solution)/shard_map/all_to_all | solution.py:33
  86.7 23.8 %all_to_all.60.h_ref = bf16[8,24,344]{2,1,0:T(8,128)(2,1)S(1)} all-to-all(bf16[8,24,344]{2,1,0:T(8,128)(2,1)S(1)} %broadcast_in_dim.11), channel_id=1, replica_groups=mesh['grp'=2,'kvh'=8,'kvp'=2,'tp'=16] {'kvh'}, dimensions={0} | all-to-all | bytes 264192 | tf_op jit(solution)/shard_map/all_to_all | solution.py:33
  110.8 21.8 %all_to_all.61 = bf16[32,24,128]{2,1,0:T(8,128)(2,1)S(1)} all-to-all(bf16[32,24,128]{2,1,0:T(8,128)(2,1)S(1)} %bitcast.68), channel_id=1, replica_groups=mesh['grp'=2,'kvh'=8,'kvp'=2,'tp'=16] {'kvp','tp'}, dimensions={0} | all-to-all | bytes 393216 | tf_op jit(solution)/shard_map/all_to_all | solution.py:33
  133.4 4.6 %all-to-all-start.4 = ((bf16[32,24,128]{2,1,0:T(8,128)(2,1)}), bf16[32,24,128]{2,1,0:T(8,128)(2,1)S(1)}, u32[]{:S(2)}, u32[]{:S(2)}) async-start(bf16[32,24,128]{2,1,0:T(8,128)(2,1)} %broadcast_in_dim.12), calls=%async_computation.4 | async-start | bytes 393216 | tf_op jit(solution)/shard_map/all_to_all | solution.py:33
  138.8 3.4 %collective-permute-start.2 = (bf16[256,256]{1,0:T(8,128)(2,1)S(1)}, bf16[256,256]{1,0:T(8,128)(2,1)S(1)}, u32[]{:S(2)}, u32[]{:S(2)}) collective-permute-start(bf16[256,256]{1,0:T(8,128)(2,1)S(1)} %get-tuple-element.46), channel_id=1, source_target_pairs={{0,16},{16,0},{1,17},{17,1},{2,18},{18,2},{3,19},{19,3},{4,20},{20... | collective-permute-start | bytes 393224 | tf_op jit(solution)/shard_map/ppermute | solution.py:144
  142.3 3.0 %collective-permute-done.2.got_ref = bf16[256,256]{1,0:T(8,128)(2,1)S(1)} collective-permute-done((bf16[256,256]{1,0:T(8,128)(2,1)S(1)}, bf16[256,256]{1,0:T(8,128)(2,1)S(1)}, u32[]{:S(2)}, u32[]{:S(2)}) %collective-permute-start.2) | collective-permute-done | bytes 131104 | tf_op jit(solution)/shard_map/ppermute | solution.py:144
  145.3 2.4 all-to-all-done.4
  147.9 14.8 %all_to_all.62.z_ref = bf16[16,16,256]{2,1,0:T(8,128)(2,1)S(1)} all-to-all(bf16[16,16,256]{2,1,0:T(8,128)(2,1)S(1)} %shard_map.187), channel_id=1, replica_groups=mesh['grp'=2,'kvh'=8,'kvp'=2,'tp'=16] {'kvh','kvp'}, dimensions={0} | all-to-all | bytes 262144 | tf_op jit(solution)/shard_map/all_to_all | solution.py:33
  164.1 17.7 %all_to_all.63 = bf16[16,12,128]{2,1,0:T(8,128)(2,1)S(1)} all-to-all(bf16[16,12,128]{2,1,0:T(8,128)(2,1)S(1)} %get-tuple-element.28), channel_id=1, replica_groups=mesh['grp'=2,'kvh'=8,'kvp'=2,'tp'=16] {'kvh','kvp'}, dimensions={0} | all-to-all | bytes 98304 | tf_op jit(solution)/shard_map/all_to_all | solution.py:33
  182.0 15.4 %all_to_all.64 = bf16[16,24,128]{2,1,0:T(8,128)(2,1)S(1)} all-to-all(bf16[16,24,128]{2,1,0:T(8,128)(2,1)S(1)} %bitcast.75), channel_id=1, replica_groups=mesh['grp'=2,'kvh'=8,'kvp'=2,'tp'=16] {'tp'}, dimensions={0} | all-to-all | bytes 196608 | tf_op jit(solution)/shard_map/all_to_all | solution.py:33
  198.2 4.3 %all-to-all-start.8 = ((bf16[32,24,128]{2,1,0:T(8,128)(2,1)}), bf16[32,24,128]{2,1,0:T(8,128)(2,1)S(1)}, u32[]{:S(2)}, u32[]{:S(2)}) async-start(bf16[32,24,128]{2,1,0:T(8,128)(2,1)} %broadcast_in_dim.13), calls=%async_computation.8 | async-start | bytes 393216 | tf_op jit(solution)/shard_map/all_to_all | solution.py:33
  202.8 3.1 %collective-permute-start.3 = (bf16[2,344,256]{2,1,0:T(8,128)(2,1)S(1)}, bf16[2,344,256]{2,1,0:T(8,128)(2,1)S(1)}, u32[]{:S(2)}, u32[]{:S(2)}) collective-permute-start(bf16[2,344,256]{2,1,0:T(8,128)(2,1)S(1)} %get-tuple-element.38), channel_id=1, source_target_pairs={{0,16},{16,0},{1,17},{17,1},{2,18},{18,2},{3,19},{19,3},{4,20},{20... | collective-permute-start | bytes 1056776 | tf_op jit(solution)/shard_map/ppermute | solution.py:144
  206.0 6.1 %all-to-all-done.8 = bf16[32,24,128]{2,1,0:T(8,128)(2,1)S(1)} async-done(((bf16[32,24,128]{2,1,0:T(8,128)(2,1)}), bf16[32,24,128]{2,1,0:T(8,128)(2,1)S(1)}, u32[]{:S(2)}, u32[]{:S(2)}) %all-to-all-start.8) | async-done | bytes 196640 | tf_op jit(solution)/shard_map/all_to_all | solution.py:33
  215.2 3.8 %all-to-all-start.9 = ((bf16[8,24,768]{2,1,0:T(8,128)(2,1)}), bf16[8,24,768]{2,1,0:T(8,128)(2,1)S(1)}, u32[]{:S(2)}, u32[]{:S(2)}) async-start(bf16[8,24,768]{2,1,0:T(8,128)(2,1)} %shard_map.189), calls=%async_computation.9 | async-start | bytes 589824 | tf_op jit(solution)/shard_map/all_to_all | solution.py:33
  219.0 3.3 %collective-permute-start.4 = (bf16[344,256]{1,0:T(8,128)(2,1)S(1)}, bf16[344,256]{1,0:T(8,128)(2,1)S(1)}, u32[]{:S(2)}, u32[]{:S(2)}) collective-permute-start(bf16[344,256]{1,0:T(8,128)(2,1)S(1)} %get-tuple-element.42), channel_id=1, source_target_pairs={{0,16},{16,0},{1,17},{17,1},{2,18},{18,2},{3,19},{19,3},{4,20},{20... | collective-permute-start | bytes 528392 | tf_op jit(solution)/shard_map/ppermute | solution.py:144
  222.3 13.0 %all-to-all-done.9 = bf16[8,24,768]{2,1,0:T(8,128)(2,1)S(1)} async-done(((bf16[8,24,768]{2,1,0:T(8,128)(2,1)}), bf16[8,24,768]{2,1,0:T(8,128)(2,1)S(1)}, u32[]{:S(2)}, u32[]{:S(2)}) %all-to-all-start.9) | async-done | bytes 294944 | tf_op jit(solution)/shard_map/all_to_all | solution.py:33
  236.6 24.0 %all_to_all.65.h_ref = bf16[8,24,344]{2,1,0:T(8,128)(2,1)S(1)} all-to-all(bf16[8,24,344]{2,1,0:T(8,128)(2,1)S(1)} %broadcast_in_dim.14), channel_id=1, replica_groups=mesh['grp'=2,'kvh'=8,'kvp'=2,'tp'=16] {'kvh'}, dimensions={0} | all-to-all | bytes 264192 | tf_op jit(solution)/shard_map/all_to_all | solution.py:33
  261.6 12.0 %all-to-all-start.11 = ((bf16[32,12,256]{2,1,0:T(8,128)(2,1)}), bf16[32,12,256]{2,1,0:T(8,128)(2,1)S(1)}, u32[]{:S(2)}, u32[]{:S(2)}) async-start(bf16[32,12,256]{2,1,0:T(8,128)(2,1)} %bitcast.36), calls=%async_computation.11 | async-start | bytes 524288 | tf_op jit(solution)/shard_map/all_to_all | solution.py:33
  274.7 9.6 %all-to-all-done.11 = bf16[32,12,256]{2,1,0:T(8,128)(2,1)S(1)} async-done(((bf16[32,12,256]{2,1,0:T(8,128)(2,1)}), bf16[32,12,256]{2,1,0:T(8,128)(2,1)S(1)}, u32[]{:S(2)}, u32[]{:S(2)}) %all-to-all-start.11) | async-done | bytes 196640 | tf_op jit(solution)/shard_map/all_to_all | solution.py:33
  (84 shorter events, 18.6 us)
Async XLA Ops:
  0.6 181.2 %copy-start = (bf16[128,256]{1,0:T(8,128)(2,1)S(1)}, bf16[128,256]{1,0:T(8,128)(2,1)}, u32[]{:S(2)}) copy-start(bf16[128,256]{1,0:T(8,128)(2,1)} %param.30) | copy-start | bytes 196612
  0.6 46.7 %copy-start.3 = (bf16[256,688]{0,1:T(8,128)(2,1)S(1)}, bf16[256,688]{0,1:T(8,128)(2,1)}, u32[]{:S(2)}) copy-start(bf16[256,688]{0,1:T(8,128)(2,1)} %param.23) | copy-start | bytes 1056772
  0.7 46.7 %copy-start.4 = (bf16[256,688]{0,1:T(8,128)(2,1)S(1)}, bf16[256,688]{0,1:T(8,128)(2,1)}, u32[]{:S(2)}) copy-start(bf16[256,688]{0,1:T(8,128)(2,1)} %param.22) | copy-start | bytes 1056772
  2.2 56.1 %all-to-all-start = ((bf16[32,12,256]{2,1,0:T(8,128)(2,1)}), bf16[32,12,256]{2,1,0:T(8,128)(2,1)S(1)}, u32[]{:S(2)}, u32[]{:S(2)}) async-start(bf16[32,12,256]{2,1,0:T(8,128)(2,1)} %broadcast_in_dim.10), calls=%async_computation | async-start | bytes 524288 | tf_op jit(solution)/shard_map/all_to_all | solution.py:33
  48.3 11.1 %collective-permute-start = (bf16[2,344,256]{2,1,0:T(8,128)(2,1)S(1)}, bf16[2,344,256]{2,1,0:T(8,128)(2,1)S(1)}, u32[]{:S(2)}, u32[]{:S(2)}) collective-permute-start(bf16[2,344,256]{2,1,0:T(8,128)(2,1)S(1)} %get-tuple-element.40), channel_id=1, source_target_pairs={{0,16},{16,0},{1,17},{17,1},{2,18},{18,2},{3,19},{19,3},{4,20},{20... | collective-permute-start | bytes 1056776 | tf_op jit(solution)/shard_map/ppermute | solution.py:144
  60.5 8.0 %copy-start.7 = (bf16[688,256]{1,0:T(8,128)(2,1)S(1)}, bf16[688,256]{1,0:T(8,128)(2,1)}, u32[]{:S(2)}) copy-start(bf16[688,256]{1,0:T(8,128)(2,1)} %param.24) | copy-start | bytes 1056772
  60.5 25.0 %all-to-all-start.1 = ((bf16[8,24,768]{2,1,0:T(8,128)(2,1)}), bf16[8,24,768]{2,1,0:T(8,128)(2,1)S(1)}, u32[]{:S(2)}, u32[]{:S(2)}) async-start(bf16[8,24,768]{2,1,0:T(8,128)(2,1)} %shard_map.185), calls=%async_computation.1 | async-start | bytes 589824 | tf_op jit(solution)/shard_map/all_to_all | solution.py:33
  68.6 18.1 %collective-permute-start.1 = (bf16[344,256]{1,0:T(8,128)(2,1)S(1)}, bf16[344,256]{1,0:T(8,128)(2,1)S(1)}, u32[]{:S(2)}, u32[]{:S(2)}) collective-permute-start(bf16[344,256]{1,0:T(8,128)(2,1)S(1)} %get-tuple-element.44), channel_id=1, source_target_pairs={{0,16},{16,0},{1,17},{17,1},{2,18},{18,2},{3,19},{19,3},{4,20},{20... | collective-permute-start | bytes 528392 | tf_op jit(solution)/shard_map/ppermute | solution.py:144
  133.3 4.6 %copy-start.9 = (bf16[256,128]{1,0:T(8,128)(2,1)S(1)}, bf16[256,128]{1,0:T(8,128)(2,1)}, u32[]{:S(2)}) copy-start(bf16[256,128]{1,0:T(8,128)(2,1)} %param.27) | copy-start | bytes 196612
  133.3 4.6 %copy-start.10 = (bf16[256,128]{1,0:T(8,128)(2,1)S(1)}, bf16[256,128]{1,0:T(8,128)(2,1)}, u32[]{:S(2)}) copy-start(bf16[256,128]{1,0:T(8,128)(2,1)} %param.26) | copy-start | bytes 196612
  133.3 4.6 %copy-start.11 = (bf16[256,128]{1,0:T(8,128)(2,1)S(1)}, bf16[256,128]{1,0:T(8,128)(2,1)}, u32[]{:S(2)}) copy-start(bf16[256,128]{1,0:T(8,128)(2,1)} %param.29) | copy-start | bytes 196612
  133.3 4.6 %copy-start.12 = (bf16[256,128]{1,0:T(8,128)(2,1)S(1)}, bf16[256,128]{1,0:T(8,128)(2,1)}, u32[]{:S(2)}) copy-start(bf16[256,128]{1,0:T(8,128)(2,1)} %param.28) | copy-start | bytes 196612
  133.4 14.3 %all-to-all-start.4 = ((bf16[32,24,128]{2,1,0:T(8,128)(2,1)}), bf16[32,24,128]{2,1,0:T(8,128)(2,1)S(1)}, u32[]{:S(2)}, u32[]{:S(2)}) async-start(bf16[32,24,128]{2,1,0:T(8,128)(2,1)} %broadcast_in_dim.12), calls=%async_computation.4 | async-start | bytes 393216 | tf_op jit(solution)/shard_map/all_to_all | solution.py:33
  138.8 23.9 %copy-start.1 = (f32[12,1,128,128]{3,2,1,0:T(8,128)S(1)}, f32[12,1,128,128]{3,2,1,0:T(8,128)}, u32[]{:S(2)}) copy-start(f32[12,1,128,128]{3,2,1,0:T(8,128)} %param.20) | copy-start | bytes 2359300
  138.8 6.4 %collective-permute-start.2 = (bf16[256,256]{1,0:T(8,128)(2,1)S(1)}, bf16[256,256]{1,0:T(8,128)(2,1)S(1)}, u32[]{:S(2)}, u32[]{:S(2)}) collective-permute-start(bf16[256,256]{1,0:T(8,128)(2,1)S(1)} %get-tuple-element.46), channel_id=1, source_target_pairs={{0,16},{16,0},{1,17},{17,1},{2,18},{18,2},{3,19},{19,3},{4,20},{20... | collective-permute-start | bytes 393224 | tf_op jit(solution)/shard_map/ppermute | solution.py:144
  197.5 5.1 %copy-start.5 = (bf16[256,688]{0,1:T(8,128)(2,1)S(1)}, bf16[256,688]{0,1:T(8,128)(2,1)}, u32[]{:S(2)}) copy-start(bf16[256,688]{0,1:T(8,128)(2,1)} %param.34) | copy-start | bytes 1056772
  197.5 5.1 %copy-start.6 = (bf16[256,688]{0,1:T(8,128)(2,1)S(1)}, bf16[256,688]{0,1:T(8,128)(2,1)}, u32[]{:S(2)}) copy-start(bf16[256,688]{0,1:T(8,128)(2,1)} %param.33) | copy-start | bytes 1056772
  198.2 4.3 %copy-start.15 = (f32[256]{0:T(256)S(1)}, f32[256]{0:T(256)}, u32[]{:S(2)}) copy-start(f32[256]{0:T(256)} %param.32) | copy-start | bytes 3076
  198.2 13.9 %all-to-all-start.8 = ((bf16[32,24,128]{2,1,0:T(8,128)(2,1)}), bf16[32,24,128]{2,1,0:T(8,128)(2,1)S(1)}, u32[]{:S(2)}, u32[]{:S(2)}) async-start(bf16[32,24,128]{2,1,0:T(8,128)(2,1)} %broadcast_in_dim.13), calls=%async_computation.8 | async-start | bytes 393216 | tf_op jit(solution)/shard_map/all_to_all | solution.py:33
  202.8 11.2 %collective-permute-start.3 = (bf16[2,344,256]{2,1,0:T(8,128)(2,1)S(1)}, bf16[2,344,256]{2,1,0:T(8,128)(2,1)S(1)}, u32[]{:S(2)}, u32[]{:S(2)}) collective-permute-start(bf16[2,344,256]{2,1,0:T(8,128)(2,1)S(1)} %get-tuple-element.38), channel_id=1, source_target_pairs={{0,16},{16,0},{1,17},{17,1},{2,18},{18,2},{3,19},{19,3},{4,20},{20... | collective-permute-start | bytes 1056776 | tf_op jit(solution)/shard_map/ppermute | solution.py:144
  215.2 3.8 %copy-start.8 = (bf16[688,256]{1,0:T(8,128)(2,1)S(1)}, bf16[688,256]{1,0:T(8,128)(2,1)}, u32[]{:S(2)}) copy-start(bf16[688,256]{1,0:T(8,128)(2,1)} %param.35) | copy-start | bytes 1056772
  215.2 20.1 %all-to-all-start.9 = ((bf16[8,24,768]{2,1,0:T(8,128)(2,1)}), bf16[8,24,768]{2,1,0:T(8,128)(2,1)S(1)}, u32[]{:S(2)}, u32[]{:S(2)}) async-start(bf16[8,24,768]{2,1,0:T(8,128)(2,1)} %shard_map.189), calls=%async_computation.9 | async-start | bytes 589824 | tf_op jit(solution)/shard_map/all_to_all | solution.py:33
  219.0 17.6 %collective-permute-start.4 = (bf16[344,256]{1,0:T(8,128)(2,1)S(1)}, bf16[344,256]{1,0:T(8,128)(2,1)S(1)}, u32[]{:S(2)}, u32[]{:S(2)}) collective-permute-start(bf16[344,256]{1,0:T(8,128)(2,1)S(1)} %get-tuple-element.42), channel_id=1, source_target_pairs={{0,16},{16,0},{1,17},{17,1},{2,18},{18,2},{3,19},{19,3},{4,20},{20... | collective-permute-start | bytes 528392 | tf_op jit(solution)/shard_map/ppermute | solution.py:144
  261.6 22.8 %all-to-all-start.11 = ((bf16[32,12,256]{2,1,0:T(8,128)(2,1)}), bf16[32,12,256]{2,1,0:T(8,128)(2,1)S(1)}, u32[]{:S(2)}, u32[]{:S(2)}) async-start(bf16[32,12,256]{2,1,0:T(8,128)(2,1)} %bitcast.36), calls=%async_computation.11 | async-start | bytes 524288 | tf_op jit(solution)/shard_map/all_to_all | solution.py:33
  (4 other events, 2.7 us)

commit v8 on v7

--- a/solution.py
+++ b/solution.py
@@ -42,10 +42,6 @@
 
 
 def fill_rows(x, y_ref, p):
-    if len(y_ref.shape) == 3:
-        x[0] = y_ref[p]
-        x[1] = y_ref[1 - p]
-        return
     _, chunks, tall, wide = y_ref.shape
     across = x.shape[2] // wide
     for n in range(chunks):
@@ -55,8 +51,23 @@
         x[(1, *place)] = y_ref[1 - p, n]
 
 
-def up_kernel(y_ref, own_ref, got_ref, out_ref, x):
-    fill_rows(x, y_ref, lax.axis_index("kvp"))
+def fill_flat(x, y_ref, scr, p):
+    _, chunks, tall, wide = y_ref.shape
+    across = x.shape[2] // wide
+    few = tall // across
+    for j, q in enumerate((p, 1 - p)):
+        for n in range(chunks):
+            block = y_ref[q, n].astype(jnp.float32)
+            for c in range(across):
+                scr[n * few : (n + 1) * few, c * wide : (c + 1) * wide] = block[c * few : (c + 1) * few]
+        x[j] = scr[...].astype(jnp.bfloat16)
+
+
+def up_kernel(flat, y_ref, own_ref, got_ref, out_ref, x, scr):
+    if flat:
+        fill_flat(x, y_ref, scr, lax.axis_index("kvp"))
+    else:
+        fill_rows(x, y_ref, lax.axis_index("kvp"))
     groups, tall, lanes = out_ref.shape
     part = own_ref.shape[1]
     half = lanes // 2
@@ -72,7 +83,7 @@
             out_ref[r, :, i * half : (i + 1) * half] = rows[r * tall : (r + 1) * tall]
 
 
-def down_kernel(h_ref, own_ref, got_ref, out_ref, h, scr):
+def down_kernel(flat, h_ref, own_ref, got_ref, out_ref, h, scr):
     groups, tall, _ = h_ref.shape
     p = lax.axis_index("kvp")
     for r in range(groups):
@@ -82,8 +93,13 @@
     for place, w in ((p, own_ref), (1 - p, got_ref)):
         scr[...] = jnp.dot(h[...], w[...], preferred_element_type=jnp.float32)
         for n in range(chunks):
-            r, c = divmod(n, across)
-            piece = scr[r * high : (r + 1) * high, c * wide : (c + 1) * wide]
+            if flat:
+                few = high // across
+                cuts = [scr[n * few : (n + 1) * few, c * wide : (c + 1) * wide] for c in range(across)]
+                piece = jnp.concatenate(cuts, axis=0)
+            else:
+                r, c = divmod(n, across)
+                piece = scr[r * high : (r + 1) * high, c * wide : (c + 1) * wide]
             out_ref[place, n] = piece.astype(jnp.bfloat16)
 
 
@@ -145,9 +161,15 @@
 
 
 def paired_weights(norm_gain, w_gate, w_up):
-    width = w_gate.shape[0]
-    scaled = [(w.T.astype(jnp.float32) * norm_gain).astype(jnp.bfloat16) for w in (w_gate, w_up)]
-    return swapped(jnp.stack([w.reshape(2, -1, width) for w in scaled], axis=1))
+    p = lax.axis_index("kvp")
+    halves = tuple(w.T.reshape(2, -1, w.shape[0]) for w in (w_gate, w_up))
+
+    def scaled(index, halves):
+        return jnp.stack([(mine(w, index).astype(jnp.float32) * norm_gain).astype(jnp.bfloat16) for w in halves])
+
+    sent = scaled(1 - p, halves)
+    sent, halves = lax.optimization_barrier((sent, halves))
+    return scaled(p, halves), lax.ppermute(sent, "kvp", [(0, 1), (1, 0)])
 
 
 def paired_rows(w_down):
@@ -161,12 +183,12 @@
     rows = gathered.size // (2 * wide)
     tall, half = rows // members, -(-(part + 1) // 128) * 128
     sent = local_call(
-        up_kernel,
+        functools.partial(up_kernel, not flat),
         jax.ShapeDtypeStruct((members, tall, 2 * half), jnp.bfloat16),
         gathered,
         own_w,
         got_w,
-        scratch=(pltpu.VMEM((2, rows, wide), jnp.bfloat16),),
+        scratch=(pltpu.VMEM((2, rows, wide), jnp.bfloat16), pltpu.VMEM((rows, wide), jnp.float32)),
         flops=8 * rows * wide * part,
     )
     total = exchange(sent, "kvh").astype(jnp.float32).sum(axis=0)
@@ -176,9 +198,9 @@
     hidden = hidden.astype(jnp.bfloat16)
     hidden, back_weights = lax.optimization_barrier((hidden, back_weights))
     everyone = spread(hidden, "kvh")
-    chunk = (rows // tp, wide) if flat else (tall, rows * wide // (tp * tall))
+    chunk = (tall, rows * wide // (tp * tall))
     back = local_call(
-        down_kernel,
+        functools.partial(down_kernel, flat),
         jax.ShapeDtypeStruct((2, tp, *chunk), jnp.bfloat16),
         everyone,
         *back_weights,
@@ -190,6 +212,8 @@
 
 def advance(own, back, branch, axis):
     share = exchange(back, axis).astype(jnp.float32).sum(axis=0)
+    if share.shape != own.shape:
+        share = jnp.concatenate(jnp.split(share, own.shape[1] // share.shape[1], axis=0), axis=1)
     return (own.astype(jnp.float32) + branch * share).astype(jnp.bfloat16)
 
 
@@ -265,25 +289,29 @@
     angles = positions.astype(jnp.float32)[:, None] * inverse[None, :]
     cosine, sine = jnp.cos(angles), jnp.sin(angles)
     cosine, sine = jnp.concatenate([cosine, cosine], axis=1), jnp.concatenate([-sine, sine], axis=1)
-    decay = jnp.exp(jnp.log1p(-(2.0 ** (-5.0 - t.astype(jnp.float32))))) * jnp.ones((1, 2 * half), jnp.float32)
+    decay = jnp.exp(jnp.log1p(-(2.0 ** (-5.0 - t.astype(jnp.float32)))))
     place = lax.div(t * few, tall)
-    ready = (cosine, sine, decay, place, t * few - place * tall)
+    scalars = (decay, place, t * few - place * tall)
 
     first_pair = paired_weights(first_gain, first_gate, first_up)
     first_back = paired_rows(first_down)
-    second_pair = paired_weights(second_gain, second_gate, second_up)
     second_back = paired_rows(second_down)
     halves = [jnp.concatenate(w, axis=1) for w in ((w_query, w_key), (w_value, w_outgate))]
     halves = jnp.stack(halves).astype(jnp.float32) * mix_gain[:, None]
     heads_pair = swapped(halves.astype(jnp.bfloat16))
 
-    gathered = spread(stream_in, BOTH).reshape(2, rows, block)
-    own = lax.dynamic_slice(gathered, (p, r * tall, c * wide), (1, tall, wide))[0]
-    gathered, own, ready = lax.optimization_barrier((gathered, own, ready))
-    cosine, sine, decay, place, offset = ready
+    cuts = jnp.concatenate(jnp.split(stream_in, across, axis=1), axis=0)
+    gathered = spread(cuts, BOTH).reshape(2, tp, tall, wide)
+    own = lax.dynamic_slice(gathered, (p, r * across, c * few, 0), (1, across, few, wide)).reshape(tall, wide)
+    gathered, own, scalars = lax.optimization_barrier((gathered, own, scalars))
+    decay, place, offset = scalars
     back = feed_forward(gathered, first_pair, first_back, False)
+    back, second_gain = lax.optimization_barrier((back, second_gain))
+    second_pair = paired_weights(second_gain, second_gate, second_up)
     own = advance(own, back, 0.5, BOTH)
     gathered = spread(own, BOTH).reshape(2, tp, tall, wide)
+    gathered, cosine, sine = lax.optimization_barrier((gathered, cosine, sine))
+    decay = jnp.broadcast_to(decay, (1, 2 * half))
     ret_out, new_state = retention(gathered, heads_pair, features, head_gain, ret_state, (cosine, sine, decay))
     back = jnp.dot(ret_out, w_out, preferred_element_type=jnp.float32).astype(jnp.bfloat16)
     back = back.reshape(groups, tall, across, wide).transpose(0, 2, 1, 3).reshape(tp, tall, wide)
@@ -291,7 +319,8 @@
     gathered = spread(own, BOTH).reshape(2, tp, tall, wide)
     own = lax.dynamic_slice(gathered, (p, place * across, offset, 0), (1, across, few, wide))[0]
     own = jnp.concatenate([own[i] for i in range(across)], axis=1)
-    gathered, own = lax.optimization_barrier((gathered, own))
+    gathered, own, scalars = lax.optimization_barrier((gathered, own, scalars))
+    decay, place, offset = scalars
     back = feed_forward(gathered, second_pair, second_back, True)
     return advance(own, back, 0.5, BOTH), new_state
 

time: 286 us -> 287 us (level)
  blocking collectives: 117 us -> 95.5 us
  starting transfers between devices: 94.8 us -> 107 us
  waiting for transfers between devices: 57.6 us -> 66.8 us
    all_to_all x6 -> x5, blocking collectives: 117 us -> 95.5 us  [exchange(): return lax.all_to_all(x, axis, split_axis=0, concat_axis=0, tiled=True)]
    all_to_all x6 -> x7, starting transfers between devices: 77.8 us -> 90 us  [exchange(): return lax.all_to_all(x, axis, split_axis=0, concat_axis=0, tiled=True)]
    all_to_all x6 -> x7, waiting for transfers between devices: 50 us -> 59.6 us  [exchange(): return lax.all_to_all(x, axis, split_axis=0, concat_axis=0, tiled=True)]
    ppermute x0 -> x2, starting transfers between devices: none -> 6.86 us  [paired_weights(): return (scaled(p, halves), lax.ppermute(sent, 'kvp', [(0, 1), (1, 0)]))]
    ppermute x5 -> x3, starting transfers between devices: 16.9 us -> 10.3 us  [swapped(): lax.ppermute(mine(both, 1 - p), 'kvp', [(0, 1), (1, 0)])]
    ppermute x5 -> x3, waiting for transfers between devices: 7.6 us -> 1.82 us  [swapped(): lax.ppermute(mine(both, 1 - p), 'kvp', [(0, 1), (1, 0)])]
    ppermute x0 -> x2, waiting for transfers between devices: none -> 5.33 us  [paired_weights(): return (scaled(p, halves), lax.ppermute(sent, 'kvp', [(0, 1), (1, 0)]))]
  transfers between devices with their start and end apart: 11 -> 12, of which waited for: 11 -> 11; matrix products, arithmetic and copies ran while one was open for 1% -> 1% of each run, Pallas kernels for 0% -> 0%
where the time goes in v8:
time: 287 us; the launch traced here: 286 us
  starting transfers between devices  107 us (37%)
  blocking collectives  95.5 us (33%)
  waiting for transfers between devices  66.8 us (23%)
  local copies, waits for them, and re-layouts  5.84 us (2%)
  Pallas kernels  5.21 us (2%)
  other arithmetic  4.24 us (1%)
    all_to_all x5, blocking collectives, exchange(): return lax.all_to_all(x, axis, split_axis=0, concat_axis=0, tiled=True)  95.5 us
    all_to_all x7, starting transfers between devices, exchange(): return lax.all_to_all(x, axis, split_axis=0, concat_axis=0, tiled=True)  90 us
    all_to_all x7, waiting for transfers between devices, exchange(): return lax.all_to_all(x, axis, split_axis=0, concat_axis=0, tiled=True)  59.6 us
    ppermute x3, starting transfers between devices, swapped(): lax.ppermute(mine(both, 1 - p), 'kvp', [(0, 1), (1, 0)])  10.3 us
    ppermute x2, starting transfers between devices, paired_weights(): return (scaled(p, halves), lax.ppermute(sent, 'kvp', [(0, 1), (1, 0)]))  6.86 us
  transfers between devices with their start and end apart: 12, of which 11 were waited for; matrix products, arithmetic and copies ran while one was open for 1% of the time, Pallas kernels for 0%

profile of v8, /device:TPU:65, one launch (start us, length us, event | category | flops | bytes accessed | tf_op | source)
XLA Modules:
  0.0 286.1 jit_solution(5763603152758218911)
XLA Ops:
  2.1 45.2 %all-to-all-start = ((bf16[32,24,128]{2,1,0:T(8,128)(2,1)}), bf16[32,24,128]{2,1,0:T(8,128)(2,1)S(1)}, u32[]{:S(2)}, u32[]{:S(2)}) async-start(bf16[32,24,128]{2,1,0:T(8,128)(2,1)} %broadcast_in_dim.12), calls=%async_computation | async-start | bytes 393216 | tf_op jit(solution)/shard_map/all_to_all | solution.py:33
  49.1 3.7 %collective-permute-start = (bf16[2,344,256]{2,1,0:T(8,128)(2,1)S(1)}, bf16[2,344,256]{2,1,0:T(8,128)(2,1)S(1)}, u32[]{:S(2)}, u32[]{:S(2)}) collective-permute-start(bf16[2,344,256]{2,1,0:T(8,128)(2,1)S(1)} %pad_maximum_fusion), channel_id=1, source_target_pairs={{0,16},{16,0},{1,17},{17,1},{2,18},{18,2},{3,19},{19,3},{4,20},{20... | collective-permute-start | bytes 1056776 | tf_op jit(solution)/shard_map/ppermute | solution.py:172
  53.1 4.3 %all-to-all-done = bf16[32,24,128]{2,1,0:T(8,128)(2,1)S(1)} async-done(((bf16[32,24,128]{2,1,0:T(8,128)(2,1)}), bf16[32,24,128]{2,1,0:T(8,128)(2,1)S(1)}, u32[]{:S(2)}, u32[]{:S(2)}) %all-to-all-start) | async-done | bytes 196640 | tf_op jit(solution)/shard_map/all_to_all | solution.py:33
  61.5 8.0 %all-to-all-start.1 = ((bf16[8,24,768]{2,1,0:T(8,128)(2,1)}), bf16[8,24,768]{2,1,0:T(8,128)(2,1)S(1)}, u32[]{:S(2)}, u32[]{:S(2)}) async-start(bf16[8,24,768]{2,1,0:T(8,128)(2,1)} %shard_map.185), calls=%async_computation.1 | async-start | bytes 589824 | tf_op jit(solution)/shard_map/all_to_all | solution.py:33
  69.5 3.6 %collective-permute-start.1 = (bf16[344,256]{1,0:T(8,128)(2,1)S(1)}, bf16[344,256]{1,0:T(8,128)(2,1)S(1)}, u32[]{:S(2)}, u32[]{:S(2)}) collective-permute-start(bf16[344,256]{1,0:T(8,128)(2,1)S(1)} %get-tuple-element.58), channel_id=1, source_target_pairs={{0,16},{16,0},{1,17},{17,1},{2,18},{18,2},{3,19},{19,3},{4,20},{20... | collective-permute-start | bytes 528392 | tf_op jit(solution)/shard_map/ppermute | solution.py:160
  73.1 13.4 %all-to-all-done.1 = bf16[8,24,768]{2,1,0:T(8,128)(2,1)S(1)} async-done(((bf16[8,24,768]{2,1,0:T(8,128)(2,1)}), bf16[8,24,768]{2,1,0:T(8,128)(2,1)S(1)}, u32[]{:S(2)}, u32[]{:S(2)}) %all-to-all-start.1) | async-done | bytes 294944 | tf_op jit(solution)/shard_map/all_to_all | solution.py:33
  87.7 23.7 %all_to_all.60.h_ref = bf16[8,24,344]{2,1,0:T(8,128)(2,1)S(1)} all-to-all(bf16[8,24,344]{2,1,0:T(8,128)(2,1)S(1)} %broadcast_in_dim.13), channel_id=1, replica_groups=mesh['grp'=2,'kvh'=8,'kvp'=2,'tp'=16] {'kvh'}, dimensions={0} | all-to-all | bytes 264192 | tf_op jit(solution)/shard_map/all_to_all | solution.py:33
  112.3 12.4 %all-to-all-start.3 = ((bf16[32,24,128]{2,1,0:T(8,128)(2,1)}), bf16[32,24,128]{2,1,0:T(8,128)(2,1)S(1)}, u32[]{:S(2)}, u32[]{:S(2)}) async-start(bf16[32,24,128]{2,1,0:T(8,128)(2,1)} %bitcast.8), calls=%async_computation.3 | async-start | bytes 393216 | tf_op jit(solution)/shard_map/all_to_all | solution.py:33
  124.9 9.7 %all-to-all-done.3 = bf16[32,24,128]{2,1,0:T(8,128)(2,1)S(1)} async-done(((bf16[32,24,128]{2,1,0:T(8,128)(2,1)}), bf16[32,24,128]{2,1,0:T(8,128)(2,1)S(1)}, u32[]{:S(2)}, u32[]{:S(2)}) %all-to-all-start.3) | async-done | bytes 196640 | tf_op jit(solution)/shard_map/all_to_all | solution.py:33
  135.3 4.4 %all-to-all-start.4 = ((bf16[32,24,128]{2,1,0:T(8,128)(2,1)}), bf16[32,24,128]{2,1,0:T(8,128)(2,1)S(1)}, u32[]{:S(2)}, u32[]{:S(2)}) async-start(bf16[32,24,128]{2,1,0:T(8,128)(2,1)} %broadcast_in_dim.14), calls=%async_computation.4 | async-start | bytes 393216 | tf_op jit(solution)/shard_map/all_to_all | solution.py:33
  140.6 3.4 %collective-permute-start.2 = (bf16[256,256]{1,0:T(8,128)(2,1)S(1)}, bf16[256,256]{1,0:T(8,128)(2,1)S(1)}, u32[]{:S(2)}, u32[]{:S(2)}) collective-permute-start(bf16[256,256]{1,0:T(8,128)(2,1)S(1)} %get-tuple-element.60), channel_id=1, source_target_pairs={{0,16},{16,0},{1,17},{17,1},{2,18},{18,2},{3,19},{19,3},{4,20},{20... | collective-permute-start | bytes 393224 | tf_op jit(solution)/shard_map/ppermute | solution.py:160
  144.2 5.2 %all-to-all-done.4 = bf16[32,24,128]{2,1,0:T(8,128)(2,1)S(1)} async-done(((bf16[32,24,128]{2,1,0:T(8,128)(2,1)}), bf16[32,24,128]{2,1,0:T(8,128)(2,1)S(1)}, u32[]{:S(2)}, u32[]{:S(2)}) %all-to-all-start.4) | async-done | bytes 196640 | tf_op jit(solution)/shard_map/all_to_all | solution.py:33
  149.7 14.8 %all_to_all.61.z_ref = bf16[16,16,256]{2,1,0:T(8,128)(2,1)S(1)} all-to-all(bf16[16,16,256]{2,1,0:T(8,128)(2,1)S(1)} %shard_map.187), channel_id=1, replica_groups=mesh['grp'=2,'kvh'=8,'kvp'=2,'tp'=16] {'kvh','kvp'}, dimensions={0} | all-to-all | bytes 262144 | tf_op jit(solution)/shard_map/all_to_all | solution.py:33
  165.9 17.7 %all_to_all.62 = bf16[16,12,128]{2,1,0:T(8,128)(2,1)S(1)} all-to-all(bf16[16,12,128]{2,1,0:T(8,128)(2,1)S(1)} %get-tuple-element.42), channel_id=1, replica_groups=mesh['grp'=2,'kvh'=8,'kvp'=2,'tp'=16] {'kvh','kvp'}, dimensions={0} | all-to-all | bytes 98304 | tf_op jit(solution)/shard_map/all_to_all | solution.py:33
  183.8 15.4 %all_to_all.63 = bf16[16,24,128]{2,1,0:T(8,128)(2,1)S(1)} all-to-all(bf16[16,24,128]{2,1,0:T(8,128)(2,1)S(1)} %bitcast.53), channel_id=1, replica_groups=mesh['grp'=2,'kvh'=8,'kvp'=2,'tp'=16] {'tp'}, dimensions={0} | all-to-all | bytes 196608 | tf_op jit(solution)/shard_map/all_to_all | solution.py:33
  199.9 4.2 %all-to-all-start.8 = ((bf16[32,24,128]{2,1,0:T(8,128)(2,1)}), bf16[32,24,128]{2,1,0:T(8,128)(2,1)S(1)}, u32[]{:S(2)}, u32[]{:S(2)}) async-start(bf16[32,24,128]{2,1,0:T(8,128)(2,1)} %broadcast_in_dim.16), calls=%async_computation.8 | async-start | bytes 393216 | tf_op jit(solution)/shard_map/all_to_all | solution.py:33
  204.9 3.1 %collective-permute-start.3 = (bf16[2,344,256]{2,1,0:T(8,128)(2,1)S(1)}, bf16[2,344,256]{2,1,0:T(8,128)(2,1)S(1)}, u32[]{:S(2)}, u32[]{:S(2)}) collective-permute-start(bf16[2,344,256]{2,1,0:T(8,128)(2,1)S(1)} %pad_maximum_fusion.2), channel_id=1, source_target_pairs={{0,16},{16,0},{1,17},{17,1},{2,18},{18,2},{3,19},{19,3},{4,20},{20... | collective-permute-start | bytes 1056776 | tf_op jit(solution)/shard_map/ppermute | solution.py:172
  208.2 5.5 %all-to-all-done.8 = bf16[32,24,128]{2,1,0:T(8,128)(2,1)S(1)} async-done(((bf16[32,24,128]{2,1,0:T(8,128)(2,1)}), bf16[32,24,128]{2,1,0:T(8,128)(2,1)S(1)}, u32[]{:S(2)}, u32[]{:S(2)}) %all-to-all-start.8) | async-done | bytes 196640 | tf_op jit(solution)/shard_map/all_to_all | solution.py:33
  217.3 3.8 %all-to-all-start.9 = ((bf16[8,24,768]{2,1,0:T(8,128)(2,1)}), bf16[8,24,768]{2,1,0:T(8,128)(2,1)S(1)}, u32[]{:S(2)}, u32[]{:S(2)}) async-start(bf16[8,24,768]{2,1,0:T(8,128)(2,1)} %shard_map.189), calls=%async_computation.9 | async-start | bytes 589824 | tf_op jit(solution)/shard_map/all_to_all | solution.py:33
  221.1 3.3 %collective-permute-start.4 = (bf16[344,256]{1,0:T(8,128)(2,1)S(1)}, bf16[344,256]{1,0:T(8,128)(2,1)S(1)}, u32[]{:S(2)}, u32[]{:S(2)}) collective-permute-start(bf16[344,256]{1,0:T(8,128)(2,1)S(1)} %get-tuple-element.56), channel_id=1, source_target_pairs={{0,16},{16,0},{1,17},{17,1},{2,18},{18,2},{3,19},{19,3},{4,20},{20... | collective-permute-start | bytes 528392 | tf_op jit(solution)/shard_map/ppermute | solution.py:160
  224.4 13.0 %all-to-all-done.9 = bf16[8,24,768]{2,1,0:T(8,128)(2,1)S(1)} async-done(((bf16[8,24,768]{2,1,0:T(8,128)(2,1)}), bf16[8,24,768]{2,1,0:T(8,128)(2,1)S(1)}, u32[]{:S(2)}, u32[]{:S(2)}) %all-to-all-start.9) | async-done | bytes 294944 | tf_op jit(solution)/shard_map/all_to_all | solution.py:33
  238.7 23.9 %all_to_all.64.h_ref = bf16[8,24,344]{2,1,0:T(8,128)(2,1)S(1)} all-to-all(bf16[8,24,344]{2,1,0:T(8,128)(2,1)S(1)} %broadcast_in_dim.17), channel_id=1, replica_groups=mesh['grp'=2,'kvh'=8,'kvp'=2,'tp'=16] {'kvh'}, dimensions={0} | all-to-all | bytes 264192 | tf_op jit(solution)/shard_map/all_to_all | solution.py:33
  263.6 12.1 %all-to-all-start.11 = ((bf16[32,24,128]{2,1,0:T(8,128)(2,1)}), bf16[32,24,128]{2,1,0:T(8,128)(2,1)S(1)}, u32[]{:S(2)}, u32[]{:S(2)}) async-start(bf16[32,24,128]{2,1,0:T(8,128)(2,1)} %bitcast.28), calls=%async_computation.11 | async-start | bytes 393216 | tf_op jit(solution)/shard_map/all_to_all | solution.py:33
  276.9 8.6 %all-to-all-done.11 = bf16[32,24,128]{2,1,0:T(8,128)(2,1)S(1)} async-done(((bf16[32,24,128]{2,1,0:T(8,128)(2,1)}), bf16[32,24,128]{2,1,0:T(8,128)(2,1)S(1)}, u32[]{:S(2)}, u32[]{:S(2)}) %all-to-all-start.11) | async-done | bytes 196640 | tf_op jit(solution)/shard_map/all_to_all | solution.py:33
  (92 shorter events, 22.6 us)
Async XLA Ops:
  0.6 183.0 %copy-start = (bf16[128,256]{1,0:T(8,128)(2,1)S(1)}, bf16[128,256]{1,0:T(8,128)(2,1)}, u32[]{:S(2)}) copy-start(bf16[128,256]{1,0:T(8,128)(2,1)} %param.30) | copy-start | bytes 196612
  0.6 46.7 %copy-start.5 = (bf16[256,688]{0,1:T(8,128)(2,1)S(1)}, bf16[256,688]{0,1:T(8,128)(2,1)}, u32[]{:S(2)}) copy-start(bf16[256,688]{0,1:T(8,128)(2,1)} %param.22) | copy-start | bytes 1056772
  2.1 55.2 %all-to-all-start = ((bf16[32,24,128]{2,1,0:T(8,128)(2,1)}), bf16[32,24,128]{2,1,0:T(8,128)(2,1)S(1)}, u32[]{:S(2)}, u32[]{:S(2)}) async-start(bf16[32,24,128]{2,1,0:T(8,128)(2,1)} %broadcast_in_dim.12), calls=%async_computation | async-start | bytes 393216 | tf_op jit(solution)/shard_map/all_to_all | solution.py:33
  49.0 3.9 %copy-start.6 = (bf16[256,688]{0,1:T(8,128)(2,1)S(1)}, bf16[256,688]{0,1:T(8,128)(2,1)}, u32[]{:S(2)}) copy-start(bf16[256,688]{0,1:T(8,128)(2,1)} %param.23) | copy-start | bytes 1056772
  49.1 11.2 %collective-permute-start = (bf16[2,344,256]{2,1,0:T(8,128)(2,1)S(1)}, bf16[2,344,256]{2,1,0:T(8,128)(2,1)S(1)}, u32[]{:S(2)}, u32[]{:S(2)}) collective-permute-start(bf16[2,344,256]{2,1,0:T(8,128)(2,1)S(1)} %pad_maximum_fusion), channel_id=1, source_target_pairs={{0,16},{16,0},{1,17},{17,1},{2,18},{18,2},{3,19},{19,3},{4,20},{20... | collective-permute-start | bytes 1056776 | tf_op jit(solution)/shard_map/ppermute | solution.py:172
  61.5 8.0 %copy-start.3 = (bf16[688,256]{1,0:T(8,128)(2,1)S(1)}, bf16[688,256]{1,0:T(8,128)(2,1)}, u32[]{:S(2)}) copy-start(bf16[688,256]{1,0:T(8,128)(2,1)} %param.24) | copy-start | bytes 1056772
  61.5 25.0 %all-to-all-start.1 = ((bf16[8,24,768]{2,1,0:T(8,128)(2,1)}), bf16[8,24,768]{2,1,0:T(8,128)(2,1)S(1)}, u32[]{:S(2)}, u32[]{:S(2)}) async-start(bf16[8,24,768]{2,1,0:T(8,128)(2,1)} %shard_map.185), calls=%async_computation.1 | async-start | bytes 589824 | tf_op jit(solution)/shard_map/all_to_all | solution.py:33
  69.5 18.2 %collective-permute-start.1 = (bf16[344,256]{1,0:T(8,128)(2,1)S(1)}, bf16[344,256]{1,0:T(8,128)(2,1)S(1)}, u32[]{:S(2)}, u32[]{:S(2)}) collective-permute-start(bf16[344,256]{1,0:T(8,128)(2,1)S(1)} %get-tuple-element.58), channel_id=1, source_target_pairs={{0,16},{16,0},{1,17},{17,1},{2,18},{18,2},{3,19},{19,3},{4,20},{20... | collective-permute-start | bytes 528392 | tf_op jit(solution)/shard_map/ppermute | solution.py:160
  112.3 12.5 %copy-start.9 = (bf16[256,128]{1,0:T(8,128)(2,1)S(1)}, bf16[256,128]{1,0:T(8,128)(2,1)}, u32[]{:S(2)}) copy-start(bf16[256,128]{1,0:T(8,128)(2,1)} %param.27) | copy-start | bytes 196612
  112.3 12.5 %copy-start.10 = (bf16[256,128]{1,0:T(8,128)(2,1)S(1)}, bf16[256,128]{1,0:T(8,128)(2,1)}, u32[]{:S(2)}) copy-start(bf16[256,128]{1,0:T(8,128)(2,1)} %param.26) | copy-start | bytes 196612
  112.3 12.5 %copy-start.11 = (bf16[256,128]{1,0:T(8,128)(2,1)S(1)}, bf16[256,128]{1,0:T(8,128)(2,1)}, u32[]{:S(2)}) copy-start(bf16[256,128]{1,0:T(8,128)(2,1)} %param.29) | copy-start | bytes 196612
  112.3 12.5 %copy-start.12 = (bf16[256,128]{1,0:T(8,128)(2,1)S(1)}, bf16[256,128]{1,0:T(8,128)(2,1)}, u32[]{:S(2)}) copy-start(bf16[256,128]{1,0:T(8,128)(2,1)} %param.28) | copy-start | bytes 196612
  112.3 22.2 %all-to-all-start.3 = ((bf16[32,24,128]{2,1,0:T(8,128)(2,1)}), bf16[32,24,128]{2,1,0:T(8,128)(2,1)S(1)}, u32[]{:S(2)}, u32[]{:S(2)}) async-start(bf16[32,24,128]{2,1,0:T(8,128)(2,1)} %bitcast.8), calls=%async_computation.3 | async-start | bytes 393216 | tf_op jit(solution)/shard_map/all_to_all | solution.py:33
  135.3 14.2 %all-to-all-start.4 = ((bf16[32,24,128]{2,1,0:T(8,128)(2,1)}), bf16[32,24,128]{2,1,0:T(8,128)(2,1)S(1)}, u32[]{:S(2)}, u32[]{:S(2)}) async-start(bf16[32,24,128]{2,1,0:T(8,128)(2,1)} %broadcast_in_dim.14), calls=%async_computation.4 | async-start | bytes 393216 | tf_op jit(solution)/shard_map/all_to_all | solution.py:33
  140.5 24.0 %copy-start.1 = (f32[12,1,128,128]{3,2,1,0:T(8,128)S(1)}, f32[12,1,128,128]{3,2,1,0:T(8,128)}, u32[]{:S(2)}) copy-start(f32[12,1,128,128]{3,2,1,0:T(8,128)} %param.20) | copy-start | bytes 2359300
  140.6 8.9 %collective-permute-start.2 = (bf16[256,256]{1,0:T(8,128)(2,1)S(1)}, bf16[256,256]{1,0:T(8,128)(2,1)S(1)}, u32[]{:S(2)}, u32[]{:S(2)}) collective-permute-start(bf16[256,256]{1,0:T(8,128)(2,1)S(1)} %get-tuple-element.60), channel_id=1, source_target_pairs={{0,16},{16,0},{1,17},{17,1},{2,18},{18,2},{3,19},{19,3},{4,20},{20... | collective-permute-start | bytes 393224 | tf_op jit(solution)/shard_map/ppermute | solution.py:160
  199.2 5.0 %copy-start.7 = (bf16[256,688]{0,1:T(8,128)(2,1)S(1)}, bf16[256,688]{0,1:T(8,128)(2,1)}, u32[]{:S(2)}) copy-start(bf16[256,688]{0,1:T(8,128)(2,1)} %param.33) | copy-start | bytes 1056772
  199.2 5.0 %copy-start.8 = (bf16[256,688]{0,1:T(8,128)(2,1)S(1)}, bf16[256,688]{0,1:T(8,128)(2,1)}, u32[]{:S(2)}) copy-start(bf16[256,688]{0,1:T(8,128)(2,1)} %param.34) | copy-start | bytes 1056772
  199.9 13.7 %all-to-all-start.8 = ((bf16[32,24,128]{2,1,0:T(8,128)(2,1)}), bf16[32,24,128]{2,1,0:T(8,128)(2,1)S(1)}, u32[]{:S(2)}, u32[]{:S(2)}) async-start(bf16[32,24,128]{2,1,0:T(8,128)(2,1)} %broadcast_in_dim.16), calls=%async_computation.8 | async-start | bytes 393216 | tf_op jit(solution)/shard_map/all_to_all | solution.py:33
  204.9 11.2 %collective-permute-start.3 = (bf16[2,344,256]{2,1,0:T(8,128)(2,1)S(1)}, bf16[2,344,256]{2,1,0:T(8,128)(2,1)S(1)}, u32[]{:S(2)}, u32[]{:S(2)}) collective-permute-start(bf16[2,344,256]{2,1,0:T(8,128)(2,1)S(1)} %pad_maximum_fusion.2), channel_id=1, source_target_pairs={{0,16},{16,0},{1,17},{17,1},{2,18},{18,2},{3,19},{19,3},{4,20},{20... | collective-permute-start | bytes 1056776 | tf_op jit(solution)/shard_map/ppermute | solution.py:172
  217.3 3.8 %copy-start.4 = (bf16[688,256]{1,0:T(8,128)(2,1)S(1)}, bf16[688,256]{1,0:T(8,128)(2,1)}, u32[]{:S(2)}) copy-start(bf16[688,256]{1,0:T(8,128)(2,1)} %param.35) | copy-start | bytes 1056772
  217.3 20.1 %all-to-all-start.9 = ((bf16[8,24,768]{2,1,0:T(8,128)(2,1)}), bf16[8,24,768]{2,1,0:T(8,128)(2,1)S(1)}, u32[]{:S(2)}, u32[]{:S(2)}) async-start(bf16[8,24,768]{2,1,0:T(8,128)(2,1)} %shard_map.189), calls=%async_computation.9 | async-start | bytes 589824 | tf_op jit(solution)/shard_map/all_to_all | solution.py:33
  221.1 17.6 %collective-permute-start.4 = (bf16[344,256]{1,0:T(8,128)(2,1)S(1)}, bf16[344,256]{1,0:T(8,128)(2,1)S(1)}, u32[]{:S(2)}, u32[]{:S(2)}) collective-permute-start(bf16[344,256]{1,0:T(8,128)(2,1)S(1)} %get-tuple-element.56), channel_id=1, source_target_pairs={{0,16},{16,0},{1,17},{17,1},{2,18},{18,2},{3,19},{19,3},{4,20},{20... | collective-permute-start | bytes 528392 | tf_op jit(solution)/shard_map/ppermute | solution.py:160
  263.6 21.8 %all-to-all-start.11 = ((bf16[32,24,128]{2,1,0:T(8,128)(2,1)}), bf16[32,24,128]{2,1,0:T(8,128)(2,1)S(1)}, u32[]{:S(2)}, u32[]{:S(2)}) async-start(bf16[32,24,128]{2,1,0:T(8,128)(2,1)} %bitcast.28), calls=%async_computation.11 | async-start | bytes 393216 | tf_op jit(solution)/shard_map/all_to_all | solution.py:33
  (5 other events, 6.3 us)

commit v9 on v8

--- a/solution.py
+++ b/solution.py
@@ -287,11 +287,9 @@
     half = ret_state.shape[-1] // 2
     inverse = 10000.0 ** (-jnp.arange(half, dtype=jnp.float32) / half)
     angles = positions.astype(jnp.float32)[:, None] * inverse[None, :]
-    cosine, sine = jnp.cos(angles), jnp.sin(angles)
-    cosine, sine = jnp.concatenate([cosine, cosine], axis=1), jnp.concatenate([-sine, sine], axis=1)
     decay = jnp.exp(jnp.log1p(-(2.0 ** (-5.0 - t.astype(jnp.float32)))))
     place = lax.div(t * few, tall)
-    scalars = (decay, place, t * few - place * tall)
+    early = (angles, decay, place, t * few - place * tall)
 
     first_pair = paired_weights(first_gain, first_gate, first_up)
     first_back = paired_rows(first_down)
@@ -303,13 +301,15 @@
     cuts = jnp.concatenate(jnp.split(stream_in, across, axis=1), axis=0)
     gathered = spread(cuts, BOTH).reshape(2, tp, tall, wide)
     own = lax.dynamic_slice(gathered, (p, r * across, c * few, 0), (1, across, few, wide)).reshape(tall, wide)
-    gathered, own, scalars = lax.optimization_barrier((gathered, own, scalars))
-    decay, place, offset = scalars
+    gathered, own, early = lax.optimization_barrier((gathered, own, early))
+    angles, decay, place, offset = early
     back = feed_forward(gathered, first_pair, first_back, False)
     back, second_gain = lax.optimization_barrier((back, second_gain))
     second_pair = paired_weights(second_gain, second_gate, second_up)
     own = advance(own, back, 0.5, BOTH)
     gathered = spread(own, BOTH).reshape(2, tp, tall, wide)
+    cosine, sine = jnp.cos(angles), jnp.sin(angles)
+    cosine, sine = jnp.concatenate([cosine, cosine], axis=1), jnp.concatenate([-sine, sine], axis=1)
     gathered, cosine, sine = lax.optimization_barrier((gathered, cosine, sine))
     decay = jnp.broadcast_to(decay, (1, 2 * half))
     ret_out, new_state = retention(gathered, heads_pair, features, head_gain, ret_state, (cosine, sine, decay))
@@ -319,8 +319,8 @@
     gathered = spread(own, BOTH).reshape(2, tp, tall, wide)
     own = lax.dynamic_slice(gathered, (p, place * across, offset, 0), (1, across, few, wide))[0]
     own = jnp.concatenate([own[i] for i in range(across)], axis=1)
-    gathered, own, scalars = lax.optimization_barrier((gathered, own, scalars))
-    decay, place, offset = scalars
+    gathered, own, early = lax.optimization_barrier((gathered, own, early))
+    angles, decay, place, offset = early
     back = feed_forward(gathered, second_pair, second_back, True)
     return advance(own, back, 0.5, BOTH), new_state
 

time: 287 us -> 286 us (level)
  blocking collectives: 95.5 us -> 117 us
  starting transfers between devices: 107 us -> 94.9 us
  waiting for transfers between devices: 66.8 us -> 56.4 us
    all_to_all x5 -> x6, blocking collectives: 95.5 us -> 117 us  [exchange(): return lax.all_to_all(x, axis, split_axis=0, concat_axis=0, tiled=True)]
    all_to_all x7 -> x6, starting transfers between devices: 90 us -> 77.7 us  [exchange(): return lax.all_to_all(x, axis, split_axis=0, concat_axis=0, tiled=True)]
    all_to_all x7 -> x6, waiting for transfers between devices: 59.6 us -> 49.2 us  [exchange(): return lax.all_to_all(x, axis, split_axis=0, concat_axis=0, tiled=True)]
  transfers between devices with their start and end apart: 12 -> 11, of which waited for: 11 -> 10; matrix products, arithmetic and copies ran while one was open for 1% -> 1% of each run, Pallas kernels for 0% -> 0%
where the time goes in v9:
time: 286 us; the launch traced here: 285 us
  blocking collectives  117 us (41%)
  starting transfers between devices  94.9 us (33%)
  waiting for transfers between devices  56.4 us (20%)
  local copies, waits for them, and re-layouts  6.54 us (2%)
  Pallas kernels  4.53 us (2%)
  other arithmetic  4.2 us (1%)
    all_to_all x6, blocking collectives, exchange(): return lax.all_to_all(x, axis, split_axis=0, concat_axis=0, tiled=True)  117 us
    all_to_all x6, starting transfers between devices, exchange(): return lax.all_to_all(x, axis, split_axis=0, concat_axis=0, tiled=True)  77.7 us
    all_to_all x6, waiting for transfers between devices, exchange(): return lax.all_to_all(x, axis, split_axis=0, concat_axis=0, tiled=True)  49.2 us
    ppermute x3, starting transfers between devices, swapped(): lax.ppermute(mine(both, 1 - p), 'kvp', [(0, 1), (1, 0)])  10.3 us
    ppermute x2, starting transfers between devices, paired_weights(): return (scaled(p, halves), lax.ppermute(sent, 'kvp', [(0, 1), (1, 0)]))  6.86 us
  transfers between devices with their start and end apart: 11, of which 10 were waited for; matrix products, arithmetic and copies ran while one was open for 1% of the time, Pallas kernels for 0%

profile of v9, /device:TPU:65, one launch (start us, length us, event | category | flops | bytes accessed | tf_op | source)
XLA Modules:
  0.0 285.3 jit_solution(9057411688126973252)
XLA Ops:
  2.1 45.2 %all-to-all-start = ((bf16[32,24,128]{2,1,0:T(8,128)(2,1)}), bf16[32,24,128]{2,1,0:T(8,128)(2,1)S(1)}, u32[]{:S(2)}, u32[]{:S(2)}) async-start(bf16[32,24,128]{2,1,0:T(8,128)(2,1)} %broadcast_in_dim.12), calls=%async_computation | async-start | bytes 393216 | tf_op jit(solution)/shard_map/all_to_all | solution.py:33
  49.1 3.7 %collective-permute-start = (bf16[2,344,256]{2,1,0:T(8,128)(2,1)S(1)}, bf16[2,344,256]{2,1,0:T(8,128)(2,1)S(1)}, u32[]{:S(2)}, u32[]{:S(2)}) collective-permute-start(bf16[2,344,256]{2,1,0:T(8,128)(2,1)S(1)} %pad_maximum_fusion), channel_id=1, source_target_pairs={{0,16},{16,0},{1,17},{17,1},{2,18},{18,2},{3,19},{19,3},{4,20},{20... | collective-permute-start | bytes 1056776 | tf_op jit(solution)/shard_map/ppermute | solution.py:172
  53.8 3.5 %all-to-all-done = bf16[32,24,128]{2,1,0:T(8,128)(2,1)S(1)} async-done(((bf16[32,24,128]{2,1,0:T(8,128)(2,1)}), bf16[32,24,128]{2,1,0:T(8,128)(2,1)S(1)}, u32[]{:S(2)}, u32[]{:S(2)}) %all-to-all-start) | async-done | bytes 196640 | tf_op jit(solution)/shard_map/all_to_all | solution.py:33
  57.4 2.9 %collective-permute-done.got_ref = bf16[2,344,256]{2,1,0:T(8,128)(2,1)S(1)} collective-permute-done((bf16[2,344,256]{2,1,0:T(8,128)(2,1)S(1)}, bf16[2,344,256]{2,1,0:T(8,128)(2,1)S(1)}, u32[]{:S(2)}, u32[]{:S(2)}) %collective-permute-start) | collective-permute-done | bytes 352288 | tf_op jit(solution)/shard_map/ppermute | solution.py:172
  61.5 8.0 %all-to-all-start.1 = ((bf16[8,24,768]{2,1,0:T(8,128)(2,1)}), bf16[8,24,768]{2,1,0:T(8,128)(2,1)S(1)}, u32[]{:S(2)}, u32[]{:S(2)}) async-start(bf16[8,24,768]{2,1,0:T(8,128)(2,1)} %shard_map.185), calls=%async_computation.1 | async-start | bytes 589824 | tf_op jit(solution)/shard_map/all_to_all | solution.py:33
  69.5 3.6 %collective-permute-start.1 = (bf16[344,256]{1,0:T(8,128)(2,1)S(1)}, bf16[344,256]{1,0:T(8,128)(2,1)S(1)}, u32[]{:S(2)}, u32[]{:S(2)}) collective-permute-start(bf16[344,256]{1,0:T(8,128)(2,1)S(1)} %get-tuple-element.60), channel_id=1, source_target_pairs={{0,16},{16,0},{1,17},{17,1},{2,18},{18,2},{3,19},{19,3},{4,20},{20... | collective-permute-start | bytes 528392 | tf_op jit(solution)/shard_map/ppermute | solution.py:160
  73.1 13.4 %all-to-all-done.1 = bf16[8,24,768]{2,1,0:T(8,128)(2,1)S(1)} async-done(((bf16[8,24,768]{2,1,0:T(8,128)(2,1)}), bf16[8,24,768]{2,1,0:T(8,128)(2,1)S(1)}, u32[]{:S(2)}, u32[]{:S(2)}) %all-to-all-start.1) | async-done | bytes 294944 | tf_op jit(solution)/shard_map/all_to_all | solution.py:33
  87.7 23.7 %all_to_all.60.h_ref = bf16[8,24,344]{2,1,0:T(8,128)(2,1)S(1)} all-to-all(bf16[8,24,344]{2,1,0:T(8,128)(2,1)S(1)} %broadcast_in_dim.13), channel_id=1, replica_groups=mesh['grp'=2,'kvh'=8,'kvp'=2,'tp'=16] {'kvh'}, dimensions={0} | all-to-all | bytes 264192 | tf_op jit(solution)/shard_map/all_to_all | solution.py:33
  111.7 21.8 %all_to_all.61 = bf16[32,24,128]{2,1,0:T(8,128)(2,1)S(1)} all-to-all(bf16[32,24,128]{2,1,0:T(8,128)(2,1)S(1)} %bitcast.52), channel_id=1, replica_groups=mesh['grp'=2,'kvh'=8,'kvp'=2,'tp'=16] {'kvp','tp'}, dimensions={0} | all-to-all | bytes 393216 | tf_op jit(solution)/shard_map/all_to_all | solution.py:33
  134.3 4.6 %all-to-all-start.4 = ((bf16[32,24,128]{2,1,0:T(8,128)(2,1)}), bf16[32,24,128]{2,1,0:T(8,128)(2,1)S(1)}, u32[]{:S(2)}, u32[]{:S(2)}) async-start(bf16[32,24,128]{2,1,0:T(8,128)(2,1)} %broadcast_in_dim.14), calls=%async_computation.4 | async-start | bytes 393216 | tf_op jit(solution)/shard_map/all_to_all | solution.py:33
  139.8 3.4 %collective-permute-start.2 = (bf16[256,256]{1,0:T(8,128)(2,1)S(1)}, bf16[256,256]{1,0:T(8,128)(2,1)S(1)}, u32[]{:S(2)}, u32[]{:S(2)}) collective-permute-start(bf16[256,256]{1,0:T(8,128)(2,1)S(1)} %get-tuple-element.62), channel_id=1, source_target_pairs={{0,16},{16,0},{1,17},{17,1},{2,18},{18,2},{3,19},{19,3},{4,20},{20... | collective-permute-start | bytes 393224 | tf_op jit(solution)/shard_map/ppermute | solution.py:160
  143.3 5.2 %all-to-all-done.4 = bf16[32,24,128]{2,1,0:T(8,128)(2,1)S(1)} async-done(((bf16[32,24,128]{2,1,0:T(8,128)(2,1)}), bf16[32,24,128]{2,1,0:T(8,128)(2,1)S(1)}, u32[]{:S(2)}, u32[]{:S(2)}) %all-to-all-start.4) | async-done | bytes 196640 | tf_op jit(solution)/shard_map/all_to_all | solution.py:33
  148.8 14.8 %all_to_all.62.z_ref = bf16[16,16,256]{2,1,0:T(8,128)(2,1)S(1)} all-to-all(bf16[16,16,256]{2,1,0:T(8,128)(2,1)S(1)} %shard_map.187), channel_id=1, replica_groups=mesh['grp'=2,'kvh'=8,'kvp'=2,'tp'=16] {'kvh','kvp'}, dimensions={0} | all-to-all | bytes 262144 | tf_op jit(solution)/shard_map/all_to_all | solution.py:33
  165.0 17.7 %all_to_all.63 = bf16[16,12,128]{2,1,0:T(8,128)(2,1)S(1)} all-to-all(bf16[16,12,128]{2,1,0:T(8,128)(2,1)S(1)} %get-tuple-element.44), channel_id=1, replica_groups=mesh['grp'=2,'kvh'=8,'kvp'=2,'tp'=16] {'kvh','kvp'}, dimensions={0} | all-to-all | bytes 98304 | tf_op jit(solution)/shard_map/all_to_all | solution.py:33
  183.0 15.4 %all_to_all.64 = bf16[16,24,128]{2,1,0:T(8,128)(2,1)S(1)} all-to-all(bf16[16,24,128]{2,1,0:T(8,128)(2,1)S(1)} %bitcast.54), channel_id=1, replica_groups=mesh['grp'=2,'kvh'=8,'kvp'=2,'tp'=16] {'tp'}, dimensions={0} | all-to-all | bytes 196608 | tf_op jit(solution)/shard_map/all_to_all | solution.py:33
  199.1 4.2 %all-to-all-start.8 = ((bf16[32,24,128]{2,1,0:T(8,128)(2,1)}), bf16[32,24,128]{2,1,0:T(8,128)(2,1)S(1)}, u32[]{:S(2)}, u32[]{:S(2)}) async-start(bf16[32,24,128]{2,1,0:T(8,128)(2,1)} %broadcast_in_dim.16), calls=%async_computation.8 | async-start | bytes 393216 | tf_op jit(solution)/shard_map/all_to_all | solution.py:33
  204.1 3.1 %collective-permute-start.3 = (bf16[2,344,256]{2,1,0:T(8,128)(2,1)S(1)}, bf16[2,344,256]{2,1,0:T(8,128)(2,1)S(1)}, u32[]{:S(2)}, u32[]{:S(2)}) collective-permute-start(bf16[2,344,256]{2,1,0:T(8,128)(2,1)S(1)} %pad_maximum_fusion.2), channel_id=1, source_target_pairs={{0,16},{16,0},{1,17},{17,1},{2,18},{18,2},{3,19},{19,3},{4,20},{20... | collective-permute-start | bytes 1056776 | tf_op jit(solution)/shard_map/ppermute | solution.py:172
  207.4 5.5 %all-to-all-done.8 = bf16[32,24,128]{2,1,0:T(8,128)(2,1)S(1)} async-done(((bf16[32,24,128]{2,1,0:T(8,128)(2,1)}), bf16[32,24,128]{2,1,0:T(8,128)(2,1)S(1)}, u32[]{:S(2)}, u32[]{:S(2)}) %all-to-all-start.8) | async-done | bytes 196640 | tf_op jit(solution)/shard_map/all_to_all | solution.py:33
  216.5 3.8 %all-to-all-start.9 = ((bf16[8,24,768]{2,1,0:T(8,128)(2,1)}), bf16[8,24,768]{2,1,0:T(8,128)(2,1)S(1)}, u32[]{:S(2)}, u32[]{:S(2)}) async-start(bf16[8,24,768]{2,1,0:T(8,128)(2,1)} %shard_map.189), calls=%async_computation.9 | async-start | bytes 589824 | tf_op jit(solution)/shard_map/all_to_all | solution.py:33
  220.3 3.3 %collective-permute-start.4 = (bf16[344,256]{1,0:T(8,128)(2,1)S(1)}, bf16[344,256]{1,0:T(8,128)(2,1)S(1)}, u32[]{:S(2)}, u32[]{:S(2)}) collective-permute-start(bf16[344,256]{1,0:T(8,128)(2,1)S(1)} %get-tuple-element.58), channel_id=1, source_target_pairs={{0,16},{16,0},{1,17},{17,1},{2,18},{18,2},{3,19},{19,3},{4,20},{20... | collective-permute-start | bytes 528392 | tf_op jit(solution)/shard_map/ppermute | solution.py:160
  223.6 13.0 %all-to-all-done.9 = bf16[8,24,768]{2,1,0:T(8,128)(2,1)S(1)} async-done(((bf16[8,24,768]{2,1,0:T(8,128)(2,1)}), bf16[8,24,768]{2,1,0:T(8,128)(2,1)S(1)}, u32[]{:S(2)}, u32[]{:S(2)}) %all-to-all-start.9) | async-done | bytes 294944 | tf_op jit(solution)/shard_map/all_to_all | solution.py:33
  237.9 23.9 %all_to_all.65.h_ref = bf16[8,24,344]{2,1,0:T(8,128)(2,1)S(1)} all-to-all(bf16[8,24,344]{2,1,0:T(8,128)(2,1)S(1)} %broadcast_in_dim.17), channel_id=1, replica_groups=mesh['grp'=2,'kvh'=8,'kvp'=2,'tp'=16] {'kvh'}, dimensions={0} | all-to-all | bytes 264192 | tf_op jit(solution)/shard_map/all_to_all | solution.py:33
  262.8 12.1 %all-to-all-start.11 = ((bf16[32,24,128]{2,1,0:T(8,128)(2,1)}), bf16[32,24,128]{2,1,0:T(8,128)(2,1)S(1)}, u32[]{:S(2)}, u32[]{:S(2)}) async-start(bf16[32,24,128]{2,1,0:T(8,128)(2,1)} %bitcast.28), calls=%async_computation.11 | async-start | bytes 393216 | tf_op jit(solution)/shard_map/all_to_all | solution.py:33
  276.1 8.6 %all-to-all-done.11 = bf16[32,24,128]{2,1,0:T(8,128)(2,1)S(1)} async-done(((bf16[32,24,128]{2,1,0:T(8,128)(2,1)}), bf16[32,24,128]{2,1,0:T(8,128)(2,1)S(1)}, u32[]{:S(2)}, u32[]{:S(2)}) %all-to-all-start.11) | async-done | bytes 196640 | tf_op jit(solution)/shard_map/all_to_all | solution.py:33
  (93 shorter events, 19.6 us)
Async XLA Ops:
  0.6 182.1 %copy-start = (bf16[128,256]{1,0:T(8,128)(2,1)S(1)}, bf16[128,256]{1,0:T(8,128)(2,1)}, u32[]{:S(2)}) copy-start(bf16[128,256]{1,0:T(8,128)(2,1)} %param.30) | copy-start | bytes 196612
  0.6 46.7 %copy-start.5 = (bf16[256,688]{0,1:T(8,128)(2,1)S(1)}, bf16[256,688]{0,1:T(8,128)(2,1)}, u32[]{:S(2)}) copy-start(bf16[256,688]{0,1:T(8,128)(2,1)} %param.22) | copy-start | bytes 1056772
  2.1 55.2 %all-to-all-start = ((bf16[32,24,128]{2,1,0:T(8,128)(2,1)}), bf16[32,24,128]{2,1,0:T(8,128)(2,1)S(1)}, u32[]{:S(2)}, u32[]{:S(2)}) async-start(bf16[32,24,128]{2,1,0:T(8,128)(2,1)} %broadcast_in_dim.12), calls=%async_computation | async-start | bytes 393216 | tf_op jit(solution)/shard_map/all_to_all | solution.py:33
  49.0 3.8 %copy-start.6 = (bf16[256,688]{0,1:T(8,128)(2,1)S(1)}, bf16[256,688]{0,1:T(8,128)(2,1)}, u32[]{:S(2)}) copy-start(bf16[256,688]{0,1:T(8,128)(2,1)} %param.23) | copy-start | bytes 1056772
  49.1 11.2 %collective-permute-start = (bf16[2,344,256]{2,1,0:T(8,128)(2,1)S(1)}, bf16[2,344,256]{2,1,0:T(8,128)(2,1)S(1)}, u32[]{:S(2)}, u32[]{:S(2)}) collective-permute-start(bf16[2,344,256]{2,1,0:T(8,128)(2,1)S(1)} %pad_maximum_fusion), channel_id=1, source_target_pairs={{0,16},{16,0},{1,17},{17,1},{2,18},{18,2},{3,19},{19,3},{4,20},{20... | collective-permute-start | bytes 1056776 | tf_op jit(solution)/shard_map/ppermute | solution.py:172
  61.5 8.0 %copy-start.3 = (bf16[688,256]{1,0:T(8,128)(2,1)S(1)}, bf16[688,256]{1,0:T(8,128)(2,1)}, u32[]{:S(2)}) copy-start(bf16[688,256]{1,0:T(8,128)(2,1)} %param.24) | copy-start | bytes 1056772
  61.5 25.0 %all-to-all-start.1 = ((bf16[8,24,768]{2,1,0:T(8,128)(2,1)}), bf16[8,24,768]{2,1,0:T(8,128)(2,1)S(1)}, u32[]{:S(2)}, u32[]{:S(2)}) async-start(bf16[8,24,768]{2,1,0:T(8,128)(2,1)} %shard_map.185), calls=%async_computation.1 | async-start | bytes 589824 | tf_op jit(solution)/shard_map/all_to_all | solution.py:33
  69.5 18.2 %collective-permute-start.1 = (bf16[344,256]{1,0:T(8,128)(2,1)S(1)}, bf16[344,256]{1,0:T(8,128)(2,1)S(1)}, u32[]{:S(2)}, u32[]{:S(2)}) collective-permute-start(bf16[344,256]{1,0:T(8,128)(2,1)S(1)} %get-tuple-element.60), channel_id=1, source_target_pairs={{0,16},{16,0},{1,17},{17,1},{2,18},{18,2},{3,19},{19,3},{4,20},{20... | collective-permute-start | bytes 528392 | tf_op jit(solution)/shard_map/ppermute | solution.py:160
  134.3 4.6 %copy-start.9 = (bf16[256,128]{1,0:T(8,128)(2,1)S(1)}, bf16[256,128]{1,0:T(8,128)(2,1)}, u32[]{:S(2)}) copy-start(bf16[256,128]{1,0:T(8,128)(2,1)} %param.27) | copy-start | bytes 196612
  134.3 4.6 %copy-start.10 = (bf16[256,128]{1,0:T(8,128)(2,1)S(1)}, bf16[256,128]{1,0:T(8,128)(2,1)}, u32[]{:S(2)}) copy-start(bf16[256,128]{1,0:T(8,128)(2,1)} %param.26) | copy-start | bytes 196612
  134.3 4.6 %copy-start.11 = (bf16[256,128]{1,0:T(8,128)(2,1)S(1)}, bf16[256,128]{1,0:T(8,128)(2,1)}, u32[]{:S(2)}) copy-start(bf16[256,128]{1,0:T(8,128)(2,1)} %param.29) | copy-start | bytes 196612
  134.3 4.6 %copy-start.12 = (bf16[256,128]{1,0:T(8,128)(2,1)S(1)}, bf16[256,128]{1,0:T(8,128)(2,1)}, u32[]{:S(2)}) copy-start(bf16[256,128]{1,0:T(8,128)(2,1)} %param.28) | copy-start | bytes 196612
  134.3 14.3 %all-to-all-start.4 = ((bf16[32,24,128]{2,1,0:T(8,128)(2,1)}), bf16[32,24,128]{2,1,0:T(8,128)(2,1)S(1)}, u32[]{:S(2)}, u32[]{:S(2)}) async-start(bf16[32,24,128]{2,1,0:T(8,128)(2,1)} %broadcast_in_dim.14), calls=%async_computation.4 | async-start | bytes 393216 | tf_op jit(solution)/shard_map/all_to_all | solution.py:33
  139.7 23.9 %copy-start.1 = (f32[12,1,128,128]{3,2,1,0:T(8,128)S(1)}, f32[12,1,128,128]{3,2,1,0:T(8,128)}, u32[]{:S(2)}) copy-start(f32[12,1,128,128]{3,2,1,0:T(8,128)} %param.20) | copy-start | bytes 2359300
  139.8 8.8 %collective-permute-start.2 = (bf16[256,256]{1,0:T(8,128)(2,1)S(1)}, bf16[256,256]{1,0:T(8,128)(2,1)S(1)}, u32[]{:S(2)}, u32[]{:S(2)}) collective-permute-start(bf16[256,256]{1,0:T(8,128)(2,1)S(1)} %get-tuple-element.62), channel_id=1, source_target_pairs={{0,16},{16,0},{1,17},{17,1},{2,18},{18,2},{3,19},{19,3},{4,20},{20... | collective-permute-start | bytes 393224 | tf_op jit(solution)/shard_map/ppermute | solution.py:160
  198.4 5.0 %copy-start.7 = (bf16[256,688]{0,1:T(8,128)(2,1)S(1)}, bf16[256,688]{0,1:T(8,128)(2,1)}, u32[]{:S(2)}) copy-start(bf16[256,688]{0,1:T(8,128)(2,1)} %param.33) | copy-start | bytes 1056772
  198.4 5.0 %copy-start.8 = (bf16[256,688]{0,1:T(8,128)(2,1)S(1)}, bf16[256,688]{0,1:T(8,128)(2,1)}, u32[]{:S(2)}) copy-start(bf16[256,688]{0,1:T(8,128)(2,1)} %param.34) | copy-start | bytes 1056772
  199.1 13.7 %all-to-all-start.8 = ((bf16[32,24,128]{2,1,0:T(8,128)(2,1)}), bf16[32,24,128]{2,1,0:T(8,128)(2,1)S(1)}, u32[]{:S(2)}, u32[]{:S(2)}) async-start(bf16[32,24,128]{2,1,0:T(8,128)(2,1)} %broadcast_in_dim.16), calls=%async_computation.8 | async-start | bytes 393216 | tf_op jit(solution)/shard_map/all_to_all | solution.py:33
  203.3 0.7 copy-start.14
  204.1 11.2 %collective-permute-start.3 = (bf16[2,344,256]{2,1,0:T(8,128)(2,1)S(1)}, bf16[2,344,256]{2,1,0:T(8,128)(2,1)S(1)}, u32[]{:S(2)}, u32[]{:S(2)}) collective-permute-start(bf16[2,344,256]{2,1,0:T(8,128)(2,1)S(1)} %pad_maximum_fusion.2), channel_id=1, source_target_pairs={{0,16},{16,0},{1,17},{17,1},{2,18},{18,2},{3,19},{19,3},{4,20},{20... | collective-permute-start | bytes 1056776 | tf_op jit(solution)/shard_map/ppermute | solution.py:172
  216.5 3.8 %copy-start.4 = (bf16[688,256]{1,0:T(8,128)(2,1)S(1)}, bf16[688,256]{1,0:T(8,128)(2,1)}, u32[]{:S(2)}) copy-start(bf16[688,256]{1,0:T(8,128)(2,1)} %param.35) | copy-start | bytes 1056772
  216.5 20.2 %all-to-all-start.9 = ((bf16[8,24,768]{2,1,0:T(8,128)(2,1)}), bf16[8,24,768]{2,1,0:T(8,128)(2,1)S(1)}, u32[]{:S(2)}, u32[]{:S(2)}) async-start(bf16[8,24,768]{2,1,0:T(8,128)(2,1)} %shard_map.189), calls=%async_computation.9 | async-start | bytes 589824 | tf_op jit(solution)/shard_map/all_to_all | solution.py:33
  220.3 17.6 %collective-permute-start.4 = (bf16[344,256]{1,0:T(8,128)(2,1)S(1)}, bf16[344,256]{1,0:T(8,128)(2,1)S(1)}, u32[]{:S(2)}, u32[]{:S(2)}) collective-permute-start(bf16[344,256]{1,0:T(8,128)(2,1)S(1)} %get-tuple-element.58), channel_id=1, source_target_pairs={{0,16},{16,0},{1,17},{17,1},{2,18},{18,2},{3,19},{19,3},{4,20},{20... | collective-permute-start | bytes 528392 | tf_op jit(solution)/shard_map/ppermute | solution.py:160
  262.8 21.8 %all-to-all-start.11 = ((bf16[32,24,128]{2,1,0:T(8,128)(2,1)}), bf16[32,24,128]{2,1,0:T(8,128)(2,1)S(1)}, u32[]{:S(2)}, u32[]{:S(2)}) async-start(bf16[32,24,128]{2,1,0:T(8,128)(2,1)} %bitcast.28), calls=%async_computation.11 | async-start | bytes 393216 | tf_op jit(solution)/shard_map/all_to_all | solution.py:33
  (4 other events, 2.7 us)

commit v10 on v9

--- a/solution.py
+++ b/solution.py
@@ -91,7 +91,7 @@
     _, chunks, high, wide = out_ref.shape
     across = scr.shape[1] // wide
     for place, w in ((p, own_ref), (1 - p, got_ref)):
-        scr[...] = jnp.dot(h[...], w[...], preferred_element_type=jnp.float32)
+        scr[...] = jnp.dot(h[...], w[: h.shape[1]], preferred_element_type=jnp.float32)
         for n in range(chunks):
             if flat:
                 few = high // across
@@ -110,7 +110,8 @@
     each = rows // members
     squares = sum(jnp.sum(jnp.square(x[j].astype(jnp.float32)), axis=1, keepdims=True) for j in range(2))
     scr[:rows, :lanes] = sum(
-        jnp.dot(x[j], w[...], preferred_element_type=jnp.float32) for j, w in enumerate((own_ref, got_ref))
+        jnp.dot(x[j], w[w.shape[0] - x.shape[2] :], preferred_element_type=jnp.float32)
+        for j, w in enumerate((own_ref, got_ref))
     )
     scr[:rows, lanes:] = jnp.broadcast_to(squares, (rows, 128))
     scr[rows:] = jnp.zeros((scr.shape[0] - rows, scr.shape[1]), jnp.float32)
@@ -221,8 +222,9 @@
     cosine, sine, decay = tables
     count, _, width, _ = state.shape
     members = lax.axis_size(KV)
-    block, lanes = weights[0].shape
+    lanes = weights[0].shape[1]
     rows = members * count
+    block = gathered.size // (2 * rows)
     high = -(-(count + 1) // 8) * 8
     sent = local_call(
         heads_kernel,
@@ -285,42 +287,42 @@
     r, c = lax.div(t, across), lax.rem(t, across)
 
     half = ret_state.shape[-1] // 2
-    inverse = 10000.0 ** (-jnp.arange(half, dtype=jnp.float32) / half)
-    angles = positions.astype(jnp.float32)[:, None] * inverse[None, :]
     decay = jnp.exp(jnp.log1p(-(2.0 ** (-5.0 - t.astype(jnp.float32)))))
     place = lax.div(t * few, tall)
-    early = (angles, decay, place, t * few - place * tall)
+    early = (decay, place, t * few - place * tall)
 
     first_pair = paired_weights(first_gain, first_gate, first_up)
-    first_back = paired_rows(first_down)
     second_back = paired_rows(second_down)
     halves = [jnp.concatenate(w, axis=1) for w in ((w_query, w_key), (w_value, w_outgate))]
     halves = jnp.stack(halves).astype(jnp.float32) * mix_gain[:, None]
-    heads_pair = swapped(halves.astype(jnp.bfloat16))
+    downs = first_down.reshape(2, -1, block)
+    mix_pair = swapped(jnp.concatenate([downs, halves.astype(jnp.bfloat16)], axis=1))
 
     cuts = jnp.concatenate(jnp.split(stream_in, across, axis=1), axis=0)
     gathered = spread(cuts, BOTH).reshape(2, tp, tall, wide)
     own = lax.dynamic_slice(gathered, (p, r * across, c * few, 0), (1, across, few, wide)).reshape(tall, wide)
     gathered, own, early = lax.optimization_barrier((gathered, own, early))
-    angles, decay, place, offset = early
-    back = feed_forward(gathered, first_pair, first_back, False)
-    back, second_gain = lax.optimization_barrier((back, second_gain))
+    decay, place, offset = early
+    back = feed_forward(gathered, first_pair, mix_pair, False)
+    own = advance(own, back, 0.5, BOTH)
+    held = (own, positions, jnp.arange(half), second_gain)
+    own, positions, steps, second_gain = lax.optimization_barrier(held)
     second_pair = paired_weights(second_gain, second_gate, second_up)
-    own = advance(own, back, 0.5, BOTH)
     gathered = spread(own, BOTH).reshape(2, tp, tall, wide)
+    inverse = 10000.0 ** (-steps.astype(jnp.float32) / half)
+    angles = positions.astype(jnp.float32)[:, None] * inverse[None, :]
     cosine, sine = jnp.cos(angles), jnp.sin(angles)
     cosine, sine = jnp.concatenate([cosine, cosine], axis=1), jnp.concatenate([-sine, sine], axis=1)
     gathered, cosine, sine = lax.optimization_barrier((gathered, cosine, sine))
     decay = jnp.broadcast_to(decay, (1, 2 * half))
-    ret_out, new_state = retention(gathered, heads_pair, features, head_gain, ret_state, (cosine, sine, decay))
+    ret_out, new_state = retention(gathered, mix_pair, features, head_gain, ret_state, (cosine, sine, decay))
     back = jnp.dot(ret_out, w_out, preferred_element_type=jnp.float32).astype(jnp.bfloat16)
     back = back.reshape(groups, tall, across, wide).transpose(0, 2, 1, 3).reshape(tp, tall, wide)
     own = advance(own, back, 1.0, "tp")
     gathered = spread(own, BOTH).reshape(2, tp, tall, wide)
     own = lax.dynamic_slice(gathered, (p, place * across, offset, 0), (1, across, few, wide))[0]
     own = jnp.concatenate([own[i] for i in range(across)], axis=1)
-    gathered, own, early = lax.optimization_barrier((gathered, own, early))
-    angles, decay, place, offset = early
+    gathered, own = lax.optimization_barrier((gathered, own))
     back = feed_forward(gathered, second_pair, second_back, True)
     return advance(own, back, 0.5, BOTH), new_state
 

time: 286 us -> 287 us (level)
  waiting for transfers between devices: 56.4 us -> 63.2 us
  starting transfers between devices: 94.9 us -> 91.4 us
    all_to_all x6, waiting for transfers between devices: 49.2 us -> 53.1 us  [exchange(): return lax.all_to_all(x, axis, split_axis=0, concat_axis=0, tiled=True)]
    ppermute x3 -> x2, starting transfers between devices: 10.3 us -> 6.88 us  [swapped(): lax.ppermute(mine(both, 1 - p), 'kvp', [(0, 1), (1, 0)])]
    ppermute x3 -> x2, waiting for transfers between devices: 1.79 us -> 4.72 us  [swapped(): lax.ppermute(mine(both, 1 - p), 'kvp', [(0, 1), (1, 0)])]
  transfers between devices with their start and end apart: 11 -> 10, of which waited for: 10 -> 10; matrix products, arithmetic and copies ran while one was open for 1% -> 1% of each run, Pallas kernels for 0% -> 0%
where the time goes in v10:
time: 287 us; the launch traced here: 286 us
  blocking collectives  115 us (40%)
  starting transfers between devices  91.4 us (32%)
  waiting for transfers between devices  63.2 us (22%)
  local copies, waits for them, and re-layouts  5.96 us (2%)
  Pallas kernels  4.54 us (2%)
  other arithmetic  4.35 us (2%)
    all_to_all x6, blocking collectives, exchange(): return lax.all_to_all(x, axis, split_axis=0, concat_axis=0, tiled=True)  115 us
    all_to_all x6, starting transfers between devices, exchange(): return lax.all_to_all(x, axis, split_axis=0, concat_axis=0, tiled=True)  77.7 us
    all_to_all x6, waiting for transfers between devices, exchange(): return lax.all_to_all(x, axis, split_axis=0, concat_axis=0, tiled=True)  53.1 us
    ppermute x2, starting transfers between devices, swapped(): lax.ppermute(mine(both, 1 - p), 'kvp', [(0, 1), (1, 0)])  6.88 us
    ppermute x2, starting transfers between devices, paired_weights(): return (scaled(p, halves), lax.ppermute(sent, 'kvp', [(0, 1), (1, 0)]))  6.86 us
  transfers between devices with their start and end apart: 10, of which 10 were waited for; matrix products, arithmetic and copies ran while one was open for 1% of the time, Pallas kernels for 0%

profile of v10, /device:TPU:65, one launch (start us, length us, event | category | flops | bytes accessed | tf_op | source)
XLA Modules:
  0.0 286.0 jit_solution(640414966355827843)
XLA Ops:
  2.1 45.2 %all-to-all-start = ((bf16[32,24,128]{2,1,0:T(8,128)(2,1)}), bf16[32,24,128]{2,1,0:T(8,128)(2,1)S(1)}, u32[]{:S(2)}, u32[]{:S(2)}) async-start(bf16[32,24,128]{2,1,0:T(8,128)(2,1)} %broadcast_in_dim.12), calls=%async_computation | async-start | bytes 393216 | tf_op jit(solution)/shard_map/all_to_all | solution.py:33
  49.1 3.7 %collective-permute-start = (bf16[2,344,256]{2,1,0:T(8,128)(2,1)S(1)}, bf16[2,344,256]{2,1,0:T(8,128)(2,1)S(1)}, u32[]{:S(2)}, u32[]{:S(2)}) collective-permute-start(bf16[2,344,256]{2,1,0:T(8,128)(2,1)S(1)} %pad_maximum_fusion), channel_id=1, source_target_pairs={{0,16},{16,0},{1,17},{17,1},{2,18},{18,2},{3,19},{19,3},{4,20},{20... | collective-permute-start | bytes 1056776 | tf_op jit(solution)/shard_map/ppermute | solution.py:173
  53.1 4.3 %all-to-all-done = bf16[32,24,128]{2,1,0:T(8,128)(2,1)S(1)} async-done(((bf16[32,24,128]{2,1,0:T(8,128)(2,1)}), bf16[32,24,128]{2,1,0:T(8,128)(2,1)S(1)}, u32[]{:S(2)}, u32[]{:S(2)}) %all-to-all-start) | async-done | bytes 196640 | tf_op jit(solution)/shard_map/all_to_all | solution.py:33
  57.4 2.9 %collective-permute-done.got_ref = bf16[2,344,256]{2,1,0:T(8,128)(2,1)S(1)} collective-permute-done((bf16[2,344,256]{2,1,0:T(8,128)(2,1)S(1)}, bf16[2,344,256]{2,1,0:T(8,128)(2,1)S(1)}, u32[]{:S(2)}, u32[]{:S(2)}) %collective-permute-start) | collective-permute-done | bytes 352288 | tf_op jit(solution)/shard_map/ppermute | solution.py:173
  61.5 8.0 %all-to-all-start.1 = ((bf16[8,24,768]{2,1,0:T(8,128)(2,1)}), bf16[8,24,768]{2,1,0:T(8,128)(2,1)S(1)}, u32[]{:S(2)}, u32[]{:S(2)}) async-start(bf16[8,24,768]{2,1,0:T(8,128)(2,1)} %shard_map.185), calls=%async_computation.1 | async-start | bytes 589824 | tf_op jit(solution)/shard_map/all_to_all | solution.py:33
  70.6 3.6 %collective-permute-start.1 = (bf16[600,256]{1,0:T(8,128)(2,1)S(1)}, bf16[600,256]{1,0:T(8,128)(2,1)S(1)}, u32[]{:S(2)}, u32[]{:S(2)}) collective-permute-start(bf16[600,256]{1,0:T(8,128)(2,1)S(1)} %get-tuple-element.60), channel_id=1, source_target_pairs={{0,16},{16,0},{1,17},{17,1},{2,18},{18,2},{3,19},{19,3},{4,20},{20... | collective-permute-start | bytes 921608 | tf_op jit(solution)/shard_map/ppermute | solution.py:161
  74.2 12.3 %all-to-all-done.1 = bf16[8,24,768]{2,1,0:T(8,128)(2,1)S(1)} async-done(((bf16[8,24,768]{2,1,0:T(8,128)(2,1)}), bf16[8,24,768]{2,1,0:T(8,128)(2,1)S(1)}, u32[]{:S(2)}, u32[]{:S(2)}) %all-to-all-start.1) | async-done | bytes 294944 | tf_op jit(solution)/shard_map/all_to_all | solution.py:33
  86.8 3.8 %collective-permute-done.1.got_ref = bf16[600,256]{1,0:T(8,128)(2,1)S(1)} collective-permute-done((bf16[600,256]{1,0:T(8,128)(2,1)S(1)}, bf16[600,256]{1,0:T(8,128)(2,1)S(1)}, u32[]{:S(2)}, u32[]{:S(2)}) %collective-permute-start.1) | collective-permute-done | bytes 307232 | tf_op jit(solution)/shard_map/ppermute | solution.py:161
  90.6 23.6 %all_to_all.60.h_ref = bf16[8,24,344]{2,1,0:T(8,128)(2,1)S(1)} all-to-all(bf16[8,24,344]{2,1,0:T(8,128)(2,1)S(1)} %broadcast_in_dim.13), channel_id=1, replica_groups=mesh['grp'=2,'kvh'=8,'kvp'=2,'tp'=16] {'kvh'}, dimensions={0} | all-to-all | bytes 264192 | tf_op jit(solution)/shard_map/all_to_all | solution.py:33
  114.5 21.8 %all_to_all.61 = bf16[32,24,128]{2,1,0:T(8,128)(2,1)S(1)} all-to-all(bf16[32,24,128]{2,1,0:T(8,128)(2,1)S(1)} %bitcast.48), channel_id=1, replica_groups=mesh['grp'=2,'kvh'=8,'kvp'=2,'tp'=16] {'kvp','tp'}, dimensions={0} | all-to-all | bytes 393216 | tf_op jit(solution)/shard_map/all_to_all | solution.py:33
  137.1 4.6 %all-to-all-start.4 = ((bf16[32,24,128]{2,1,0:T(8,128)(2,1)}), bf16[32,24,128]{2,1,0:T(8,128)(2,1)S(1)}, u32[]{:S(2)}, u32[]{:S(2)}) async-start(bf16[32,24,128]{2,1,0:T(8,128)(2,1)} %broadcast_in_dim.14), calls=%async_computation.4 | async-start | bytes 393216 | tf_op jit(solution)/shard_map/all_to_all | solution.py:33
  142.0 9.4 %all-to-all-done.4 = bf16[32,24,128]{2,1,0:T(8,128)(2,1)S(1)} async-done(((bf16[32,24,128]{2,1,0:T(8,128)(2,1)}), bf16[32,24,128]{2,1,0:T(8,128)(2,1)S(1)}, u32[]{:S(2)}, u32[]{:S(2)}) %all-to-all-start.4) | async-done | bytes 196640 | tf_op jit(solution)/shard_map/all_to_all | solution.py:33
  151.7 14.8 %all_to_all.62.z_ref = bf16[16,16,256]{2,1,0:T(8,128)(2,1)S(1)} all-to-all(bf16[16,16,256]{2,1,0:T(8,128)(2,1)S(1)} %shard_map.187), channel_id=1, replica_groups=mesh['grp'=2,'kvh'=8,'kvp'=2,'tp'=16] {'kvh','kvp'}, dimensions={0} | all-to-all | bytes 262144 | tf_op jit(solution)/shard_map/all_to_all | solution.py:33
  167.9 17.7 %all_to_all.63 = bf16[16,12,128]{2,1,0:T(8,128)(2,1)S(1)} all-to-all(bf16[16,12,128]{2,1,0:T(8,128)(2,1)S(1)} %get-tuple-element.46), channel_id=1, replica_groups=mesh['grp'=2,'kvh'=8,'kvp'=2,'tp'=16] {'kvh','kvp'}, dimensions={0} | all-to-all | bytes 98304 | tf_op jit(solution)/shard_map/all_to_all | solution.py:33
  185.8 13.3 %all_to_all.64 = bf16[16,24,128]{2,1,0:T(8,128)(2,1)S(1)} all-to-all(bf16[16,24,128]{2,1,0:T(8,128)(2,1)S(1)} %bitcast.50), channel_id=1, replica_groups=mesh['grp'=2,'kvh'=8,'kvp'=2,'tp'=16] {'tp'}, dimensions={0} | all-to-all | bytes 196608 | tf_op jit(solution)/shard_map/all_to_all | solution.py:33
  199.8 4.2 %all-to-all-start.8 = ((bf16[32,24,128]{2,1,0:T(8,128)(2,1)}), bf16[32,24,128]{2,1,0:T(8,128)(2,1)S(1)}, u32[]{:S(2)}, u32[]{:S(2)}) async-start(bf16[32,24,128]{2,1,0:T(8,128)(2,1)} %broadcast_in_dim.16), calls=%async_computation.8 | async-start | bytes 393216 | tf_op jit(solution)/shard_map/all_to_all | solution.py:33
  204.8 3.1 %collective-permute-start.2 = (bf16[2,344,256]{2,1,0:T(8,128)(2,1)S(1)}, bf16[2,344,256]{2,1,0:T(8,128)(2,1)S(1)}, u32[]{:S(2)}, u32[]{:S(2)}) collective-permute-start(bf16[2,344,256]{2,1,0:T(8,128)(2,1)S(1)} %pad_maximum_fusion.2), channel_id=1, source_target_pairs={{0,16},{16,0},{1,17},{17,1},{2,18},{18,2},{3,19},{19,3},{4,20},{20... | collective-permute-start | bytes 1056776 | tf_op jit(solution)/shard_map/ppermute | solution.py:173
  208.1 5.5 %all-to-all-done.8 = bf16[32,24,128]{2,1,0:T(8,128)(2,1)S(1)} async-done(((bf16[32,24,128]{2,1,0:T(8,128)(2,1)}), bf16[32,24,128]{2,1,0:T(8,128)(2,1)S(1)}, u32[]{:S(2)}, u32[]{:S(2)}) %all-to-all-start.8) | async-done | bytes 196640 | tf_op jit(solution)/shard_map/all_to_all | solution.py:33
  217.2 3.8 %all-to-all-start.9 = ((bf16[8,24,768]{2,1,0:T(8,128)(2,1)}), bf16[8,24,768]{2,1,0:T(8,128)(2,1)S(1)}, u32[]{:S(2)}, u32[]{:S(2)}) async-start(bf16[8,24,768]{2,1,0:T(8,128)(2,1)} %shard_map.189), calls=%async_computation.9 | async-start | bytes 589824 | tf_op jit(solution)/shard_map/all_to_all | solution.py:33
  221.0 3.3 %collective-permute-start.3 = (bf16[344,256]{1,0:T(8,128)(2,1)S(1)}, bf16[344,256]{1,0:T(8,128)(2,1)S(1)}, u32[]{:S(2)}, u32[]{:S(2)}) collective-permute-start(bf16[344,256]{1,0:T(8,128)(2,1)S(1)} %get-tuple-element.62), channel_id=1, source_target_pairs={{0,16},{16,0},{1,17},{17,1},{2,18},{18,2},{3,19},{19,3},{4,20},{20... | collective-permute-start | bytes 528392 | tf_op jit(solution)/shard_map/ppermute | solution.py:161
  224.3 13.0 %all-to-all-done.9 = bf16[8,24,768]{2,1,0:T(8,128)(2,1)S(1)} async-done(((bf16[8,24,768]{2,1,0:T(8,128)(2,1)}), bf16[8,24,768]{2,1,0:T(8,128)(2,1)S(1)}, u32[]{:S(2)}, u32[]{:S(2)}) %all-to-all-start.9) | async-done | bytes 294944 | tf_op jit(solution)/shard_map/all_to_all | solution.py:33
  238.6 23.9 %all_to_all.65.h_ref = bf16[8,24,344]{2,1,0:T(8,128)(2,1)S(1)} all-to-all(bf16[8,24,344]{2,1,0:T(8,128)(2,1)S(1)} %broadcast_in_dim.17), channel_id=1, replica_groups=mesh['grp'=2,'kvh'=8,'kvp'=2,'tp'=16] {'kvh'}, dimensions={0} | all-to-all | bytes 264192 | tf_op jit(solution)/shard_map/all_to_all | solution.py:33
  263.5 12.0 %all-to-all-start.11 = ((bf16[32,24,128]{2,1,0:T(8,128)(2,1)}), bf16[32,24,128]{2,1,0:T(8,128)(2,1)S(1)}, u32[]{:S(2)}, u32[]{:S(2)}) async-start(bf16[32,24,128]{2,1,0:T(8,128)(2,1)} %bitcast.26), calls=%async_computation.11 | async-start | bytes 393216 | tf_op jit(solution)/shard_map/all_to_all | solution.py:33
  276.8 8.6 %all-to-all-done.11 = bf16[32,24,128]{2,1,0:T(8,128)(2,1)S(1)} async-done(((bf16[32,24,128]{2,1,0:T(8,128)(2,1)}), bf16[32,24,128]{2,1,0:T(8,128)(2,1)S(1)}, u32[]{:S(2)}, u32[]{:S(2)}) %all-to-all-start.11) | async-done | bytes 196640 | tf_op jit(solution)/shard_map/all_to_all | solution.py:33
  (90 shorter events, 18.4 us)
Async XLA Ops:
  0.6 184.9 %copy-start = (bf16[128,256]{1,0:T(8,128)(2,1)S(1)}, bf16[128,256]{1,0:T(8,128)(2,1)}, u32[]{:S(2)}) copy-start(bf16[128,256]{1,0:T(8,128)(2,1)} %param.30) | copy-start | bytes 196612
  0.6 46.7 %copy-start.5 = (bf16[256,688]{0,1:T(8,128)(2,1)S(1)}, bf16[256,688]{0,1:T(8,128)(2,1)}, u32[]{:S(2)}) copy-start(bf16[256,688]{0,1:T(8,128)(2,1)} %param.22) | copy-start | bytes 1056772
  2.1 55.2 %all-to-all-start = ((bf16[32,24,128]{2,1,0:T(8,128)(2,1)}), bf16[32,24,128]{2,1,0:T(8,128)(2,1)S(1)}, u32[]{:S(2)}, u32[]{:S(2)}) async-start(bf16[32,24,128]{2,1,0:T(8,128)(2,1)} %broadcast_in_dim.12), calls=%async_computation | async-start | bytes 393216 | tf_op jit(solution)/shard_map/all_to_all | solution.py:33
  49.0 3.9 %copy-start.6 = (bf16[256,688]{0,1:T(8,128)(2,1)S(1)}, bf16[256,688]{0,1:T(8,128)(2,1)}, u32[]{:S(2)}) copy-start(bf16[256,688]{0,1:T(8,128)(2,1)} %param.23) | copy-start | bytes 1056772
  49.1 11.2 %collective-permute-start = (bf16[2,344,256]{2,1,0:T(8,128)(2,1)S(1)}, bf16[2,344,256]{2,1,0:T(8,128)(2,1)S(1)}, u32[]{:S(2)}, u32[]{:S(2)}) collective-permute-start(bf16[2,344,256]{2,1,0:T(8,128)(2,1)S(1)} %pad_maximum_fusion), channel_id=1, source_target_pairs={{0,16},{16,0},{1,17},{17,1},{2,18},{18,2},{3,19},{19,3},{4,20},{20... | collective-permute-start | bytes 1056776 | tf_op jit(solution)/shard_map/ppermute | solution.py:173
  61.5 8.0 %copy-start.9 = (bf16[256,128]{1,0:T(8,128)(2,1)S(1)}, bf16[256,128]{1,0:T(8,128)(2,1)}, u32[]{:S(2)}) copy-start(bf16[256,128]{1,0:T(8,128)(2,1)} %param.27) | copy-start | bytes 196612
  61.5 8.0 %copy-start.10 = (bf16[256,128]{1,0:T(8,128)(2,1)S(1)}, bf16[256,128]{1,0:T(8,128)(2,1)}, u32[]{:S(2)}) copy-start(bf16[256,128]{1,0:T(8,128)(2,1)} %param.26) | copy-start | bytes 196612
  61.5 8.0 %copy-start.11 = (bf16[256,128]{1,0:T(8,128)(2,1)S(1)}, bf16[256,128]{1,0:T(8,128)(2,1)}, u32[]{:S(2)}) copy-start(bf16[256,128]{1,0:T(8,128)(2,1)} %param.29) | copy-start | bytes 196612
  61.5 8.0 %copy-start.12 = (bf16[256,128]{1,0:T(8,128)(2,1)S(1)}, bf16[256,128]{1,0:T(8,128)(2,1)}, u32[]{:S(2)}) copy-start(bf16[256,128]{1,0:T(8,128)(2,1)} %param.28) | copy-start | bytes 196612
  61.5 25.0 %all-to-all-start.1 = ((bf16[8,24,768]{2,1,0:T(8,128)(2,1)}), bf16[8,24,768]{2,1,0:T(8,128)(2,1)S(1)}, u32[]{:S(2)}, u32[]{:S(2)}) async-start(bf16[8,24,768]{2,1,0:T(8,128)(2,1)} %shard_map.185), calls=%async_computation.1 | async-start | bytes 589824 | tf_op jit(solution)/shard_map/all_to_all | solution.py:33
  69.5 0.7 copy-start.15
  69.5 1.0 copy-start.3
  70.6 20.0 %collective-permute-start.1 = (bf16[600,256]{1,0:T(8,128)(2,1)S(1)}, bf16[600,256]{1,0:T(8,128)(2,1)S(1)}, u32[]{:S(2)}, u32[]{:S(2)}) collective-permute-start(bf16[600,256]{1,0:T(8,128)(2,1)S(1)} %get-tuple-element.60), channel_id=1, source_target_pairs={{0,16},{16,0},{1,17},{17,1},{2,18},{18,2},{3,19},{19,3},{4,20},{20... | collective-permute-start | bytes 921608 | tf_op jit(solution)/shard_map/ppermute | solution.py:161
  136.4 5.3 %copy-start.16 = (s32[12]{0:T(128)S(1)}, s32[12]{0:T(128)}, u32[]{:S(2)}) copy-start(s32[12]{0:T(128)} %param.19) | copy-start | bytes 148
  137.1 29.4 %copy-start.1 = (f32[12,1,128,128]{3,2,1,0:T(8,128)S(1)}, f32[12,1,128,128]{3,2,1,0:T(8,128)}, u32[]{:S(2)}) copy-start(f32[12,1,128,128]{3,2,1,0:T(8,128)} %param.20) | copy-start | bytes 2359300
  137.1 14.3 %all-to-all-start.4 = ((bf16[32,24,128]{2,1,0:T(8,128)(2,1)}), bf16[32,24,128]{2,1,0:T(8,128)(2,1)S(1)}, u32[]{:S(2)}, u32[]{:S(2)}) async-start(bf16[32,24,128]{2,1,0:T(8,128)(2,1)} %broadcast_in_dim.14), calls=%async_computation.4 | async-start | bytes 393216 | tf_op jit(solution)/shard_map/all_to_all | solution.py:33
  199.1 5.0 %copy-start.7 = (bf16[256,688]{0,1:T(8,128)(2,1)S(1)}, bf16[256,688]{0,1:T(8,128)(2,1)}, u32[]{:S(2)}) copy-start(bf16[256,688]{0,1:T(8,128)(2,1)} %param.33) | copy-start | bytes 1056772
  199.1 5.0 %copy-start.8 = (bf16[256,688]{0,1:T(8,128)(2,1)S(1)}, bf16[256,688]{0,1:T(8,128)(2,1)}, u32[]{:S(2)}) copy-start(bf16[256,688]{0,1:T(8,128)(2,1)} %param.34) | copy-start | bytes 1056772
  199.8 13.7 %all-to-all-start.8 = ((bf16[32,24,128]{2,1,0:T(8,128)(2,1)}), bf16[32,24,128]{2,1,0:T(8,128)(2,1)S(1)}, u32[]{:S(2)}, u32[]{:S(2)}) async-start(bf16[32,24,128]{2,1,0:T(8,128)(2,1)} %broadcast_in_dim.16), calls=%async_computation.8 | async-start | bytes 393216 | tf_op jit(solution)/shard_map/all_to_all | solution.py:33
  204.8 11.2 %collective-permute-start.2 = (bf16[2,344,256]{2,1,0:T(8,128)(2,1)S(1)}, bf16[2,344,256]{2,1,0:T(8,128)(2,1)S(1)}, u32[]{:S(2)}, u32[]{:S(2)}) collective-permute-start(bf16[2,344,256]{2,1,0:T(8,128)(2,1)S(1)} %pad_maximum_fusion.2), channel_id=1, source_target_pairs={{0,16},{16,0},{1,17},{17,1},{2,18},{18,2},{3,19},{19,3},{4,20},{20... | collective-permute-start | bytes 1056776 | tf_op jit(solution)/shard_map/ppermute | solution.py:173
  217.2 3.8 %copy-start.4 = (bf16[688,256]{1,0:T(8,128)(2,1)S(1)}, bf16[688,256]{1,0:T(8,128)(2,1)}, u32[]{:S(2)}) copy-start(bf16[688,256]{1,0:T(8,128)(2,1)} %param.35) | copy-start | bytes 1056772
  217.2 20.1 %all-to-all-start.9 = ((bf16[8,24,768]{2,1,0:T(8,128)(2,1)}), bf16[8,24,768]{2,1,0:T(8,128)(2,1)S(1)}, u32[]{:S(2)}, u32[]{:S(2)}) async-start(bf16[8,24,768]{2,1,0:T(8,128)(2,1)} %shard_map.189), calls=%async_computation.9 | async-start | bytes 589824 | tf_op jit(solution)/shard_map/all_to_all | solution.py:33
  221.0 17.6 %collective-permute-start.3 = (bf16[344,256]{1,0:T(8,128)(2,1)S(1)}, bf16[344,256]{1,0:T(8,128)(2,1)S(1)}, u32[]{:S(2)}, u32[]{:S(2)}) collective-permute-start(bf16[344,256]{1,0:T(8,128)(2,1)S(1)} %get-tuple-element.62), channel_id=1, source_target_pairs={{0,16},{16,0},{1,17},{17,1},{2,18},{18,2},{3,19},{19,3},{4,20},{20... | collective-permute-start | bytes 528392 | tf_op jit(solution)/shard_map/ppermute | solution.py:161
  263.5 21.8 %all-to-all-start.11 = ((bf16[32,24,128]{2,1,0:T(8,128)(2,1)}), bf16[32,24,128]{2,1,0:T(8,128)(2,1)S(1)}, u32[]{:S(2)}, u32[]{:S(2)}) async-start(bf16[32,24,128]{2,1,0:T(8,128)(2,1)} %bitcast.26), calls=%async_computation.11 | async-start | bytes 393216 | tf_op jit(solution)/shard_map/all_to_all | solution.py:33
  (3 other events, 2.0 us)
